TPU v7x, 512 devices: a whole 4x8x8 slice. The times are simulated.
512 devices in a mesh: sp: 32 (over z, x), tp: 16 (over y, core).
Axes of the slice: x: 4, y: 8, z: 8, core: 2. Of those that a mesh axis runs over, the one named last changes fastest.
Arguments:
- resid: bfloat16 [16384, 2048], P(('sp', 'tp')), may hold values from -6 to 6
- recurrent_input: bfloat16 [16384, 2048], P('sp', 'tp'), may hold values from -12.2 to 12.2
- recurrent_out_gate: bfloat16 [16384, 2048], P('sp', 'tp'), may hold values from -6 to 6
- filter_weight: float32 [4, 2048], P(None, 'tp'), may hold values from -3 to 3
- recurrence_gate_matrix: bfloat16 [32, 64, 64], P('tp'), may hold values from -0.75 to 0.75
- input_gate_matrix: bfloat16 [32, 64, 64], P('tp'), may hold values from -0.75 to 0.75
- channel_decay_raw: float32 [2048], P('tp'), may hold values from 4.8 to 13.5
- token_decay_boost: float32 [16384, 2048], P('sp', 'tp'), may hold values from -0.7 to 0
- output_projection_weight: bfloat16 [2048, 2048], P('tp'), may hold values from -0.375 to 0.375
- expert_norm_gain: float32 [2048], replicated, may hold values from 0.1 to 1.9
- routes: int32 [16384, 2], P('sp'), may hold values from 0 to 31, all different within a row; in each aligned block of 32 rows (0 to 31, 32 to 63, ...) at most 3 rows name the same one
- expert_pair_weight: float32 [16384, 2], P(('sp', 'tp')), may hold values from 0.2 to 0.8
- gate_weight: bfloat16 [32, 2048, 2048], P('sp', None, 'tp'), may hold values from -0.125 to 0.125
- up_weight: bfloat16 [32, 2048, 2048], P('sp', None, 'tp'), may hold values from -0.125 to 0.125
- down_weight: bfloat16 [32, 2048, 2048], P('sp', None, 'tp'), may hold values from -0.25 to 0.25
Outputs:
- layer_out: bfloat16 [16384, 2048], P(('sp', 'tp'))
Inputs may be any that keep to these rules, and one draw needn't show every extreme that they name: `routes`: in each aligned block of 32 rows no expert is named by more than 3 rows, and the two experts of a row differ.
All inputs are finite; a program needn't handle non-finite values.
Results may differ from a plain program's by a relative error of at most 0.013.
Values may be sent and summed in bfloat16 or wider, within the bound.
No kernel may reach another device: no remote copies, remote signals or barrier semaphores. Data moves between devices by JAX's collectives and lax.ppermute only.
A program may use at most 64 MiB of HBM per device.

v0:
```python
import jax
import jax.numpy as jnp
from jax import lax
from jax.sharding import PartitionSpec as P

RECURRENT_SCALE = 8.0
EPSILON = 1e-06


def shifted(block, axis, distance):
    devices = range(lax.axis_size(axis))
    route = [(i - distance, i) for i in devices if i - distance in devices]
    return lax.ppermute(block, axis, route)


def from_everyone(x, axis):
    size = lax.axis_size(axis)
    return lax.all_to_all(jnp.broadcast_to(x[None], (size, *x.shape)), axis, 0, 0, tiled=True)


def collected_together(x, axis):
    leaves = jax.tree.leaves(x)
    order = sorted(range(len(leaves)), key=lambda k: -leaves[k].size)
    width = (1, *leaves[order[0]].shape)[-1]
    lines = [
        jnp.pad(leaves[k].reshape(-1), (0, -leaves[k].size % width)).reshape(-1, width)
        for k in order
    ]
    both, at, found = (from_everyone(jnp.concatenate(lines), axis), 0, {})
    for k, line in zip(order, lines):
        slab = both[:, at : at + len(line)].reshape(len(both), -1)
        found[k] = slab[:, : leaves[k].size].reshape(-1, *leaves[k].shape)
        at += len(line)
    numbers = iter(range(len(leaves)))
    return jax.tree.map(lambda _: found[next(numbers)], x)


def joined_by_halves(pieces, combine):
    while len(jax.tree.leaves(pieces)[0]) > 1:
        pieces = jax.vmap(combine)(
            *(jax.tree.map(lambda part: part[side::2], pieces) for side in (0, 1))
        )
    return jax.tree.map(lambda part: part[0], pieces)


def carried_in(x, axis, combine, identity):
    size, position = (lax.axis_size(axis), lax.axis_index(axis))
    passed = jnp.arange(size) < position

    def kept(part, zero, own):
        part = jnp.where(
            passed.reshape(-1, *(1 for _ in own.shape)), part, jnp.asarray(zero, own.dtype)
        )
        return part

    pieces = collected_together(x, axis)
    return joined_by_halves(jax.tree.map(kept, pieces, identity, x), combine)


def split_up(x, dim, size):
    before, after = (x.shape[:dim], x.shape[dim + 1 :])
    return jnp.moveaxis(x.reshape(*before, size, -1, *after), dim, 0)


def sum_at_owner(x, axis, dim):
    pieces = split_up(x, dim, lax.axis_size(axis))
    arrived = lax.all_to_all(pieces, axis, split_axis=0, concat_axis=0, tiled=True)
    return arrived.astype(jnp.float32).sum(axis=0)


def in_order(pieces, dim):
    pieces = jnp.moveaxis(pieces, 0, dim)
    dims = pieces.shape
    return pieces.reshape(*dims[:dim], dims[dim] * dims[dim + 1], *dims[dim + 2 :])


def piecewise(x, axis, dim, work, out_dim):
    extent = x.shape[dim]
    pieces = jnp.split(x, 2, axis=dim) if extent % 2 == 0 else [x]
    first = jnp.arange(lax.axis_size(axis)) * extent
    blocks = [lax.all_gather(slab, axis) for slab in pieces]
    made = [jax.vmap(work)(b, first + k * (extent // len(pieces))) for k, b in enumerate(blocks)]
    return in_order(jnp.concatenate(made, axis=out_dim + 1), out_dim)


def chain_step(earlier, later):
    return (earlier[0] * later[0], later[0] * earlier[1] + later[1])


def slot_numbers(picks, experts):
    flat = picks.reshape(-1)
    onehot = (flat[:, None] == jnp.arange(experts, dtype=jnp.int32)[None, :]).astype(jnp.int32)
    before = jnp.cumsum(onehot, axis=0) - onehot
    return (flat, jnp.sum(before * onehot, axis=1))


def fill_slots(source_rows, slot_of, row_of, slot_count):
    match = slot_of[None, :] == jnp.arange(slot_count, dtype=jnp.int32)[:, None]
    picked = jnp.sum(jnp.where(match, row_of[None, :], 0), axis=1)
    present = jnp.any(match, axis=1)
    return jnp.where(present[:, None], source_rows[picked], jnp.zeros((), source_rows.dtype))


def expert_hidden(rows, gate_weight, up_weight):
    gate = jnp.dot(rows, gate_weight[0], preferred_element_type=jnp.float32)
    upward = jnp.dot(rows, up_weight[0], preferred_element_type=jnp.float32)
    return (jax.nn.silu(gate) * upward).astype(jnp.bfloat16)


def expert_down(active, down_weight):
    columns = down_weight[0]
    return jnp.dot(
        lax.all_gather(active, "tp", axis=1, tiled=True),
        columns,
        preferred_element_type=jnp.float32,
    ).astype(jnp.bfloat16)


def body(
    resid,
    recurrent_input,
    recurrent_out_gate,
    filter_weight,
    recurrence_gate_matrix,
    input_gate_matrix,
    channel_decay_raw,
    token_decay_boost,
    output_projection_weight,
    expert_norm_gain,
    routes,
    expert_pair_weight,
    gate_weight,
    up_weight,
    down_weight,
):
    tokens_here, channels = recurrent_input.shape
    taps = filter_weight.shape[0]
    rim = shifted(recurrent_input[tokens_here - taps + 1 :], "sp", 1)
    extended = jnp.concatenate([rim, recurrent_input], axis=0).astype(jnp.float32)
    mixed_in = extended[0:tokens_here] * filter_weight[0]
    for offset in range(1, taps):
        mixed_in = mixed_in + extended[offset : offset + tokens_here] * filter_weight[offset]
    smoothed = mixed_in.astype(jnp.bfloat16)
    grouped = smoothed.reshape(
        tokens_here, recurrence_gate_matrix.shape[0], recurrence_gate_matrix.shape[1]
    )
    recurrence_gate = jax.nn.sigmoid(
        jnp.einsum(
            "tni,nij->tnj", grouped, recurrence_gate_matrix, preferred_element_type=jnp.float32
        ).reshape(tokens_here, channels)
    )
    input_gate = jax.nn.sigmoid(
        jnp.einsum(
            "tni,nij->tnj", grouped, input_gate_matrix, preferred_element_type=jnp.float32
        ).reshape(tokens_here, channels)
    )
    decay_logarithm = (
        -RECURRENT_SCALE * recurrence_gate * jax.nn.softplus(-channel_decay_raw) + token_decay_boost
    )
    decay = jnp.exp(decay_logarithm)
    drive = jnp.sqrt(-jnp.expm1(2.0 * decay_logarithm)) * (
        input_gate * smoothed.astype(jnp.float32)
    )
    running, local_state = lax.associative_scan(chain_step, (decay, drive), axis=0)
    identity = (jnp.ones((channels,), jnp.float32), jnp.zeros((channels,), jnp.float32))
    carried = carried_in((running[-1], local_state[-1]), "sp", chain_step, identity)
    state = local_state + running * carried[1][None, :]
    branch = (jax.nn.gelu(recurrent_out_gate.astype(jnp.float32)) * state).astype(jnp.bfloat16)
    tp_size = lax.axis_size("tp")
    rows_dev = tokens_here // tp_size
    projected = sum_at_owner(
        jnp.dot(branch, output_projection_weight, preferred_element_type=jnp.float32).astype(
            jnp.bfloat16
        ),
        "tp",
        0,
    )
    stream = (resid.astype(jnp.float32) + projected).astype(jnp.bfloat16)
    stream_wide = stream.astype(jnp.float32)
    normed = (
        stream_wide
        * lax.rsqrt(jnp.mean(stream_wide * stream_wide, axis=1, keepdims=True) + EPSILON)
        * expert_norm_gain
    ).astype(jnp.bfloat16)
    model_width = normed.shape[1]
    experts = lax.axis_size("sp")
    capacity = max(2, 3 * rows_dev // experts)
    own_routes = lax.dynamic_slice_in_dim(routes, lax.axis_index("tp") * rows_dev, rows_dev, 0)
    own_flat, own_rank = slot_numbers(own_routes, experts)
    own_slots = own_flat * capacity + own_rank
    row_of = jnp.arange(2 * rows_dev, dtype=jnp.int32) // 2
    outgoing = fill_slots(normed, own_slots, row_of, experts * capacity).reshape(
        experts, capacity, model_width
    )
    arrived = lax.all_to_all(outgoing, "sp", split_axis=0, concat_axis=0, tiled=True)

    def hidden_piece(piece, start):
        flat_rows = piece.reshape(piece.shape[0] * piece.shape[1], model_width)
        return expert_hidden(flat_rows, gate_weight, up_weight).reshape(
            piece.shape[0], piece.shape[1], -1
        )

    active = piecewise(
        arrived.reshape(1, experts * capacity, model_width), "tp", 0, hidden_piece, 0
    )
    result = expert_down(active.reshape(-1, active.shape[2]), down_weight)
    joined = lax.all_to_all(
        result.reshape(tp_size, experts * capacity, -1),
        "tp",
        split_axis=0,
        concat_axis=2,
        tiled=True,
    )
    returned = lax.all_to_all(
        joined.reshape(experts, capacity, model_width),
        "sp",
        split_axis=0,
        concat_axis=0,
        tiled=True,
    )
    picked = (
        returned.reshape(experts * capacity, model_width)[own_slots]
        .astype(jnp.float32)
        .reshape(rows_dev, 2, model_width)
    )
    blended = jnp.sum(picked * expert_pair_weight[:, :, None], axis=1)
    return (stream_wide + blended).astype(jnp.bfloat16)


def solution(mesh):
    placed = (
        P(("sp", "tp"), None),
        P("sp", "tp"),
        P("sp", "tp"),
        P(None, "tp"),
        P("tp", None, None),
        P("tp", None, None),
        P("tp"),
        P("sp", "tp"),
        P("tp", None),
        P(),
        P("sp", None),
        P(("sp", "tp"), None),
        P("sp", None, "tp"),
        P("sp", None, "tp"),
        P("sp", None, "tp"),
    )
    return jax.shard_map(
        body, mesh=mesh, in_specs=placed, out_specs=P(("sp", "tp"), None), check_vma=False
    )
```

profile of v0, /device:TPU:1, one launch (start us, length us, event | category | flops | bytes accessed | tf_op | source)
XLA Modules:
  0.0 395.4 jit_solution(9061123407506774359)
XLA Ops:
  6.5 0.7 slice.359
  7.4 3.9 collective-permute-start
  11.4 0.8 slice_bitcast_fusion.3
  12.2 0.7 fusion.50
  12.9 1.0 copy.85
  13.9 1.1 copy.87
  15.0 1.0 copy.83
  16.5 1.0 fusion.12
  17.5 1.0 fusion.15
  19.0 4.5 %slice.371 = f32[256,128]{0,1:T(8,128)S(1)} slice(f32[512,128]{0,1:T(8,128)S(1)} %get-tuple-element.9), slice={[0:511:2], [0:128:1]} | slice | bytes 262144 | tf_op jit(solution)/shard_map/slice | solution.py:164
  23.5 4.5 %slice.372 = f32[256,128]{0,1:T(8,128)S(1)} slice(f32[512,128]{0,1:T(8,128)S(1)} %get-tuple-element.9), slice={[1:512:2], [0:128:1]} | slice | bytes 262144 | tf_op jit(solution)/shard_map/slice | solution.py:164
  27.9 4.5 %slice.370 = f32[256,128]{0,1:T(8,128)S(1)} slice(f32[512,128]{0,1:T(8,128)S(1)} %get-tuple-element.10), slice={[1:512:2], [0:128:1]} | slice | bytes 262144 | tf_op jit(solution)/shard_map/slice | solution.py:164
  32.4 4.7 %slice.374 = f32[256,128]{0,1:T(8,128)S(1)} slice(f32[512,128]{0,1:T(8,128)S(1)} %get-tuple-element.10), slice={[0:511:2], [0:128:1]} | slice | bytes 262144 | tf_op jit(solution)/shard_map/slice | solution.py:164
  37.2 2.2 slice.377
  39.4 2.2 slice.378
  41.6 2.2 slice.376
  43.9 2.2 slice.380
  46.1 1.1 slice.383
  47.2 1.2 slice.384
  48.4 1.2 slice.382
  49.6 1.1 slice.386
  51.9 1.1 slice.388
  57.0 0.8 add_multiply_fusion.15
  60.4 1.1 slice.381
  61.5 1.1 slice.430
  62.7 2.2 slice.375
  64.9 2.2 slice.432
  67.1 4.5 %slice.369 = f32[255,128]{0,1:T(8,128)S(1)} slice(f32[512,128]{0,1:T(8,128)S(1)} %get-tuple-element.10), slice={[2:512:2], [0:128:1]} | slice | bytes 261120 | tf_op jit(solution)/shard_map/slice | solution.py:164
  71.6 4.6 %slice.434 = f32[255,128]{0,1:T(8,128)S(1)} slice(f32[512,128]{0,1:T(8,128)S(1)} %get-tuple-element.9), slice={[2:512:2], [0:128:1]} | slice | bytes 261120 | tf_op jit(solution)/shard_map/slice | solution.py:164
  76.3 0.9 copy.113
  84.7 1.1 pad.140
  85.8 1.1 pad.141
  87.0 1.1 pad.123
  88.2 1.1 pad.122
  89.5 2.2 pad.142
  91.7 2.2 pad.143
  93.9 4.5 %pad.145 = f32[512,128]{0,1:T(8,128)S(1)} pad(f32[256,128]{0,1:T(8,128)S(1)} %add.346, f32[]{:T(128)} %constant.25.clone.1), padding=1_0_1x0_0_0 | pad | bytes 393220 | tf_op jit(solution)/shard_map/pad | solution.py:164
  98.6 2.2 pad.124
  100.8 2.2 pad.125
  103.2 4.4 %pad.144 = f32[512,128]{0,1:T(8,128)S(1)} pad(f32[256,128]{0,1:T(8,128)S(1)} %pad_maximum_fusion.1, f32[]{:T(128)} %constant.25.clone.1), padding=0_1_1x0_0_0 | pad | bytes 393220 | tf_op jit(solution)/shard_map/pad | solution.py:164
  107.7 4.8 %pad.127 = f32[512,128]{0,1:T(8,128)S(1)} pad(f32[256,128]{0,1:T(8,128)S(1)} %add.336, f32[]{:T(128)} %constant.25.clone.1), padding=1_0_1x0_0_0 | pad | bytes 393220 | tf_op jit(solution)/shard_map/pad | solution.py:164
  112.6 4.4 %pad.126 = f32[512,128]{0,1:T(8,128)S(1)} pad(f32[256,128]{0,1:T(8,128)S(1)} %pad_maximum_fusion, f32[]{:T(128)} %constant.25.clone.1), padding=0_1_1x0_0_0 | pad | bytes 393220 | tf_op jit(solution)/shard_map/pad | solution.py:164
  117.2 0.6 broadcast_in_dim.64
  117.8 12.6 %all-to-all-start = ((f32[32,2,128]{2,1,0:T(2,128)}), f32[32,2,128]{2,1,0:T(2,128)S(1)}, u32[]{:S(2)}, u32[]{:S(2)}) async-start(f32[32,2,128]{2,1,0:T(2,128)} %broadcast_in_dim.64), calls=%async_computation | async-start | bytes 65536 | tf_op jit(solution)/shard_map/all_to_all | solution.py:18
  130.4 8.7 %all-to-all-done = f32[32,2,128]{2,1,0:T(2,128)S(1)} async-done(((f32[32,2,128]{2,1,0:T(2,128)}), f32[32,2,128]{2,1,0:T(2,128)S(1)}, u32[]{:S(2)}, u32[]{:S(2)}) %all-to-all-start) | async-done | bytes 32800 | tf_op jit(solution)/shard_map/all_to_all | solution.py:18
  139.6 2.2 convolution_convert_fusion
  141.7 9.5 %all-to-all-start.1 = ((bf16[16,32,2048]{2,1,0:T(8,128)(2,1)}), bf16[16,32,2048]{2,1,0:T(8,128)(2,1)S(1)}, u32[]{:S(2)}, u32[]{:S(2)}) async-start(bf16[16,32,2048]{2,1,0:T(8,128)(2,1)} %bitcast.12), calls=%async_computation.1 | async-start | bytes 4194304 | tf_op jit(solution)/shard_map/all_to_all | solution.py:67
  151.3 0.8 broadcast_multiply_fusion
  153.0 47.3 %all-to-all-done.1 = bf16[16,32,2048]{2,1,0:T(8,128)(2,1)S(1)} async-done(((bf16[16,32,2048]{2,1,0:T(8,128)(2,1)}), bf16[16,32,2048]{2,1,0:T(8,128)(2,1)S(1)}, u32[]{:S(2)}, u32[]{:S(2)}) %all-to-all-start.1) | async-done | bytes 2097184 | tf_op jit(solution)/shard_map/all_to_all | solution.py:67
  200.9 0.8 gather_fusion
  202.3 19.6 %all_to_all.35 = bf16[32,3,2048]{2,1,0:T(4,128)(2,1)S(1)} all-to-all(bf16[32,3,2048]{2,1,0:T(4,128)(2,1)S(1)} %broadcast_select_fusion), channel_id=1, replica_groups=mesh['sp'=32,'tp'=16] {'sp'}, dimensions={0} | all-to-all | bytes 786432 | tf_op jit(solution)/shard_map/all_to_all | solution.py:195
  221.9 1.1 all_gather_reshape.3
  223.2 43.8 %all-gather.3.cloned.1.call-done = bf16[16,1,96,2048]{3,2,1,0:T(8,128)(2,1)} async-done(((bf16[1,1,96,2048]{3,2,1,0:T(8,128)(2,1)}), bf16[16,1,96,2048]{3,2,1,0:T(8,128)(2,1)}) %all-gather.3.cloned.1.call-update) | async-done | bytes 6291472 | tf_op jit(solution)/shard_map/all_gather | solution.py:81
  267.0 4.7 %fusion.2 = f32[16,96,128]{2,1,0:T(8,128)S(1)} fusion(bf16[16,1,96,2048]{3,2,1,0:T(8,128)(2,1)} %all-gather.3.cloned.1.call-done, bf16[1,2048,128]{2,1,0:T(8,128)(2,1)S(1)} %copy-done.5), kind=kOutput, calls=%fused_computation.4 | convolution fusion | flops 805306368 | bytes 7602176 | tf_op jit(solution)/shard_map/vmap()/dot_general | solution.py:105
  271.8 2.6 fusion.7
  274.4 58.5 %all-gather.5.cloned.1.call-done = bf16[1536,2048]{1,0:T(8,128)(2,1)} async-done(((bf16[1536,128]{1,0:T(8,128)(2,1)}), bf16[1536,2048]{1,0:T(8,128)(2,1)}) %all-gather.5.cloned.1.call-update) | async-done | bytes 6291472 | tf_op jit(solution)/shard_map/all_gather | solution.py:113
  332.9 4.6 %convolution_convert_fusion.1 = bf16[1536,128]{1,0:T(8,128)(2,1)S(1)} fusion(bf16[1536,2048]{1,0:T(8,128)(2,1)} %all-gather.5.cloned.1.call-done, bf16[1,2048,128]{2,1,0:T(8,128)(2,1)S(1)} %copy-done.7), kind=kOutput, calls=%fused_computation.8 | convolution fusion | flops 805502976 | bytes 7208960 | tf_op jit(solution)/shard_map/dot_general | solution.py:112
  337.5 19.4 %all_to_all.36 = bf16[16,96,128]{2,1,0:T(8,128)(2,1)S(1)} all-to-all(bf16[16,96,128]{2,1,0:T(8,128)(2,1)S(1)} %bitcast.97), channel_id=1, replica_groups=mesh['sp'=32,'tp'=16] {'tp'}, dimensions={0} | all-to-all | bytes 786432 | tf_op jit(solution)/shard_map/all_to_all | solution.py:207
  357.1 0.9 reshape.148
  358.0 9.9 %all-to-all-start.4 = ((bf16[32,3,2048]{2,1,0:T(4,128)(2,1)}), bf16[32,3,2048]{2,1,0:T(4,128)(2,1)S(1)}, u32[]{:S(2)}, u32[]{:S(2)}) async-start(bf16[32,3,2048]{2,1,0:T(4,128)(2,1)} %reshape.148), calls=%async_computation.4 | async-start | bytes 1048576 | tf_op jit(solution)/shard_map/all_to_all | solution.py:214
  368.2 17.4 %all-to-all-done.4 = bf16[32,3,2048]{2,1,0:T(4,128)(2,1)S(1)} async-done(((bf16[32,3,2048]{2,1,0:T(4,128)(2,1)}), bf16[32,3,2048]{2,1,0:T(4,128)(2,1)S(1)}, u32[]{:S(2)}, u32[]{:S(2)}) %all-to-all-start.4) | async-done | bytes 393248 | tf_op jit(solution)/shard_map/all_to_all | solution.py:214
  385.9 0.7 gather_fusion.1
  387.0 0.7 multiply_reduce_fusion
  387.7 0.7 fusion.22
  (191 shorter events, 20.7 us)
Async XLA Ops:
  6.5 133.0 %copy-start = (bf16[128,2048]{1,0:T(8,128)(2,1)S(1)}, bf16[128,2048]{1,0:T(8,128)(2,1)}, u32[]{:S(2)}) copy-start(bf16[128,2048]{1,0:T(8,128)(2,1)} %param.23) | copy-start | bytes 1572868
  7.4 8.6 %collective-permute-start = (bf16[3,128]{0,1:T(8,128)(2,1)S(1)}, bf16[3,128]{0,1:T(8,128)(2,1)S(1)}, u32[]{:S(2)}, u32[]{:S(2)}) collective-permute-start(bf16[3,128]{0,1:T(8,128)(2,1)S(1)} %copy.84), channel_id=1, source_target_pairs={{0,16},{16,32},{32,48},{48,64},{64,80},{80,96},{96,112},{112,128},... | collective-permute-start | bytes 2312 | tf_op jit(solution)/shard_map/ppermute | solution.py:13
  107.6 93.0 %copy-start.1 = (bf16[32,2048]{1,0:T(8,128)(2,1)S(1)}, bf16[32,2048]{1,0:T(8,128)(2,1)}, u32[]{:S(2)}) copy-start(bf16[32,2048]{1,0:T(8,128)(2,1)} %param.15) | copy-start | bytes 393220
  112.5 88.3 %copy-start.2 = (f32[2048]{0:T(1024)S(1)}, f32[2048]{0:T(1024)}, u32[]{:S(2)}) copy-start(f32[2048]{0:T(1024)} %param.24) | copy-start | bytes 24580
  117.8 21.3 %all-to-all-start = ((f32[32,2,128]{2,1,0:T(2,128)}), f32[32,2,128]{2,1,0:T(2,128)S(1)}, u32[]{:S(2)}, u32[]{:S(2)}) async-start(f32[32,2,128]{2,1,0:T(2,128)} %broadcast_in_dim.64), calls=%async_computation | async-start | bytes 65536 | tf_op jit(solution)/shard_map/all_to_all | solution.py:18
  141.7 58.5 %all-to-all-start.1 = ((bf16[16,32,2048]{2,1,0:T(8,128)(2,1)}), bf16[16,32,2048]{2,1,0:T(8,128)(2,1)S(1)}, u32[]{:S(2)}, u32[]{:S(2)}) async-start(bf16[16,32,2048]{2,1,0:T(8,128)(2,1)} %bitcast.12), calls=%async_computation.1 | async-start | bytes 4194304 | tf_op jit(solution)/shard_map/all_to_all | solution.py:67
  151.2 115.8 %copy-start.5 = (bf16[1,2048,128]{2,1,0:T(8,128)(2,1)S(1)}, bf16[1,2048,128]{2,1,0:T(8,128)(2,1)}, u32[]{:S(2)}) copy-start(bf16[1,2048,128]{2,1,0:T(8,128)(2,1)} %param.27) | copy-start | bytes 1572868
  151.2 115.8 %all-gather.3.cloned.1.call-start = ((), (), s32[]{:S(2)}) async-start(), calls=%async_computation.5 | async-start | bytes 6684672 | tf_op jit(solution)/shard_map/all_gather | solution.py:81
  223.0 48.8 %copy-start.6 = (bf16[1,2048,128]{2,1,0:T(8,128)(2,1)S(1)}, bf16[1,2048,128]{2,1,0:T(8,128)(2,1)}, u32[]{:S(2)}) copy-start(bf16[1,2048,128]{2,1,0:T(8,128)(2,1)} %param.28) | copy-start | bytes 1572868
  223.0 109.9 %all-gather.5.cloned.1.call-start = ((), (), s32[]{:S(2)}) async-start(), calls=%async_computation.6 | async-start | bytes 6684672 | tf_op jit(solution)/shard_map/all_gather | solution.py:113
  267.0 4.8 %copy-start.4 = (bf16[16,1,96,2048]{3,2,1,0:T(8,128)(2,1)S(1)}, bf16[16,1,96,2048]{3,2,1,0:T(8,128)(2,1)}, u32[]{:S(2)}) copy-start(bf16[16,1,96,2048]{3,2,1,0:T(8,128)(2,1)} %all-gather.3.cloned.1.call-done) | copy-start | bytes 18874372
  271.8 61.1 %copy-start.7 = (bf16[1,2048,128]{2,1,0:T(8,128)(2,1)S(1)}, bf16[1,2048,128]{2,1,0:T(8,128)(2,1)}, u32[]{:S(2)}) copy-start(bf16[1,2048,128]{2,1,0:T(8,128)(2,1)} %param.29) | copy-start | bytes 1572868
  274.4 93.7 %copy-start.3 = (f32[32,2]{0,1:T(2,128)S(1)}, f32[32,2]{0,1:T(2,128)}, u32[]{:S(2)}) copy-start(f32[32,2]{0,1:T(2,128)} %param.26) | copy-start | bytes 772
  358.0 27.6 %all-to-all-start.4 = ((bf16[32,3,2048]{2,1,0:T(4,128)(2,1)}), bf16[32,3,2048]{2,1,0:T(4,128)(2,1)S(1)}, u32[]{:S(2)}, u32[]{:S(2)}) async-start(bf16[32,3,2048]{2,1,0:T(4,128)(2,1)} %reshape.148), calls=%async_computation.4 | async-start | bytes 1048576 | tf_op jit(solution)/shard_map/all_to_all | solution.py:214
Sparse Core Ops, SparseCore 0:
  223.1 43.8 all-gather.2
  274.5 58.3 all-gather.4
where the time goes:
time: 403 us; the launch traced here: 395 us
  waiting for transfers between devices  176 us (44%)
  local copies, waits for them, and re-layouts  105 us (26%)
  blocking collectives  39 us (10%)
  starting transfers between devices  36.1 us (9%)
  matrix products  16.1 us (4%)
  between operations  14.8 us (4%)
  other arithmetic  8.3 us (2%)
    all_gather x1, waiting for transfers between devices, expert_down(): lax.all_gather(active, 'tp', axis=1, tiled=True)  58.5 us
    slice x50, local copies, waits for them, and re-layouts, body(): lax.associative_scan(chain_step, (decay, drive), axis=0)  55.8 us
    all_to_all x1, waiting for transfers between devices, sum_at_owner(): lax.all_to_all(pieces, axis, split_axis=0, concat_axis=0, tiled=True)  47.3 us
    all_gather x1, waiting for transfers between devices, piecewise(): blocks = [lax.all_gather(slab, axis) for slab in pieces]  43.8 us
    pad x32, local copies, waits for them, and re-layouts, body(): lax.associative_scan(chain_step, (decay, drive), axis=0)  36.6 us
    all_to_all x1, blocking collectives, body(): lax.all_to_all(outgoing, 'sp', split_axis=0, concat_axis=0, tiled=True)  19.6 us
    all_to_all x1, blocking collectives, body(): lax.all_to_all(result.reshape(tp_size, experts * capacity, -1), 'tp', spl...  19.4 us
    all_to_all x1, waiting for transfers between devices, body(): lax.all_to_all(joined.reshape(experts, capacity, model_width), 'sp', spli...  17.4 us
  transfers between devices with their start and end apart: 6, of which 5 were waited for; matrix products, arithmetic and copies ran while one was open for 2% of the time, Pallas kernels for 0%

commit v1 on v0

v1 whole, which is shorter than its diff:
```python
import jax
import jax.numpy as jnp
from jax import lax
from jax.experimental import pallas as pl
from jax.experimental.pallas import tpu as pltpu
from jax.sharding import PartitionSpec as P


RECURRENT_SCALE = 8.0
EPSILON = 1e-06
SEGMENTS = 8
CORES = 2
CAP = 3
GELU_SCALE = 0.7978845608028654

VMEM = pl.BlockSpec(memory_space=pltpu.VMEM)
SMEM = pl.BlockSpec(memory_space=pltpu.SMEM)


def shifted(block, axis, distance):
    devices = range(lax.axis_size(axis))
    route = [(i - distance, i) for i in devices if i - distance in devices]
    return lax.ppermute(block, axis, route)


def from_everyone(x, axis):
    size = lax.axis_size(axis)
    return lax.all_to_all(jnp.broadcast_to(x[None], (size, *x.shape)), axis, 0, 0, tiled=True)


def core_groups(size):
    return [[core + CORES * y for y in range(size // CORES)] for core in range(CORES)]


def swap_cores(x):
    size = lax.axis_size("tp")
    return lax.ppermute(x, "tp", [(i, i ^ 1) for i in range(size)])


def minus_expm1(x):
    series = 1.0 + x * (1.0 / 7.0)
    for k in (6, 5, 4, 3, 2):
        series = 1.0 + x * (1.0 / k) * series
    return jnp.where(x > -0.35, -x * series, 1.0 - jnp.exp(x))


def recurrence_kernel(
    x_ref, rim_ref, filter_ref, gates_ref, rate_ref, boost_ref,
    state_ref, running_ref, total_ref, ext, decay, drive,
):
    tokens, channels = x_ref.shape
    taps = filter_ref.shape[0]
    lead = 8
    ext[lead - taps + 1 : lead, :] = rim_ref[...].astype(jnp.float32)
    ext[lead : lead + tokens, :] = x_ref[...].astype(jnp.float32)
    first = lead - taps + 1
    mixed = ext[first : first + tokens, :] * filter_ref[0:1, :]
    for k in range(1, taps):
        mixed = mixed + ext[first + k : first + k + tokens, :] * filter_ref[k : k + 1, :]
    smoothed = mixed.astype(jnp.bfloat16)
    logits = jnp.dot(smoothed, gates_ref[...], preferred_element_type=jnp.float32)
    both = jax.nn.sigmoid(logits)
    log_decay = both[:, :channels] * rate_ref[...] + boost_ref[...]
    decay[...] = jnp.exp(log_decay)
    drive[...] = jnp.sqrt(minus_expm1(2.0 * log_decay)) * (
        both[:, channels:] * smoothed.astype(jnp.float32)
    )
    length = tokens // SEGMENTS

    def step(i, held):
        state, running = held
        rows = pl.ds(i, SEGMENTS, stride=length)
        a, b = decay[rows, :], drive[rows, :]
        state, running = a * state + b, running * a
        state_ref[rows, :] = state
        running_ref[rows, :] = running
        return state, running

    start = (jnp.zeros((SEGMENTS, channels), jnp.float32), jnp.ones((SEGMENTS, channels), jnp.float32))
    state, running = lax.fori_loop(0, length, step, start, unroll=8)
    whole_a, whole_b = running[0:1], state[0:1]
    for k in range(1, SEGMENTS):
        whole_b = running[k : k + 1] * whole_b + state[k : k + 1]
        whole_a = whole_a * running[k : k + 1]
    total_ref[0:1, :] = whole_a
    total_ref[1:2, :] = whole_b


def branch_kernel(place_ref, pieces_ref, state_ref, running_ref, gate_ref, keep_ref, send_ref):
    place, core = place_ref[0], place_ref[1]
    devices, _, channels = pieces_ref.shape
    carry = jnp.zeros((1, channels), jnp.float32)
    for k in range(devices):
        piece = pieces_ref[k]
        carry = jnp.where(k < place, piece[0:1] * carry + piece[1:2], carry)
    length = state_ref.shape[0] // SEGMENTS
    half = length // CORES
    for k in range(SEGMENTS):
        for out, side in ((keep_ref, core), (send_ref, 1 - core)):
            rows = pl.ds(pl.multiple_of(k * length + side * half, half), half)
            state = state_ref[rows, :] + running_ref[rows, :] * carry
            g = gate_ref[rows, :].astype(jnp.float32)
            gelu = 0.5 * g * (1.0 + jnp.tanh(GELU_SCALE * (g + 0.044715 * (g * g * g))))
            out[k * half : (k + 1) * half, :] = (gelu * state).astype(jnp.bfloat16)
        last = (k + 1) * length - 1
        carry = running_ref[last : last + 1, :] * carry + state_ref[last : last + 1, :]


def slots_kernel(routes_ref, slots_ref):
    rows = routes_ref.shape[0]
    experts = 32
    number = lax.broadcasted_iota(jnp.int32, (rows, experts), 1)
    hot = [(routes_ref[:, k : k + 1] == number).astype(jnp.float32) for k in range(2)]
    earlier = (
        lax.broadcasted_iota(jnp.int32, (rows, rows), 1)
        < lax.broadcasted_iota(jnp.int32, (rows, rows), 0)
    ).astype(jnp.float32)
    before = jnp.dot(earlier, hot[0] + hot[1], preferred_element_type=jnp.float32)
    for k in range(2):
        rank = jnp.sum(before * hot[k], axis=1, keepdims=True).astype(jnp.int32)
        slots_ref[:, k : k + 1] = routes_ref[:, k : k + 1] * CAP + rank


def dispatch_kernel(parts_ref, resid_ref, gain_ref, slots_ref, stream_ref, out_ref):
    rows, width = resid_ref.shape
    projected = parts_ref[0].astype(jnp.float32)
    for k in range(1, parts_ref.shape[0]):
        projected = projected + parts_ref[k].astype(jnp.float32)
    stream = (resid_ref[...].astype(jnp.float32) + projected).astype(jnp.bfloat16)
    stream_ref[...] = stream
    wide = stream.astype(jnp.float32)
    mean = jnp.sum(wide * wide, axis=1, keepdims=True) * (1.0 / width)
    normed = (wide * lax.rsqrt(mean + EPSILON) * gain_ref[...]).astype(jnp.bfloat16)
    slot = lax.broadcasted_iota(jnp.int32, (rows, out_ref.shape[0]), 1)
    pick = (slots_ref[:, 0:1] == slot) | (slots_ref[:, 1:2] == slot)
    pick = pick.astype(jnp.float32).T.astype(jnp.bfloat16)
    out_ref[...] = jnp.dot(pick, normed, preferred_element_type=jnp.float32).astype(jnp.bfloat16)


def combine_kernel(stream_ref, returned_ref, slots_ref, weight_ref, out_ref):
    rows = stream_ref.shape[0]
    slot = lax.broadcasted_iota(jnp.int32, (rows, returned_ref.shape[0]), 1)
    total = jnp.zeros(stream_ref.shape, jnp.float32)
    for k in range(2):
        pick = (slots_ref[:, k : k + 1] == slot).astype(jnp.float32).astype(jnp.bfloat16)
        chosen = jnp.dot(pick, returned_ref[...], preferred_element_type=jnp.float32)
        total = total + weight_ref[:, k : k + 1] * chosen
    out_ref[...] = (stream_ref[...].astype(jnp.float32) + total).astype(jnp.bfloat16)


def block_diagonal(blocks):
    count, width, _ = blocks.shape
    rows = [
        jnp.pad(blocks[k], ((0, 0), (k * width, (count - 1 - k) * width))) for k in range(count)
    ]
    return jnp.concatenate(rows, axis=0)


def layer(
    resid,
    recurrent_input,
    recurrent_out_gate,
    filter_weight,
    recurrence_gate_matrix,
    input_gate_matrix,
    channel_decay_raw,
    token_decay_boost,
    output_projection_weight,
    expert_norm_gain,
    routes,
    expert_pair_weight,
    gate_weight,
    up_weight,
    down_weight,
):
    tokens, channels = recurrent_input.shape
    taps = filter_weight.shape[0]
    tp, experts = lax.axis_size("tp"), lax.axis_size("sp")
    here, place = lax.axis_index("tp"), lax.axis_index("sp")
    core = here % CORES
    chips = tp // CORES
    groups = core_groups(tp)
    rows_dev, width = resid.shape
    f32, bf16 = jnp.float32, jnp.bfloat16

    rim = shifted(recurrent_input[tokens - taps + 1 :], "sp", 1)
    gates = jnp.concatenate(
        [block_diagonal(recurrence_gate_matrix), block_diagonal(input_gate_matrix)], axis=1
    )
    rate = (-RECURRENT_SCALE * jax.nn.softplus(-channel_decay_raw))[None, :]

    down_all = lax.all_gather(down_weight[0], "tp")
    projection_other = swap_cores(output_projection_weight)
    gate_other = swap_cores(gate_weight[0])
    up_other = swap_cores(up_weight[0])

    own_routes = lax.dynamic_slice_in_dim(routes, here * rows_dev, rows_dev, 0)
    slots = pl.pallas_call(
        slots_kernel,
        out_shape=jax.ShapeDtypeStruct((rows_dev, 2), jnp.int32),
        in_specs=[VMEM],
        out_specs=VMEM,
        name="slots",
    )(own_routes)

    state, running, total = pl.pallas_call(
        recurrence_kernel,
        out_shape=(
            jax.ShapeDtypeStruct((tokens, channels), f32),
            jax.ShapeDtypeStruct((tokens, channels), f32),
            jax.ShapeDtypeStruct((2, channels), f32),
        ),
        in_specs=[VMEM] * 6,
        out_specs=(VMEM,) * 3,
        scratch_shapes=[
            pltpu.VMEM((tokens + 8, channels), f32),
            pltpu.VMEM((tokens, channels), f32),
            pltpu.VMEM((tokens, channels), f32),
        ],
        cost_estimate=pl.CostEstimate(flops=10**9, bytes_accessed=2**20, transcendentals=0),
        name="recurrence",
    )(recurrent_input, rim, filter_weight, gates, rate, token_decay_boost)

    pieces = from_everyone(total, "sp")
    keep, send = pl.pallas_call(
        branch_kernel,
        out_shape=(jax.ShapeDtypeStruct((tokens // CORES, channels), bf16),) * 2,
        in_specs=[SMEM] + [VMEM] * 4,
        out_specs=(VMEM,) * 2,
        name="branch",
    )(jnp.stack([place, core]).astype(jnp.int32), pieces, state, running, recurrent_out_gate)
    got = swap_cores(send)

    both = jnp.concatenate([keep, got], axis=1)
    projection = jnp.concatenate([output_projection_weight, projection_other], axis=0)
    partial = jnp.dot(both, projection, preferred_element_type=f32).astype(bf16)
    parts = lax.all_to_all(
        partial.reshape(chips, rows_dev, width), "tp", 0, 0, axis_index_groups=groups, tiled=True
    )
    slot_count = experts * CAP
    parts, down_all = lax.optimization_barrier((parts, down_all))
    stream, outgoing = pl.pallas_call(
        dispatch_kernel,
        out_shape=(
            jax.ShapeDtypeStruct((rows_dev, width), bf16),
            jax.ShapeDtypeStruct((slot_count, width), bf16),
        ),
        in_specs=[VMEM] * 4,
        out_specs=(VMEM,) * 2,
        name="dispatch",
    )(parts, resid, expert_norm_gain[None, :], slots)
    arrived = lax.all_to_all(
        outgoing.reshape(experts, CAP, width), "sp", split_axis=0, concat_axis=0, tiled=True
    ).reshape(slot_count, width)

    rows = lax.all_gather(arrived, "tp", axis=0, axis_index_groups=groups, tiled=True)
    gate_both = jnp.concatenate([gate_weight[0], gate_other], axis=1)
    up_both = jnp.concatenate([up_weight[0], up_other], axis=1)
    gate = jnp.dot(rows, gate_both, preferred_element_type=f32)
    upward = jnp.dot(rows, up_both, preferred_element_type=f32)
    active = (jax.nn.silu(gate) * upward).astype(bf16)

    hidden = gate_weight.shape[2]
    down_own = lax.dynamic_slice_in_dim(down_all, here * hidden, hidden, 1)
    down_other = lax.dynamic_slice_in_dim(down_all, (here + 1 - 2 * core) * hidden, hidden, 1)
    down = jnp.concatenate([down_own, down_other], axis=1)
    down = jnp.moveaxis(down, 0, 1).reshape(CORES * hidden, width)
    summed = jnp.dot(active, down, preferred_element_type=f32).astype(bf16)
    result = lax.psum_scatter(
        summed, "tp", scatter_dimension=0, axis_index_groups=groups, tiled=True
    )

    returned = lax.all_to_all(
        result.reshape(experts, CAP, width), "sp", split_axis=0, concat_axis=0, tiled=True
    ).reshape(slot_count, width)
    return pl.pallas_call(
        combine_kernel,
        out_shape=jax.ShapeDtypeStruct((rows_dev, width), bf16),
        in_specs=[VMEM] * 4,
        out_specs=VMEM,
        name="combine",
    )(stream, returned, slots, expert_pair_weight)


def solution(mesh):
    placed = (
        P(("sp", "tp"), None),
        P("sp", "tp"),
        P("sp", "tp"),
        P(None, "tp"),
        P("tp", None, None),
        P("tp", None, None),
        P("tp"),
        P("sp", "tp"),
        P("tp", None),
        P(),
        P("sp", None),
        P(("sp", "tp"), None),
        P("sp", None, "tp"),
        P("sp", None, "tp"),
        P("sp", None, "tp"),
    )
    return jax.shard_map(
        layer, mesh=mesh, in_specs=placed, out_specs=P(("sp", "tp"), None), check_vma=False
    )
```

time: 403 us -> 266 us (0.66)
  the two profiles are of different devices: /device:TPU:1 before, /device:TPU:24 now
where the time goes in v1:
time: 266 us; the launch traced here: 265 us
  waiting for transfers between devices  127 us (48%)
  starting transfers between devices  42.6 us (16%)
  blocking collectives  29.6 us (11%)
  local copies, waits for them, and re-layouts  25.8 us (10%)
  between operations  13.2 us (5%)
  matrix products  13.1 us (5%)
  Pallas kernels  11.2 us (4%)
  other arithmetic  2.7 us (1%)
    reduce_scatter x1, waiting for transfers between devices, layer(): lax.psum_scatter(summed, 'tp', scatter_dimension=0, axis_index_groups=gro...  48.5 us
    all_to_all x1, blocking collectives, layer(): lax.all_to_all(outgoing.reshape(experts, CAP, width), 'sp', split_axis=0,...  29.6 us
    all_to_all x1, waiting for transfers between devices, layer(): lax.all_to_all(partial.reshape(chips, rows_dev, width), 'tp', 0, 0, axis_...  29.5 us
    all_gather x1, waiting for transfers between devices, layer(): lax.all_gather(arrived, 'tp', axis=0, axis_index_groups=groups, tiled=True)  22.7 us
    all_to_all x1, waiting for transfers between devices, layer(): lax.all_to_all(result.reshape(experts, CAP, width), 'sp', split_axis=0, c...  14.4 us
    all_to_all x1, starting transfers between devices, from_everyone(): lax.all_to_all(jnp.broadcast_to(x[None], (size, *x.shape)), axis, 0, 0, t...  13.3 us
    optimization_barrier x1, local copies, waits for them, and re-layouts, layer(): parts, down_all = lax.optimization_barrier((parts, down_all))  12.3 us
    all_to_all x1, starting transfers between devices, layer(): lax.all_to_all(result.reshape(experts, CAP, width), 'sp', split_axis=0, c...  10.3 us
  transfers between devices with their start and end apart: 11, of which 6 were waited for; matrix products, arithmetic and copies ran while one was open for 10% of the time, Pallas kernels for 3%

profile of v1, /device:TPU:24, one launch (start us, length us, event | category | flops | bytes accessed | tf_op | source)
XLA Modules:
  0.0 264.9 jit_solution(6084490443081606334)
XLA Ops:
  6.5 0.0 copy-start
  6.5 0.0 copy-start.4
  6.5 0.0 all-gather.3.cloned.1.call-start
  6.5 0.7 all-gather.3.cloned.1.call-update
  7.3 1.9 collective-permute-start.2
  9.2 0.7 slice.15
  9.9 3.4 %collective-permute-start = (bf16[3,128]{1,0:T(4,128)(2,1)S(1)}, bf16[3,128]{1,0:T(4,128)(2,1)S(1)}, u32[]{:S(2)}, u32[]{:S(2)}) collective-permute-start(bf16[3,128]{1,0:T(4,128)(2,1)S(1)} %slice.15), channel_id=1, source_target_pairs={{0,16},{16,32},{32,48},{48,64},{64,80},{80,96},{96,112},{112,128},... | collective-permute-start | bytes 2312 | tf_op jit(solution)/shard_map/ppermute | solution.py:23
  13.3 0.8 slice_bitcast_fusion.1
  14.1 0.7 fusion.32.gates_ref
  14.8 1.3 fusion.35.rate_ref
  16.0 0.0 collective-permute-done.rim_ref
  16.0 0.0 copy-start.7
  16.0 0.6 copy-done.7
  16.6 3.2 %recurrence.1 = (f32[512,128]{1,0:T(8,128)}, f32[512,128]{1,0:T(8,128)}, f32[2,128]{1,0:T(2,128)}) custom-call(bf16[512,128]{1,0:T(8,128)(2,1)} %x_ref.1, bf16[3,128]{1,0:T(4,128)(2,1)} %copy-done.7, f32[4,128]{1,0:T(4,128)} %filter_ref.1, bf16[128,256]{1,0:T(8,128)(2,1)} %fusion.32.gates_ref, f32[1,128]{1,0:T(1,128)} %fusion.35.rate_ref, f32[512,128]{1,0:T(8,128)} %boost_ref.1), custom_call_target="tpu_custom_call" | custom-call | flops 1000000000 | bytes 1048576 | tf_op jit(solution)/shard_map/recurrence/pallas_call | solution.py:206
  19.8 1.3 broadcast_in_dim.13
  21.1 13.3 %all-to-all-start = ((f32[32,2,128]{2,1,0:T(2,128)}), f32[32,2,128]{2,1,0:T(2,128)S(1)}, u32[]{:S(2)}, u32[]{:S(2)}) async-start(f32[32,2,128]{2,1,0:T(2,128)} %broadcast_in_dim.13), calls=%async_computation | async-start | bytes 65536 | tf_op jit(solution)/shard_map/all_to_all | solution.py:28
  34.4 0.6 pad_add_fusion.place_ref
  35.0 9.3 %all-to-all-done.pieces_ref = f32[32,2,128]{2,1,0:T(2,128)S(1)} async-done(((f32[32,2,128]{2,1,0:T(2,128)}), f32[32,2,128]{2,1,0:T(2,128)S(1)}, u32[]{:S(2)}, u32[]{:S(2)}) %all-to-all-start) | async-done | bytes 32800 | tf_op jit(solution)/shard_map/all_to_all | solution.py:28
  44.2 0.0 copy-start.2
  44.2 0.6 copy-done.2
  44.9 1.9 branch.1
  46.8 1.9 collective-permute-start.1
  48.7 1.5 collective-permute-done.1
  50.2 0.0 collective-permute-done.2
  50.2 0.0 copy-done.4
  50.2 2.3 convolution_convert_fusion.1
  52.5 0.0 copy-start.5
  52.5 0.0 copy-start.6
  52.5 7.4 %all-to-all-start.1 = ((bf16[8,32,2048]{2,1,0:T(8,128)(2,1)}), bf16[8,32,2048]{2,1,0:T(8,128)(2,1)S(1)}, u32[]{:S(2)}, u32[]{:S(2)}) async-start(bf16[8,32,2048]{2,1,0:T(8,128)(2,1)} %bitcast.7), calls=%async_computation.1 | async-start | bytes 2097152 | tf_op jit(solution)/shard_map/all_to_all | solution.py:237
  59.9 0.0 all-gather.5.cloned.1.call-start
  59.9 0.0 copy-done
  60.0 0.1 constant_dynamic-slice_fusion.2
  60.0 0.7 copy.25.routes_ref
  60.7 1.6 slots.1.slots_ref
  62.3 29.5 %all-to-all-done.1.parts_ref = bf16[8,32,2048]{2,1,0:T(8,128)(2,1)S(1)} async-done(((bf16[8,32,2048]{2,1,0:T(8,128)(2,1)}), bf16[8,32,2048]{2,1,0:T(8,128)(2,1)S(1)}, u32[]{:S(2)}, u32[]{:S(2)}) %all-to-all-start.1) | async-done | bytes 1048608 | tf_op jit(solution)/shard_map/all_to_all | solution.py:237
  91.8 0.0 copy-start.1
  91.8 1.0 copy-done.1
  92.9 2.6 dispatch.1
  95.4 1.4 reshape.20
  96.9 29.6 %all_to_all.20 = bf16[32,3,2048]{2,1,0:T(4,128)(2,1)S(1)} all-to-all(bf16[32,3,2048]{2,1,0:T(4,128)(2,1)S(1)} %reshape.20), channel_id=1, replica_groups=mesh['sp'=32,'tp'=16] {'sp'}, dimensions={0} | all-to-all | bytes 786432 | tf_op jit(solution)/shard_map/all_to_all | solution.py:252
  126.5 1.1 reshape.21
  127.6 0.0 all-gather.5.cloned.1.call-update
  127.6 0.0 reduce-scatter.2.cloned.1.call-start
  127.6 0.0 copy-done.5
  127.6 1.9 collective-permute-start.3
  129.6 0.0 copy-done.6
  129.6 2.4 collective-permute-start.4
  132.0 12.3 %copy.22 = bf16[16,2048,128]{1,2,0:T(8,128)(2,1)} copy(bf16[16,2048,128]{2,1,0:T(8,128)(2,1)} %all-gather.3.cloned.1.call-done) | data formatting | bytes 16777216 | tf_op jit(solution)/shard_map/optimization_barrier | solution.py:241
  144.3 1.3 constant_dynamic-slice_fusion.1
  145.6 0.1 pad_maximum_fusion
  145.8 0.0 collective-permute-done.3
  145.8 22.7 %all-gather.5.cloned.1.call-done = bf16[768,2048]{1,0:T(8,128)(2,1)} async-done(((bf16[96,2048]{1,0:T(8,128)(2,1)}), bf16[768,2048]{1,0:T(8,128)(2,1)}) %all-gather.5.cloned.1.call-update) | async-done | bytes 3145744 | tf_op jit(solution)/shard_map/all_gather | solution.py:256
  168.5 3.8 %fusion.3 = f32[768,256]{1,0:T(8,128)} fusion(bf16[768,2048]{1,0:T(8,128)(2,1)} %all-gather.5.cloned.1.call-done, bf16[2048,128]{1,0:T(8,128)(2,1)S(1)} %collective-permute-done.3, bf16[2048,128]{1,0:T(8,128)(2,1)S(1)} %bitcast.25), kind=kOutput, calls=%fused_computation.5 | convolution fusion | flops 807403520 | bytes 4980736 | tf_op jit(solution)/shard_map/dot_general | solution.py:259
  172.2 0.0 collective-permute-done.4
  172.2 7.0 %convolution_convert_fusion = bf16[768,2048]{1,0:T(8,128)(2,1)} fusion(bf16[256,2048]{0,1:T(8,128)(2,1)S(1)} %bitcast.22, f32[768,256]{1,0:T(8,128)} %fusion.3, bf16[768,2048]{1,0:T(8,128)(2,1)} %all-gather.5.cloned.1.call-done, bf16[2048,128]{1,0:T(8,128)(2,1)S(1)} %collective-permute-done.4, bf16[2048,128]{1,0:T(8,128)(2,1)S(1)} %bitcast.27), kind=kOutput, calls=%fused_computation | convolution fusion | flops 1615462400 | bytes 9175040 | tf_op jit(solution)/shard_map/dot_general | solution.py:268
  179.3 0.0 reduce-scatter.2.cloned.1.call-update
  179.3 48.5 %reduce-scatter.2.cloned.1.call-done = bf16[96,2048]{1,0:T(8,128)(2,1)} async-done(((bf16[768,2048]{1,0:T(8,128)(2,1)}), bf16[96,2048]{1,0:T(8,128)(2,1)}) %reduce-scatter.2.cloned.1.call-update) | async-done | bytes 393232 | tf_op jit(solution)/shard_map/reduce_scatter | solution.py:269
  227.8 2.1 reshape.23
  229.9 10.3 %all-to-all-start.3 = ((bf16[32,3,2048]{2,1,0:T(4,128)(2,1)}), bf16[32,3,2048]{2,1,0:T(4,128)(2,1)S(1)}, u32[]{:S(2)}, u32[]{:S(2)}) async-start(bf16[32,3,2048]{2,1,0:T(4,128)(2,1)} %reshape.23), calls=%async_computation.4 | async-start | bytes 1048576 | tf_op jit(solution)/shard_map/all_to_all | solution.py:273
  240.2 0.0 copy-done.3
  240.2 0.7 copy.24.weight_ref
  240.9 14.4 %all-to-all-done.3 = bf16[32,3,2048]{2,1,0:T(4,128)(2,1)S(1)} async-done(((bf16[32,3,2048]{2,1,0:T(4,128)(2,1)}), bf16[32,3,2048]{2,1,0:T(4,128)(2,1)S(1)}, u32[]{:S(2)}, u32[]{:S(2)}) %all-to-all-start.3) | async-done | bytes 393248 | tf_op jit(solution)/shard_map/all_to_all | solution.py:273
  255.3 1.1 reshape.24.returned_ref
  256.4 2.0 combine.1
  (2 shorter events, 0.0 us)
Async XLA Ops:
  6.5 53.4 %copy-start = (s32[512,2]{0,1:T(2,128)S(1)}, s32[512,2]{0,1:T(2,128)}, u32[]{:S(2)}) copy-start(s32[512,2]{0,1:T(2,128)} %param.25) | copy-start | bytes 12292
  6.5 43.6 %copy-start.4 = (bf16[128,2048]{1,0:T(8,128)(2,1)S(1)}, bf16[128,2048]{1,0:T(8,128)(2,1)}, u32[]{:S(2)}) copy-start(bf16[128,2048]{1,0:T(8,128)(2,1)} %param.23) | copy-start | bytes 1572868
  6.5 85.3 %all-gather.3.cloned.1.call-start = ((), (), s32[]{:S(2)}) async-start(), calls=%async_computation.5 | async-start | bytes 8912896 | tf_op jit(solution)/shard_map/all_gather | solution.py:192
  7.3 42.9 %collective-permute-start.2 = (bf16[128,2048]{1,0:T(8,128)(2,1)}, bf16[128,2048]{1,0:T(8,128)(2,1)S(1)}, u32[]{:S(2)}, u32[]{:S(2)}) collective-permute-start(bf16[128,2048]{1,0:T(8,128)(2,1)} %param.23), channel_id=1, source_target_pairs={{0,1},{1,0},{2,3},{3,2},{4,5},{5,4},{6,7},{7,6},{8,9},{9,8},{10,11... | collective-permute-start | bytes 1572872 | tf_op jit(solution)/shard_map/ppermute | solution.py:37
  9.9 6.1 %collective-permute-start = (bf16[3,128]{1,0:T(4,128)(2,1)S(1)}, bf16[3,128]{1,0:T(4,128)(2,1)S(1)}, u32[]{:S(2)}, u32[]{:S(2)}) collective-permute-start(bf16[3,128]{1,0:T(4,128)(2,1)S(1)} %slice.15), channel_id=1, source_target_pairs={{0,16},{16,32},{32,48},{48,64},{64,80},{80,96},{96,112},{112,128},... | collective-permute-start | bytes 2312 | tf_op jit(solution)/shard_map/ppermute | solution.py:23
  16.0 0.6 copy-start.7
  21.1 23.2 %all-to-all-start = ((f32[32,2,128]{2,1,0:T(2,128)}), f32[32,2,128]{2,1,0:T(2,128)S(1)}, u32[]{:S(2)}, u32[]{:S(2)}) async-start(f32[32,2,128]{2,1,0:T(2,128)} %broadcast_in_dim.13), calls=%async_computation | async-start | bytes 65536 | tf_op jit(solution)/shard_map/all_to_all | solution.py:28
  44.2 0.6 copy-start.2
  46.8 3.4 %collective-permute-start.1 = (bf16[256,128]{1,0:T(8,128)(2,1)}, bf16[256,128]{1,0:T(8,128)(2,1)S(1)}, u32[]{:S(2)}, u32[]{:S(2)}) collective-permute-start(bf16[256,128]{1,0:T(8,128)(2,1)} %get-tuple-element.18), channel_id=1, source_target_pairs={{0,1},{1,0},{2,3},{3,2},{4,5},{5,4},{6,7},{7,6},{8,9},{9,8},{10,11... | collective-permute-start | bytes 196616 | tf_op jit(solution)/shard_map/ppermute | solution.py:37
  52.5 75.1 %copy-start.5 = (bf16[1,2048,128]{2,1,0:T(8,128)(2,1)S(1)}, bf16[1,2048,128]{2,1,0:T(8,128)(2,1)}, u32[]{:S(2)}) copy-start(bf16[1,2048,128]{2,1,0:T(8,128)(2,1)} %param.27) | copy-start | bytes 1572868
  52.5 77.1 %copy-start.6 = (bf16[1,2048,128]{2,1,0:T(8,128)(2,1)S(1)}, bf16[1,2048,128]{2,1,0:T(8,128)(2,1)}, u32[]{:S(2)}) copy-start(bf16[1,2048,128]{2,1,0:T(8,128)(2,1)} %param.28) | copy-start | bytes 1572868
  52.5 39.3 %all-to-all-start.1 = ((bf16[8,32,2048]{2,1,0:T(8,128)(2,1)}), bf16[8,32,2048]{2,1,0:T(8,128)(2,1)S(1)}, u32[]{:S(2)}, u32[]{:S(2)}) async-start(bf16[8,32,2048]{2,1,0:T(8,128)(2,1)} %bitcast.7), calls=%async_computation.1 | async-start | bytes 2097152 | tf_op jit(solution)/shard_map/all_to_all | solution.py:237
  59.9 108.5 %all-gather.5.cloned.1.call-start = ((), (), s32[]{:S(2)}) async-start(), calls=%async_computation.6 | async-start | bytes 3538944 | tf_op jit(solution)/shard_map/all_gather | solution.py:256
  91.8 1.0 copy-start.1
  127.6 100.2 %reduce-scatter.2.cloned.1.call-start = ((), (), s32[]{:S(2)}) async-start(), calls=%async_computation.7 | async-start | bytes 3538944 | tf_op jit(solution)/shard_map/reduce_scatter | solution.py:269
  127.6 18.1 %collective-permute-start.3 = (bf16[2048,128]{1,0:T(8,128)(2,1)S(1)}, bf16[2048,128]{1,0:T(8,128)(2,1)S(1)}, u32[]{:S(2)}, u32[]{:S(2)}) collective-permute-start(bf16[2048,128]{1,0:T(8,128)(2,1)S(1)} %bitcast.24), channel_id=1, source_target_pairs={{0,1},{1,0},{2,3},{3,2},{4,5},{5,4},{6,7},{7,6},{8,9},{9,8},{10,11... | collective-permute-start | bytes 1572872 | tf_op jit(solution)/shard_map/ppermute | solution.py:37
  129.6 42.6 %collective-permute-start.4 = (bf16[2048,128]{1,0:T(8,128)(2,1)S(1)}, bf16[2048,128]{1,0:T(8,128)(2,1)S(1)}, u32[]{:S(2)}, u32[]{:S(2)}) collective-permute-start(bf16[2048,128]{1,0:T(8,128)(2,1)S(1)} %bitcast.26), channel_id=1, source_target_pairs={{0,1},{1,0},{2,3},{3,2},{4,5},{5,4},{6,7},{7,6},{8,9},{9,8},{10,11... | collective-permute-start | bytes 1572872 | tf_op jit(solution)/shard_map/ppermute | solution.py:37
  179.3 60.9 %copy-start.3 = (f32[32,2]{0,1:T(2,128)S(1)}, f32[32,2]{0,1:T(2,128)}, u32[]{:S(2)}) copy-start(f32[32,2]{0,1:T(2,128)} %param.26) | copy-start | bytes 772
  229.9 25.4 %all-to-all-start.3 = ((bf16[32,3,2048]{2,1,0:T(4,128)(2,1)}), bf16[32,3,2048]{2,1,0:T(4,128)(2,1)S(1)}, u32[]{:S(2)}, u32[]{:S(2)}) async-start(bf16[32,3,2048]{2,1,0:T(4,128)(2,1)} %reshape.23), calls=%async_computation.4 | async-start | bytes 1048576 | tf_op jit(solution)/shard_map/all_to_all | solution.py:273
Sparse Core Ops, SparseCore 0:
  9.5 75.8 all-gather.2
  127.7 40.7 all-gather.4
  179.4 48.3 reduce-scatter.1

commit v2 on v1

v2 whole, which is shorter than its diff:
```python
import jax
import jax.numpy as jnp
from jax import lax
from jax.experimental import pallas as pl
from jax.experimental.pallas import tpu as pltpu
from jax.sharding import PartitionSpec as P


RECURRENT_SCALE = 8.0
EPSILON = 1e-06
SEGMENTS = 8
CORES = 2
CAP = 3
PIECES = 8
GELU_SCALE = 0.7978845608028654

VMEM = pl.BlockSpec(memory_space=pltpu.VMEM)
SMEM = pl.BlockSpec(memory_space=pltpu.SMEM)


def shifted(block, axis, distance):
    devices = range(lax.axis_size(axis))
    route = [(i - distance, i) for i in devices if i - distance in devices]
    return lax.ppermute(block, axis, route)


def core_groups(size):
    return [[core + CORES * y for y in range(size // CORES)] for core in range(CORES)]


def swap_cores(x):
    size = lax.axis_size("tp")
    return lax.ppermute(x, "tp", [(i, i ^ 1) for i in range(size)])


def minus_expm1(x):
    series = 1.0 + x * (1.0 / 7.0)
    for k in (6, 5, 4, 3, 2):
        series = 1.0 + x * (1.0 / k) * series
    return jnp.where(x > -0.35, -x * series, 1.0 - jnp.exp(x))


def recurrence_kernel(
    x_ref, rim_ref, filter_ref, recur_ref, input_ref, raw_ref, boost_ref,
    state_ref, running_ref, total_ref, ext, decay, drive, gates,
):
    tokens, channels = x_ref.shape
    taps = filter_ref.shape[0]
    blocks, wide, _ = recur_ref.shape
    gates[...] = jnp.zeros_like(gates)
    for at, matrix in ((0, recur_ref), (channels, input_ref)):
        for k in range(blocks):
            low = k * wide
            gates[low : low + wide, at + low : at + low + wide] = matrix[k]
    lead = 8
    ext[lead - taps + 1 : lead, :] = rim_ref[...].astype(jnp.float32)
    ext[lead : lead + tokens, :] = x_ref[...].astype(jnp.float32)
    first = lead - taps + 1
    mixed = ext[first : first + tokens, :] * filter_ref[0:1, :]
    for k in range(1, taps):
        mixed = mixed + ext[first + k : first + k + tokens, :] * filter_ref[k : k + 1, :]
    smoothed = mixed.astype(jnp.bfloat16)
    logits = jnp.dot(smoothed, gates[...], preferred_element_type=jnp.float32)
    both = jax.nn.sigmoid(logits)
    minus_raw = -raw_ref[...]
    soft = jnp.maximum(minus_raw, 0.0) + jnp.log1p(jnp.exp(-jnp.abs(minus_raw)))
    log_decay = both[:, :channels] * (-RECURRENT_SCALE * soft) + boost_ref[...]
    decay[...] = jnp.exp(log_decay)
    drive[...] = jnp.sqrt(minus_expm1(2.0 * log_decay)) * (
        both[:, channels:] * smoothed.astype(jnp.float32)
    )
    length = tokens // SEGMENTS

    def step(i, held):
        state, running = held
        rows = pl.ds(i, SEGMENTS, stride=length)
        a, b = decay[rows, :], drive[rows, :]
        state, running = a * state + b, running * a
        state_ref[rows, :] = state
        running_ref[rows, :] = running
        return state, running

    start = (jnp.zeros((SEGMENTS, channels), jnp.float32), jnp.ones((SEGMENTS, channels), jnp.float32))
    state, running = lax.fori_loop(0, length, step, start, unroll=8)
    whole_a, whole_b = running[0:1], state[0:1]
    for k in range(1, SEGMENTS):
        whole_b = running[k : k + 1] * whole_b + state[k : k + 1]
        whole_a = whole_a * running[k : k + 1]
    total_ref[:, 0:1, :] = jnp.broadcast_to(whole_a[None], (total_ref.shape[0], 1, channels))
    total_ref[:, 1:2, :] = jnp.broadcast_to(whole_b[None], (total_ref.shape[0], 1, channels))


def branch_kernel(place_ref, pieces_ref, state_ref, running_ref, gate_ref, out_ref):
    place = place_ref[0]
    devices, _, channels = pieces_ref.shape
    carry = jnp.zeros((1, channels), jnp.float32)
    for k in range(devices):
        piece = pieces_ref[k]
        carry = jnp.where(k < place, piece[0:1] * carry + piece[1:2], carry)
    length = state_ref.shape[0] // SEGMENTS
    for k in range(SEGMENTS):
        rows = slice(k * length, (k + 1) * length)
        state = state_ref[rows, :] + running_ref[rows, :] * carry
        g = gate_ref[rows, :].astype(jnp.float32)
        gelu = 0.5 * g * (1.0 + jnp.tanh(GELU_SCALE * (g + 0.044715 * (g * g * g))))
        out_ref[rows, :] = (gelu * state).astype(jnp.bfloat16)
        carry = state[length - 1 : length, :]


def slots_kernel(routes_ref, column_ref, line_ref):
    rows = routes_ref.shape[0]
    experts = 32
    number = lax.broadcasted_iota(jnp.int32, (rows, experts), 1)
    hot = [(routes_ref[:, k : k + 1] == number).astype(jnp.float32) for k in range(2)]
    earlier = (
        lax.broadcasted_iota(jnp.int32, (rows, rows), 1)
        < lax.broadcasted_iota(jnp.int32, (rows, rows), 0)
    ).astype(jnp.float32)
    before = jnp.dot(earlier, hot[0] + hot[1], preferred_element_type=jnp.float32)
    wide = line_ref.shape[1]
    lane = lax.broadcasted_iota(jnp.int32, (rows, wide), 1)
    same = lane % rows == lax.broadcasted_iota(jnp.int32, (rows, wide), 0)
    for k in range(2):
        rank = jnp.sum(before * hot[k], axis=1, keepdims=True).astype(jnp.int32)
        slot = routes_ref[:, k : k + 1] * CAP + rank
        column_ref[k * rows : (k + 1) * rows, :] = slot * PIECES
        spread = jnp.where(same, (slot * PIECES).astype(jnp.float32), 0.0)
        line_ref[k : k + 1, :] = (
            jnp.sum(spread, axis=0, keepdims=True).astype(jnp.int32) + lane[0:1] // rows
        )


def mix_kernel(
    branch_ref, weight_ref, resid_ref, gain_ref, line_ref, stream_ref, out_ref, total
):
    step = pl.program_id(0)
    branch = jnp.concatenate([branch_ref[k] for k in range(branch_ref.shape[0])], axis=1)
    term = jnp.dot(branch, weight_ref[...], preferred_element_type=jnp.float32)

    @pl.when(step == 0)
    def _():
        total[...] = term

    @pl.when(step > 0)
    def _():
        total[...] += term

    @pl.when(step == pl.num_programs(0) - 1)
    def _():
        rows, width = resid_ref.shape
        stream = (resid_ref[...].astype(jnp.float32) + total[...]).astype(jnp.bfloat16)
        stream_ref[...] = stream
        wide = stream.astype(jnp.float32)
        mean = jnp.sum(wide * wide, axis=1, keepdims=True) * (1.0 / width)
        normed = (wide * lax.rsqrt(mean + EPSILON) * gain_ref[...]).astype(jnp.bfloat16)
        piece = width // PIECES
        stacked = jnp.concatenate(
            [normed[:, k * piece : (k + 1) * piece] for k in range(PIECES)], axis=0
        )
        spot = lax.broadcasted_iota(jnp.int32, (out_ref.shape[0], rows * PIECES), 0)
        pick = (line_ref[0:1, :] == spot) | (line_ref[1:2, :] == spot)
        pick = pick.astype(jnp.float32).astype(jnp.bfloat16)
        out_ref[...] = jnp.dot(pick, stacked, preferred_element_type=jnp.float32).astype(
            jnp.bfloat16
        )


def expert_kernel(rows_ref, gate_ref, up_ref, down_ref, out_ref):
    rows = rows_ref[...]
    gate = jnp.dot(rows, gate_ref[...], preferred_element_type=jnp.float32)
    upward = jnp.dot(rows, up_ref[...], preferred_element_type=jnp.float32)
    active = (jax.nn.silu(gate) * upward).astype(jnp.bfloat16)
    out_ref[...] = jnp.dot(active, down_ref[...], preferred_element_type=jnp.float32).astype(
        jnp.bfloat16
    )


def combine_kernel(stream_ref, returned_ref, column_ref, weight_ref, out_ref):
    rows, width = stream_ref.shape
    piece = width // PIECES
    spot = lax.broadcasted_iota(jnp.int32, (2 * rows, returned_ref.shape[0]), 1)
    for k in range(PIECES):
        pick = (column_ref[...] + k == spot).astype(jnp.float32).astype(jnp.bfloat16)
        chosen = jnp.dot(pick, returned_ref[...], preferred_element_type=jnp.float32)
        lanes = slice(k * piece, (k + 1) * piece)
        total = weight_ref[:, 0:1] * chosen[:rows] + weight_ref[:, 1:2] * chosen[rows:]
        out_ref[:, lanes] = (stream_ref[:, lanes].astype(jnp.float32) + total).astype(jnp.bfloat16)


def natural(own, other, core, axis):
    return jnp.where(
        core == 0,
        jnp.concatenate([own, other], axis=axis),
        jnp.concatenate([other, own], axis=axis),
    )


def layer(
    resid,
    recurrent_input,
    recurrent_out_gate,
    filter_weight,
    recurrence_gate_matrix,
    input_gate_matrix,
    channel_decay_raw,
    token_decay_boost,
    output_projection_weight,
    expert_norm_gain,
    routes,
    expert_pair_weight,
    gate_weight,
    up_weight,
    down_weight,
):
    tokens, channels = recurrent_input.shape
    taps = filter_weight.shape[0]
    tp, experts = lax.axis_size("tp"), lax.axis_size("sp")
    here, place = lax.axis_index("tp"), lax.axis_index("sp")
    core = here % CORES
    chips = tp // CORES
    groups = core_groups(tp)
    rows_dev, width = resid.shape
    f32, bf16 = jnp.float32, jnp.bfloat16

    rim = shifted(recurrent_input[tokens - taps + 1 :], "sp", 1)
    projection = lax.all_gather(output_projection_weight, "tp", axis=0, tiled=True)

    own_routes = lax.dynamic_slice_in_dim(routes, here * rows_dev, rows_dev, 0)
    column, line = pl.pallas_call(
        slots_kernel,
        out_shape=(
            jax.ShapeDtypeStruct((2 * rows_dev, 1), jnp.int32),
            jax.ShapeDtypeStruct((2, PIECES * rows_dev), jnp.int32),
        ),
        in_specs=[VMEM],
        out_specs=(VMEM,) * 2,
        name="slots",
    )(own_routes)

    state, running, total = pl.pallas_call(
        recurrence_kernel,
        out_shape=(
            jax.ShapeDtypeStruct((tokens, channels), f32),
            jax.ShapeDtypeStruct((tokens, channels), f32),
            jax.ShapeDtypeStruct((experts, 2, channels), f32),
        ),
        in_specs=[VMEM] * 7,
        out_specs=(VMEM,) * 3,
        scratch_shapes=[
            pltpu.VMEM((tokens + 8, channels), f32),
            pltpu.VMEM((tokens, channels), f32),
            pltpu.VMEM((tokens, channels), f32),
            pltpu.VMEM((channels, 2 * channels), bf16),
        ],
        cost_estimate=pl.CostEstimate(flops=10**9, bytes_accessed=2**20, transcendentals=0),
        name="recurrence",
    )(
        recurrent_input,
        rim,
        filter_weight,
        recurrence_gate_matrix,
        input_gate_matrix,
        channel_decay_raw[None, :],
        token_decay_boost,
    )

    pieces = lax.all_to_all(total, "sp", 0, 0, tiled=True)
    branch = pl.pallas_call(
        branch_kernel,
        out_shape=jax.ShapeDtypeStruct((tokens, channels), bf16),
        in_specs=[SMEM] + [VMEM] * 4,
        out_specs=VMEM,
        name="branch",
    )(place.astype(jnp.int32)[None], pieces, state, running, recurrent_out_gate)
    mine = lax.all_to_all(branch.reshape(tp, rows_dev, channels), "tp", 0, 0, tiled=True)

    slot_count = experts * CAP
    depth = CORES * channels
    whole = lambda *shape: pl.BlockSpec(shape, lambda k: (0,) * len(shape))
    stream, outgoing = pl.pallas_call(
        mix_kernel,
        grid=(chips,),
        out_shape=(
            jax.ShapeDtypeStruct((rows_dev, width), bf16),
            jax.ShapeDtypeStruct((slot_count * PIECES, width // PIECES), bf16),
        ),
        in_specs=[
            pl.BlockSpec((CORES, rows_dev, channels), lambda k: (k, 0, 0)),
            pl.BlockSpec((depth, width), lambda k: (k, 0)),
            whole(rows_dev, width),
            whole(1, width),
            whole(2, PIECES * rows_dev),
        ],
        out_specs=(
            whole(rows_dev, width),
            whole(slot_count * PIECES, width // PIECES),
        ),
        scratch_shapes=[pltpu.VMEM((rows_dev, width), f32)],
        name="mix",
    )(mine, projection, resid, expert_norm_gain[None, :], line)
    packed = (experts, CAP * PIECES, width // PIECES)
    arrived = lax.all_to_all(outgoing.reshape(packed), "sp", 0, 0, tiled=True)
    arrived = arrived.reshape(slot_count, width)

    rows = lax.all_gather(arrived, "tp", axis=0, axis_index_groups=groups, tiled=True)
    arrived, down_part, gate_own, up_own = lax.optimization_barrier(
        (arrived, down_weight[0], gate_weight[0], up_weight[0])
    )
    hidden = gate_own.shape[1]
    down_own = lax.all_to_all(
        down_part.reshape(chips, CORES * hidden, -1), "tp", 0, 0,
        axis_index_groups=groups, tiled=True,
    )
    gate = natural(gate_own, swap_cores(gate_own), core, 1)
    upward = natural(up_own, swap_cores(up_own), core, 1)
    down = natural(down_own[:, None], swap_cores(down_own)[:, None], core, 1)
    down = jnp.moveaxis(down.reshape(tp, CORES * hidden, -1), 0, 1).reshape(CORES * hidden, width)
    depth = CORES * hidden
    block = rows.shape[0] // 4
    summed = pl.pallas_call(
        expert_kernel,
        grid=(4,),
        out_shape=jax.ShapeDtypeStruct(rows.shape, bf16),
        in_specs=[
            pl.BlockSpec((block, width), lambda k: (k, 0)),
            whole(width, depth),
            whole(width, depth),
            whole(depth, width),
        ],
        out_specs=pl.BlockSpec((block, width), lambda k: (k, 0)),
        name="experts",
    )(rows, gate, upward, down)
    result = lax.psum_scatter(
        summed, "tp", scatter_dimension=0, axis_index_groups=groups, tiled=True
    )

    returned = lax.all_to_all(result.reshape(packed), "sp", 0, 0, tiled=True)
    return pl.pallas_call(
        combine_kernel,
        out_shape=jax.ShapeDtypeStruct((rows_dev, width), bf16),
        in_specs=[VMEM] * 4,
        out_specs=VMEM,
        name="combine",
    )(stream, returned.reshape(slot_count * PIECES, width // PIECES), column, expert_pair_weight)


def solution(mesh):
    placed = (
        P(("sp", "tp"), None),
        P("sp", "tp"),
        P("sp", "tp"),
        P(None, "tp"),
        P("tp", None, None),
        P("tp", None, None),
        P("tp"),
        P("sp", "tp"),
        P("tp", None),
        P(),
        P("sp", None),
        P(("sp", "tp"), None),
        P("sp", None, "tp"),
        P("sp", None, "tp"),
        P("sp", None, "tp"),
    )
    return jax.shard_map(
        layer, mesh=mesh, in_specs=placed, out_specs=P(("sp", "tp"), None), check_vma=False
    )
```

time: 266 us -> 244 us (0.917)
  the two profiles are of different devices: /device:TPU:24 before, /device:TPU:1 now
where the time goes in v2:
time: 244 us; the launch traced here: 239 us
  waiting for transfers between devices  107 us (44%)
  starting transfers between devices  58 us (24%)
  Pallas kernels  24.7 us (10%)
  blocking collectives  24.1 us (10%)
  between operations  13.2 us (5%)
  local copies, waits for them, and re-layouts  9.34 us (4%)
  other arithmetic  2.94 us (1%)
    reduce_scatter x1, waiting for transfers between devices, layer(): lax.psum_scatter(summed, 'tp', scatter_dimension=0, axis_index_groups=gro...  40.7 us
    all_to_all x1, blocking collectives, layer(): arrived = lax.all_to_all(outgoing.reshape(packed), 'sp', 0, 0, tiled=True)  24.1 us
    ppermute x3, starting transfers between devices, swap_cores(): return lax.ppermute(x, 'tp', [(i, i ^ 1) for i in range(size)])  15.4 us
    all_to_all x1, starting transfers between devices, layer(): pieces = lax.all_to_all(total, 'sp', 0, 0, tiled=True)  14.2 us
    all_gather x1, waiting for transfers between devices, layer(): lax.all_gather(arrived, 'tp', axis=0, axis_index_groups=groups, tiled=True)  13.8 us
    all_gather x1, waiting for transfers between devices, layer(): lax.all_gather(output_projection_weight, 'tp', axis=0, tiled=True)  13.4 us
    all_to_all x1, waiting for transfers between devices, layer(): returned = lax.all_to_all(result.reshape(packed), 'sp', 0, 0, tiled=True)  10.8 us
    all_to_all x1, starting transfers between devices, layer(): lax.all_to_all(branch.reshape(tp, rows_dev, channels), 'tp', 0, 0, tiled=...  10.4 us
  transfers between devices with their start and end apart: 11, of which 8 were waited for; matrix products, arithmetic and copies ran while one was open for 3% of the time, Pallas kernels for 3%

profile of v2, /device:TPU:1, one launch (start us, length us, event | category | flops | bytes accessed | tf_op | source)
XLA Modules:
  0.0 239.5 jit_solution(6332733461464593171)
XLA Ops:
  6.5 0.0 copy-start
  6.5 0.0 all-gather.3.cloned.1.call-start
  6.5 0.7 all-gather.3.cloned.1.call-update
  7.3 0.7 slice.3
  7.9 3.9 %collective-permute-start = (bf16[3,128]{1,0:T(4,128)(2,1)S(1)}, bf16[3,128]{1,0:T(4,128)(2,1)S(1)}, u32[]{:S(2)}, u32[]{:S(2)}) collective-permute-start(bf16[3,128]{1,0:T(4,128)(2,1)S(1)} %slice.3), channel_id=1, source_target_pairs={{0,16},{16,32},{32,48},{48,64},{64,80},{80,96},{96,112},{112,128},... | collective-permute-start | bytes 2312 | tf_op jit(solution)/shard_map/ppermute | solution.py:24
  11.9 0.7 collective-permute-done.rim_ref
  12.6 0.0 copy-start.7
  12.6 0.6 copy-done.7
  13.2 3.2 %recurrence.1 = (f32[512,128]{1,0:T(8,128)}, f32[512,128]{1,0:T(8,128)}, f32[32,2,128]{2,1,0:T(2,128)}) custom-call(bf16[512,128]{1,0:T(8,128)(2,1)} %x_ref.1, bf16[3,128]{1,0:T(4,128)(2,1)} %copy-done.7, f32[4,128]{1,0:T(4,128)} %filter_ref.1, bf16[2,64,64]{2,1,0:T(8,128)(2,1)} %recur_ref.1, bf16[2,64,64]{2,1,0:T(8,128)(2,1)} %input_ref.1, ...), custom_call_target="tpu_custom_call" | custom-call | flops 1000000000 | bytes 1048576 | tf_op jit(solution)/shard_map/recurrence/pallas_call | solution.py:240
  16.4 14.2 %all-to-all-start = ((f32[32,2,128]{2,1,0:T(2,128)}), f32[32,2,128]{2,1,0:T(2,128)S(1)}, u32[]{:S(2)}, u32[]{:S(2)}) async-start(f32[32,2,128]{2,1,0:T(2,128)} %get-tuple-element.15), calls=%async_computation | async-start | bytes 65536 | tf_op jit(solution)/shard_map/all_to_all | solution.py:267
  30.6 8.7 %all-to-all-done.pieces_ref = f32[32,2,128]{2,1,0:T(2,128)S(1)} async-done(((f32[32,2,128]{2,1,0:T(2,128)}), f32[32,2,128]{2,1,0:T(2,128)S(1)}, u32[]{:S(2)}, u32[]{:S(2)}) %all-to-all-start) | async-done | bytes 32800 | tf_op jit(solution)/shard_map/all_to_all | solution.py:267
  39.3 0.0 copy-start.5
  39.3 0.6 copy-done.5
  39.9 1.9 branch.1
  41.8 10.4 %all-to-all-start.1 = ((bf16[16,32,128]{2,1,0:T(8,128)(2,1)}), bf16[16,32,128]{2,1,0:T(8,128)(2,1)S(1)}, u32[]{:S(2)}, u32[]{:S(2)}) async-start(bf16[16,32,128]{2,1,0:T(8,128)(2,1)} %bitcast.28), calls=%async_computation.1 | async-start | bytes 262144 | tf_op jit(solution)/shard_map/all_to_all | solution.py:275
  52.2 0.0 all-gather.5.cloned.1.call-start
  52.2 0.0 copy-done
  52.2 0.1 constant_dynamic-slice_fusion
  52.3 0.7 copy.19.routes_ref
  53.0 1.7 slots.1
  54.7 8.2 %all-to-all-done.1.branch_ref = bf16[16,32,128]{2,1,0:T(8,128)(2,1)S(1)} async-done(((bf16[16,32,128]{2,1,0:T(8,128)(2,1)}), bf16[16,32,128]{2,1,0:T(8,128)(2,1)S(1)}, u32[]{:S(2)}, u32[]{:S(2)}) %all-to-all-start.1) | async-done | bytes 131104 | tf_op jit(solution)/shard_map/all_to_all | solution.py:275
  62.9 0.0 copy-start.2
  62.9 13.4 %all-gather.3.cloned.1.call-done.weight_ref = bf16[2048,2048]{1,0:T(8,128)(2,1)} async-done(((bf16[128,2048]{1,0:T(8,128)(2,1)}), bf16[2048,2048]{1,0:T(8,128)(2,1)}) %all-gather.3.cloned.1.call-update) | async-done | bytes 8388624 | tf_op jit(solution)/shard_map/all_gather | solution.py:226
  76.3 0.0 copy-done.2
  76.3 8.2 %mix.1 = (bf16[32,2048]{1,0:T(8,128)(2,1)}, bf16[768,256]{1,0:T(8,128)(2,1)}) custom-call(bf16[16,32,128]{2,1,0:T(8,128)(2,1)} %copy-done.2, bf16[2048,2048]{1,0:T(8,128)(2,1)} %all-gather.3.cloned.1.call-done.weight_ref, bf16[32,2048]{1,0:T(8,128)(2,1)} %resid_ref.1, f32[1,2048]{1,0:T(1,128)} %bitcast.30, s32[2,256]{1,0:T(2,128)} %get-tuple-element.18.line_ref), custom_call_target="tpu_custom_call" | custom-call | tf_op jit(solution)/shard_map/mix/pallas_call | solution.py:280
  84.6 0.0 copy-start.3
  84.6 0.0 copy-start.4
  84.6 24.1 %all_to_all.25 = bf16[32,24,256]{2,1,0:T(8,128)(2,1)S(1)} all-to-all(bf16[32,24,256]{2,1,0:T(8,128)(2,1)} %bitcast.29), channel_id=1, replica_groups=mesh['sp'=32,'tp'=16] {'sp'}, dimensions={0} | all-to-all | bytes 786432 | tf_op jit(solution)/shard_map/all_to_all | solution.py:302
  108.7 0.9 reshape.28
  109.6 0.0 all-gather.5.cloned.1.call-update
  109.6 4.2 %all-to-all-start.3 = ((bf16[8,256,128]{2,1,0:T(8,128)(2,1)}), bf16[8,256,128]{2,1,0:T(8,128)(2,1)S(1)}, u32[]{:S(2)}, u32[]{:S(2)}) async-start(bf16[8,256,128]{2,1,0:T(8,128)(2,1)} %bitcast.8), calls=%async_computation.3 | async-start | bytes 1048576 | tf_op jit(solution)/shard_map/all_to_all | solution.py:310
  113.8 0.0 reduce-scatter.2.cloned.1.call-start
  113.9 0.0 copy-done.3
  113.9 4.4 %collective-permute-start.1 = (bf16[2048,128]{1,0:T(8,128)(2,1)S(1)}, bf16[2048,128]{1,0:T(8,128)(2,1)S(1)}, u32[]{:S(2)}, u32[]{:S(2)}) collective-permute-start(bf16[2048,128]{1,0:T(8,128)(2,1)S(1)} %bitcast.23), channel_id=1, source_target_pairs={{0,1},{1,0},{2,3},{3,2},{4,5},{5,4},{6,7},{7,6},{8,9},{9,8},{10,11... | collective-permute-start | bytes 1572872 | tf_op jit(solution)/shard_map/ppermute | solution.py:33
  118.3 0.0 copy-done.4
  118.3 1.9 collective-permute-start.2
  120.2 10.1 %all-to-all-done.3 = bf16[8,256,128]{2,1,0:T(8,128)(2,1)S(1)} async-done(((bf16[8,256,128]{2,1,0:T(8,128)(2,1)}), bf16[8,256,128]{2,1,0:T(8,128)(2,1)S(1)}, u32[]{:S(2)}, u32[]{:S(2)}) %all-to-all-start.3) | async-done | bytes 524320 | tf_op jit(solution)/shard_map/all_to_all | solution.py:310
  130.3 9.0 %collective-permute-start.3 = (bf16[8,256,128]{2,1,0:T(8,128)(2,1)S(1)}, bf16[8,256,128]{2,1,0:T(8,128)(2,1)S(1)}, u32[]{:S(2)}, u32[]{:S(2)}) collective-permute-start(bf16[8,256,128]{2,1,0:T(8,128)(2,1)S(1)} %all-to-all-done.3), channel_id=1, source_target_pairs={{0,1},{1,0},{2,3},{3,2},{4,5},{5,4},{6,7},{7,6},{8,9},{9,8},{10,11... | collective-permute-start | bytes 1572872 | tf_op jit(solution)/shard_map/ppermute | solution.py:33
  139.4 0.0 collective-permute-done.1
  139.4 1.3 maximum_select_fusion.gate_ref
  140.7 0.0 collective-permute-done.2
  140.7 1.4 maximum_select_fusion.1.up_ref
  142.2 0.0 collective-permute-done.3
  142.2 0.2 maximum_select_fusion.2
  142.3 1.1 copy.17
  143.4 1.3 copy.22
  144.8 13.8 %all-gather.5.cloned.1.call-done.rows_ref = bf16[768,2048]{1,0:T(8,128)(2,1)} async-done(((bf16[96,2048]{1,0:T(8,128)(2,1)}), bf16[768,2048]{1,0:T(8,128)(2,1)}) %all-gather.5.cloned.1.call-update) | async-done | bytes 3145744 | tf_op jit(solution)/shard_map/all_gather | solution.py:305
  158.6 7.2 %experts.1 = bf16[768,2048]{1,0:T(8,128)(2,1)} custom-call(bf16[768,2048]{1,0:T(8,128)(2,1)} %all-gather.5.cloned.1.call-done.rows_ref, bf16[2048,256]{1,0:T(8,128)(2,1)} %maximum_select_fusion.gate_ref, bf16[2048,256]{1,0:T(8,128)(2,1)} %maximum_select_fusion.1.up_ref, bf16[256,2048]{1,0:T(8,128)(2,1)} %bitcast.19), custom_call_target="tpu_custom_call" | custom-call | tf_op jit(solution)/shard_map/experts/pallas_call | solution.py:320
  165.8 0.0 copy-start.6
  165.8 0.0 reduce-scatter.2.cloned.1.call-update
  165.8 40.7 %reduce-scatter.2.cloned.1.call-done = bf16[96,2048]{1,0:T(8,128)(2,1)} async-done(((bf16[768,2048]{1,0:T(8,128)(2,1)}), bf16[96,2048]{1,0:T(8,128)(2,1)}) %reduce-scatter.2.cloned.1.call-update) | async-done | bytes 393232 | tf_op jit(solution)/shard_map/reduce_scatter | solution.py:333
  206.5 1.9 reshape.31
  208.4 9.9 %all-to-all-start.4 = ((bf16[32,24,256]{2,1,0:T(8,128)(2,1)}), bf16[32,24,256]{2,1,0:T(8,128)(2,1)S(1)}, u32[]{:S(2)}, u32[]{:S(2)}) async-start(bf16[32,24,256]{2,1,0:T(8,128)(2,1)} %reshape.31), calls=%async_computation.5 | async-start | bytes 786432 | tf_op jit(solution)/shard_map/all_to_all | solution.py:337
  218.3 0.0 copy-done.6
  218.3 0.7 copy.18.weight_ref
  219.0 10.8 %all-to-all-done.4 = bf16[32,24,256]{2,1,0:T(8,128)(2,1)S(1)} async-done(((bf16[32,24,256]{2,1,0:T(8,128)(2,1)}), bf16[32,24,256]{2,1,0:T(8,128)(2,1)S(1)}, u32[]{:S(2)}, u32[]{:S(2)}) %all-to-all-start.4) | async-done | bytes 393248 | tf_op jit(solution)/shard_map/all_to_all | solution.py:337
  229.8 0.0 copy-start.1
  229.8 0.8 copy-done.1
  230.5 2.4 %combine.1 = bf16[32,2048]{1,0:T(8,128)(2,1)} custom-call(bf16[32,2048]{1,0:T(8,128)(2,1)} %get-tuple-element.19.stream_ref, bf16[768,256]{1,0:T(8,128)(2,1)} %bitcast.22, s32[64,1]{1,0:T(8,128)} %get-tuple-element.24.column_ref, f32[32,2]{1,0:T(8,128)} %copy.18.weight_ref), custom_call_target="tpu_custom_call" | custom-call | tf_op jit(solution)/shard_map/combine/pallas_call | solution.py:338
Async XLA Ops:
  6.5 45.7 %copy-start = (s32[512,2]{0,1:T(2,128)S(1)}, s32[512,2]{0,1:T(2,128)}, u32[]{:S(2)}) copy-start(s32[512,2]{0,1:T(2,128)} %param.25) | copy-start | bytes 12292
  6.5 69.8 %all-gather.3.cloned.1.call-start = ((), (), s32[]{:S(2)}) async-start(), calls=%async_computation.6 | async-start | bytes 8912896 | tf_op jit(solution)/shard_map/all_gather | solution.py:226
  7.9 4.6 %collective-permute-start = (bf16[3,128]{1,0:T(4,128)(2,1)S(1)}, bf16[3,128]{1,0:T(4,128)(2,1)S(1)}, u32[]{:S(2)}, u32[]{:S(2)}) collective-permute-start(bf16[3,128]{1,0:T(4,128)(2,1)S(1)} %slice.3), channel_id=1, source_target_pairs={{0,16},{16,32},{32,48},{48,64},{64,80},{80,96},{96,112},{112,128},... | collective-permute-start | bytes 2312 | tf_op jit(solution)/shard_map/ppermute | solution.py:24
  12.6 0.6 copy-start.7
  16.4 22.9 %all-to-all-start = ((f32[32,2,128]{2,1,0:T(2,128)}), f32[32,2,128]{2,1,0:T(2,128)S(1)}, u32[]{:S(2)}, u32[]{:S(2)}) async-start(f32[32,2,128]{2,1,0:T(2,128)} %get-tuple-element.15), calls=%async_computation | async-start | bytes 65536 | tf_op jit(solution)/shard_map/all_to_all | solution.py:267
  39.3 0.6 copy-start.5
  41.8 21.1 %all-to-all-start.1 = ((bf16[16,32,128]{2,1,0:T(8,128)(2,1)}), bf16[16,32,128]{2,1,0:T(8,128)(2,1)S(1)}, u32[]{:S(2)}, u32[]{:S(2)}) async-start(bf16[16,32,128]{2,1,0:T(8,128)(2,1)} %bitcast.28), calls=%async_computation.1 | async-start | bytes 262144 | tf_op jit(solution)/shard_map/all_to_all | solution.py:275
  52.2 106.4 %all-gather.5.cloned.1.call-start = ((), (), s32[]{:S(2)}) async-start(), calls=%async_computation.7 | async-start | bytes 3538944 | tf_op jit(solution)/shard_map/all_gather | solution.py:305
  62.9 13.4 %copy-start.2 = (bf16[16,32,128]{2,1,0:T(8,128)(2,1)}, bf16[16,32,128]{2,1,0:T(8,128)(2,1)S(1)}, u32[]{:S(2)}) copy-start(bf16[16,32,128]{2,1,0:T(8,128)(2,1)S(1)} %all-to-all-done.1.branch_ref) | copy-start | bytes 393220
  84.6 29.3 %copy-start.3 = (bf16[1,2048,128]{2,1,0:T(8,128)(2,1)S(1)}, bf16[1,2048,128]{2,1,0:T(8,128)(2,1)}, u32[]{:S(2)}) copy-start(bf16[1,2048,128]{2,1,0:T(8,128)(2,1)} %param.27) | copy-start | bytes 1572868
  84.6 33.7 %copy-start.4 = (bf16[1,2048,128]{2,1,0:T(8,128)(2,1)S(1)}, bf16[1,2048,128]{2,1,0:T(8,128)(2,1)}, u32[]{:S(2)}) copy-start(bf16[1,2048,128]{2,1,0:T(8,128)(2,1)} %param.28) | copy-start | bytes 1572868
  109.6 20.7 %all-to-all-start.3 = ((bf16[8,256,128]{2,1,0:T(8,128)(2,1)}), bf16[8,256,128]{2,1,0:T(8,128)(2,1)S(1)}, u32[]{:S(2)}, u32[]{:S(2)}) async-start(bf16[8,256,128]{2,1,0:T(8,128)(2,1)} %bitcast.8), calls=%async_computation.3 | async-start | bytes 1048576 | tf_op jit(solution)/shard_map/all_to_all | solution.py:310
  113.8 92.7 %reduce-scatter.2.cloned.1.call-start = ((), (), s32[]{:S(2)}) async-start(), calls=%async_computation.8 | async-start | bytes 3538944 | tf_op jit(solution)/shard_map/reduce_scatter | solution.py:333
  113.9 25.5 %collective-permute-start.1 = (bf16[2048,128]{1,0:T(8,128)(2,1)S(1)}, bf16[2048,128]{1,0:T(8,128)(2,1)S(1)}, u32[]{:S(2)}, u32[]{:S(2)}) collective-permute-start(bf16[2048,128]{1,0:T(8,128)(2,1)S(1)} %bitcast.23), channel_id=1, source_target_pairs={{0,1},{1,0},{2,3},{3,2},{4,5},{5,4},{6,7},{7,6},{8,9},{9,8},{10,11... | collective-permute-start | bytes 1572872 | tf_op jit(solution)/shard_map/ppermute | solution.py:33
  118.3 22.4 %collective-permute-start.2 = (bf16[2048,128]{1,0:T(8,128)(2,1)S(1)}, bf16[2048,128]{1,0:T(8,128)(2,1)S(1)}, u32[]{:S(2)}, u32[]{:S(2)}) collective-permute-start(bf16[2048,128]{1,0:T(8,128)(2,1)S(1)} %bitcast.25), channel_id=1, source_target_pairs={{0,1},{1,0},{2,3},{3,2},{4,5},{5,4},{6,7},{7,6},{8,9},{9,8},{10,11... | collective-permute-start | bytes 1572872 | tf_op jit(solution)/shard_map/ppermute | solution.py:33
  130.3 11.9 %collective-permute-start.3 = (bf16[8,256,128]{2,1,0:T(8,128)(2,1)S(1)}, bf16[8,256,128]{2,1,0:T(8,128)(2,1)S(1)}, u32[]{:S(2)}, u32[]{:S(2)}) collective-permute-start(bf16[8,256,128]{2,1,0:T(8,128)(2,1)S(1)} %all-to-all-done.3), channel_id=1, source_target_pairs={{0,1},{1,0},{2,3},{3,2},{4,5},{5,4},{6,7},{7,6},{8,9},{9,8},{10,11... | collective-permute-start | bytes 1572872 | tf_op jit(solution)/shard_map/ppermute | solution.py:33
  165.8 52.6 %copy-start.6 = (f32[32,2]{0,1:T(2,128)S(1)}, f32[32,2]{0,1:T(2,128)}, u32[]{:S(2)}) copy-start(f32[32,2]{0,1:T(2,128)} %param.26) | copy-start | bytes 772
  208.4 21.3 %all-to-all-start.4 = ((bf16[32,24,256]{2,1,0:T(8,128)(2,1)}), bf16[32,24,256]{2,1,0:T(8,128)(2,1)S(1)}, u32[]{:S(2)}, u32[]{:S(2)}) async-start(bf16[32,24,256]{2,1,0:T(8,128)(2,1)} %reshape.31), calls=%async_computation.5 | async-start | bytes 786432 | tf_op jit(solution)/shard_map/all_to_all | solution.py:337
  229.8 0.8 copy-start.1
Sparse Core Ops, SparseCore 0:
  9.5 66.8 all-gather.2
  109.8 48.7 all-gather.4
  165.9 40.5 reduce-scatter.1

commit v3 on v2

--- a/solution.py
+++ b/solution.py
@@ -12,6 +12,7 @@
 CORES = 2
 CAP = 3
 PIECES = 8
+INNER = 4
 GELU_SCALE = 0.7978845608028654
 
 VMEM = pl.BlockSpec(memory_space=pltpu.VMEM)
@@ -26,6 +27,15 @@
 
 def core_groups(size):
     return [[core + CORES * y for y in range(size // CORES)] for core in range(CORES)]
+
+
+def halves_of_chips(size):
+    return [[i for i in range(size) if i // CORES % 2 == side] for side in range(2)]
+
+
+def swap_neighbours(x):
+    size = lax.axis_size("tp")
+    return lax.ppermute(x, "tp", [(i, i ^ CORES) for i in range(size)])
 
 
 def swap_cores(x):
@@ -90,20 +100,35 @@
     total_ref[:, 1:2, :] = jnp.broadcast_to(whole_b[None], (total_ref.shape[0], 1, channels))
 
 
-def branch_kernel(place_ref, pieces_ref, state_ref, running_ref, gate_ref, out_ref):
-    place = place_ref[0]
-    devices, _, channels = pieces_ref.shape
-    carry = jnp.zeros((1, channels), jnp.float32)
-    for k in range(devices):
-        piece = pieces_ref[k]
-        carry = jnp.where(k < place, piece[0:1] * carry + piece[1:2], carry)
+def inner_kernel(pieces_ref, total_ref):
+    count, _, channels = pieces_ref.shape
+    whole_a, whole_b = pieces_ref[0, 0:1, :], pieces_ref[0, 1:2, :]
+    for k in range(1, count):
+        a, b = pieces_ref[k, 0:1, :], pieces_ref[k, 1:2, :]
+        whole_b = a * whole_b + b
+        whole_a = whole_a * a
+    total_ref[:, 0:1, :] = jnp.broadcast_to(whole_a[None], (total_ref.shape[0], 1, channels))
+    total_ref[:, 1:2, :] = jnp.broadcast_to(whole_b[None], (total_ref.shape[0], 1, channels))
+
+
+def branch_kernel(place_ref, outer_ref, inner_ref, state_ref, running_ref, gate_ref, out_ref):
+    carry = jnp.zeros((1, state_ref.shape[1]), jnp.float32)
+    for place, pieces in ((place_ref[0], outer_ref), (place_ref[1], inner_ref)):
+        for k in range(pieces.shape[0]):
+            after = pieces[k, 0:1, :] * carry + pieces[k, 1:2, :]
+            carry = jnp.where(k < place, after, carry)
     length = state_ref.shape[0] // SEGMENTS
+    half = length // CORES
     for k in range(SEGMENTS):
         rows = slice(k * length, (k + 1) * length)
         state = state_ref[rows, :] + running_ref[rows, :] * carry
         g = gate_ref[rows, :].astype(jnp.float32)
         gelu = 0.5 * g * (1.0 + jnp.tanh(GELU_SCALE * (g + 0.044715 * (g * g * g))))
-        out_ref[rows, :] = (gelu * state).astype(jnp.bfloat16)
+        branch = (gelu * state).astype(jnp.bfloat16)
+        for core in range(CORES):
+            out_ref[k // 2 * CORES + core, k % 2 * half : (k % 2 + 1) * half, :] = branch[
+                core * half : (core + 1) * half
+            ]
         carry = state[length - 1 : length, :]
 
 
@@ -130,9 +155,7 @@
         )
 
 
-def mix_kernel(
-    branch_ref, weight_ref, resid_ref, gain_ref, line_ref, stream_ref, out_ref, total
-):
+def project_kernel(side_ref, branch_ref, weight_ref, keep_ref, send_ref, total):
     step = pl.program_id(0)
     branch = jnp.concatenate([branch_ref[k] for k in range(branch_ref.shape[0])], axis=1)
     term = jnp.dot(branch, weight_ref[...], preferred_element_type=jnp.float32)
@@ -147,22 +170,28 @@
 
     @pl.when(step == pl.num_programs(0) - 1)
     def _():
-        rows, width = resid_ref.shape
-        stream = (resid_ref[...].astype(jnp.float32) + total[...]).astype(jnp.bfloat16)
-        stream_ref[...] = stream
-        wide = stream.astype(jnp.float32)
-        mean = jnp.sum(wide * wide, axis=1, keepdims=True) * (1.0 / width)
-        normed = (wide * lax.rsqrt(mean + EPSILON) * gain_ref[...]).astype(jnp.bfloat16)
-        piece = width // PIECES
-        stacked = jnp.concatenate(
-            [normed[:, k * piece : (k + 1) * piece] for k in range(PIECES)], axis=0
-        )
-        spot = lax.broadcasted_iota(jnp.int32, (out_ref.shape[0], rows * PIECES), 0)
-        pick = (line_ref[0:1, :] == spot) | (line_ref[1:2, :] == spot)
-        pick = pick.astype(jnp.float32).astype(jnp.bfloat16)
-        out_ref[...] = jnp.dot(pick, stacked, preferred_element_type=jnp.float32).astype(
-            jnp.bfloat16
-        )
+        side, rows = side_ref[0], keep_ref.shape[0]
+        keep_ref[...] = total[pl.ds(pl.multiple_of(side * rows, rows), rows), :]
+        other = pl.ds(pl.multiple_of((1 - side) * rows, rows), rows)
+        send_ref[...] = total[other, :].astype(jnp.bfloat16)
+
+
+def dispatch_kernel(keep_ref, got_ref, resid_ref, gain_ref, line_ref, stream_ref, out_ref):
+    rows, width = resid_ref.shape
+    projected = keep_ref[...] + got_ref[...].astype(jnp.float32)
+    stream = (resid_ref[...].astype(jnp.float32) + projected).astype(jnp.bfloat16)
+    stream_ref[...] = stream
+    wide = stream.astype(jnp.float32)
+    mean = jnp.sum(wide * wide, axis=1, keepdims=True) * (1.0 / width)
+    normed = (wide * lax.rsqrt(mean + EPSILON) * gain_ref[...]).astype(jnp.bfloat16)
+    piece = width // PIECES
+    stacked = jnp.concatenate(
+        [normed[:, k * piece : (k + 1) * piece] for k in range(PIECES)], axis=0
+    )
+    spot = lax.broadcasted_iota(jnp.int32, (out_ref.shape[0], rows * PIECES), 0)
+    pick = (line_ref[0:1, :] == spot) | (line_ref[1:2, :] == spot)
+    pick = pick.astype(jnp.float32).astype(jnp.bfloat16)
+    out_ref[...] = jnp.dot(pick, stacked, preferred_element_type=jnp.float32).astype(jnp.bfloat16)
 
 
 def expert_kernel(rows_ref, gate_ref, up_ref, down_ref, out_ref):
@@ -218,12 +247,18 @@
     here, place = lax.axis_index("tp"), lax.axis_index("sp")
     core = here % CORES
     chips = tp // CORES
-    groups = core_groups(tp)
+    groups, halves = core_groups(tp), halves_of_chips(tp)
+    side = here // CORES % 2
+    outer = experts // INNER
+    inner_groups = [[k * INNER + i for i in range(INNER)] for k in range(outer)]
+    outer_groups = [[k * INNER + i for k in range(outer)] for i in range(INNER)]
     rows_dev, width = resid.shape
     f32, bf16 = jnp.float32, jnp.bfloat16
 
     rim = shifted(recurrent_input[tokens - taps + 1 :], "sp", 1)
-    projection = lax.all_gather(output_projection_weight, "tp", axis=0, tiled=True)
+    projection = lax.all_gather(
+        output_projection_weight, "tp", axis=0, axis_index_groups=halves, tiled=True
+    )
 
     own_routes = lax.dynamic_slice_in_dim(routes, here * rows_dev, rows_dev, 0)
     column, line = pl.pallas_call(
@@ -242,7 +277,7 @@
         out_shape=(
             jax.ShapeDtypeStruct((tokens, channels), f32),
             jax.ShapeDtypeStruct((tokens, channels), f32),
-            jax.ShapeDtypeStruct((experts, 2, channels), f32),
+            jax.ShapeDtypeStruct((INNER, 2, channels), f32),
         ),
         in_specs=[VMEM] * 7,
         out_specs=(VMEM,) * 3,
@@ -264,40 +299,62 @@
         token_decay_boost,
     )
 
-    pieces = lax.all_to_all(total, "sp", 0, 0, tiled=True)
+    inner_pieces = lax.all_to_all(
+        total, "sp", 0, 0, axis_index_groups=inner_groups, tiled=True
+    )
+    total = pl.pallas_call(
+        inner_kernel,
+        out_shape=jax.ShapeDtypeStruct((outer, 2, channels), f32),
+        in_specs=[VMEM],
+        out_specs=VMEM,
+        name="inner",
+    )(inner_pieces)
+    outer_pieces = lax.all_to_all(
+        total, "sp", 0, 0, axis_index_groups=outer_groups, tiled=True
+    )
+    peers = tp // 2
     branch = pl.pallas_call(
         branch_kernel,
-        out_shape=jax.ShapeDtypeStruct((tokens, channels), bf16),
-        in_specs=[SMEM] + [VMEM] * 4,
+        out_shape=jax.ShapeDtypeStruct((peers, 2 * rows_dev, channels), bf16),
+        in_specs=[SMEM] + [VMEM] * 5,
         out_specs=VMEM,
         name="branch",
-    )(place.astype(jnp.int32)[None], pieces, state, running, recurrent_out_gate)
-    mine = lax.all_to_all(branch.reshape(tp, rows_dev, channels), "tp", 0, 0, tiled=True)
+    )(
+        jnp.stack([place // INNER, place % INNER]).astype(jnp.int32),
+        outer_pieces, inner_pieces, state, running, recurrent_out_gate,
+    )
+    mine = lax.all_to_all(branch, "tp", 0, 0, axis_index_groups=halves, tiled=True)
 
     slot_count = experts * CAP
     depth = CORES * channels
     whole = lambda *shape: pl.BlockSpec(shape, lambda k: (0,) * len(shape))
+    keep, send = pl.pallas_call(
+        project_kernel,
+        grid=(peers // CORES,),
+        out_shape=(
+            jax.ShapeDtypeStruct((rows_dev, width), f32),
+            jax.ShapeDtypeStruct((rows_dev, width), bf16),
+        ),
+        in_specs=[
+            SMEM,
+            pl.BlockSpec((CORES, 2 * rows_dev, channels), lambda k: (k, 0, 0)),
+            pl.BlockSpec((depth, width), lambda k: (k, 0)),
+        ],
+        out_specs=(whole(rows_dev, width),) * 2,
+        scratch_shapes=[pltpu.VMEM((2 * rows_dev, width), f32)],
+        name="project",
+    )(side.astype(jnp.int32)[None], mine, projection)
+    got = swap_neighbours(send)
     stream, outgoing = pl.pallas_call(
-        mix_kernel,
-        grid=(chips,),
+        dispatch_kernel,
         out_shape=(
             jax.ShapeDtypeStruct((rows_dev, width), bf16),
             jax.ShapeDtypeStruct((slot_count * PIECES, width // PIECES), bf16),
         ),
-        in_specs=[
-            pl.BlockSpec((CORES, rows_dev, channels), lambda k: (k, 0, 0)),
-            pl.BlockSpec((depth, width), lambda k: (k, 0)),
-            whole(rows_dev, width),
-            whole(1, width),
-            whole(2, PIECES * rows_dev),
-        ],
-        out_specs=(
-            whole(rows_dev, width),
-            whole(slot_count * PIECES, width // PIECES),
-        ),
-        scratch_shapes=[pltpu.VMEM((rows_dev, width), f32)],
-        name="mix",
-    )(mine, projection, resid, expert_norm_gain[None, :], line)
+        in_specs=[VMEM] * 5,
+        out_specs=(VMEM,) * 2,
+        name="dispatch",
+    )(keep, got, resid, expert_norm_gain[None, :], line)
     packed = (experts, CAP * PIECES, width // PIECES)
     arrived = lax.all_to_all(outgoing.reshape(packed), "sp", 0, 0, tiled=True)
     arrived = arrived.reshape(slot_count, width)

time: 244 us -> 246 us (level)
  starting transfers between devices: 58 us -> 65.6 us
  waiting for transfers between devices: 107 us -> 100 us
    all_gather x1, waiting for transfers between devices: 13.4 us -> 0.01 us  [layer(): lax.all_gather(output_projection_weight, 'tp', axis=0, axis_index_groups=...]
    all_to_all x2 -> x3, waiting for transfers between devices: 16.9 us -> 23.3 us  [the longest x1 13.1 us: layer(): lax.all_to_all(branch, 'tp', 0, 0, axis_index_groups=halves, tiled=True)]
    all_to_all x2 -> x3, starting transfers between devices: 24.6 us -> 28.5 us  [the longest x1 12.5 us: layer(): lax.all_to_all(total, 'sp', 0, 0, axis_index_groups=outer_groups, tiled=T...]
    ppermute x0 -> x1, starting transfers between devices: none -> 2.7 us  [swap_neighbours(): return lax.ppermute(x, 'tp', [(i, i ^ CORES) for i in range(size)])]
    unnamed x19 -> x23, local copies, waits for them, and re-layouts: 4.66 us -> 6.47 us
    pallas_call x2 -> x4, Pallas kernels: 10.1 us -> 9.9 us  [the longest x1 4.42 us: layer(): pl.pallas_call(project_kernel, grid=(peers // CORES,), out_shape=(jax.Sha...]
  transfers between devices with their start and end apart: 11 -> 13, of which waited for: 8 -> 9; matrix products, arithmetic and copies ran while one was open for 3% -> 3% of each run, Pallas kernels for 3% -> 3%
where the time goes in v3:
time: 246 us; the launch traced here: 242 us
  waiting for transfers between devices  100 us (41%)
  starting transfers between devices  65.6 us (27%)
  Pallas kernels  24.4 us (10%)
  blocking collectives  24.3 us (10%)
  between operations  13.2 us (5%)
  local copies, waits for them, and re-layouts  11.2 us (5%)
  other arithmetic  3.52 us (1%)
    reduce_scatter x1, waiting for transfers between devices, layer(): lax.psum_scatter(summed, 'tp', scatter_dimension=0, axis_index_groups=gro...  41.1 us
    all_to_all x1, blocking collectives, layer(): arrived = lax.all_to_all(outgoing.reshape(packed), 'sp', 0, 0, tiled=True)  24.3 us
    ppermute x3, starting transfers between devices, swap_cores(): return lax.ppermute(x, 'tp', [(i, i ^ 1) for i in range(size)])  16.8 us
    all_gather x1, waiting for transfers between devices, layer(): lax.all_gather(arrived, 'tp', axis=0, axis_index_groups=groups, tiled=True)  13.8 us
    all_to_all x1, waiting for transfers between devices, layer(): lax.all_to_all(branch, 'tp', 0, 0, axis_index_groups=halves, tiled=True)  13.1 us
    all_to_all x1, starting transfers between devices, layer(): lax.all_to_all(total, 'sp', 0, 0, axis_index_groups=outer_groups, tiled=T...  12.5 us
    all_to_all x1, starting transfers between devices, layer(): lax.all_to_all(branch, 'tp', 0, 0, axis_index_groups=halves, tiled=True)  11.5 us
    all_to_all x1, waiting for transfers between devices, layer(): returned = lax.all_to_all(result.reshape(packed), 'sp', 0, 0, tiled=True)  10.9 us
  transfers between devices with their start and end apart: 13, of which 9 were waited for; matrix products, arithmetic and copies ran while one was open for 3% of the time, Pallas kernels for 3%

profile of v3, /device:TPU:1, one launch (start us, length us, event | category | flops | bytes accessed | tf_op | source)
XLA Modules:
  0.0 242.2 jit_solution(14099524298614131741)
XLA Ops:
  6.5 0.0 copy-start
  6.5 0.0 all-gather.3.cloned.1.call-start
  6.5 0.7 all-gather.3.cloned.1.call-update
  7.3 0.7 slice.3
  7.9 3.9 %collective-permute-start = (bf16[3,128]{1,0:T(4,128)(2,1)S(1)}, bf16[3,128]{1,0:T(4,128)(2,1)S(1)}, u32[]{:S(2)}, u32[]{:S(2)}) collective-permute-start(bf16[3,128]{1,0:T(4,128)(2,1)S(1)} %slice.3), channel_id=1, source_target_pairs={{0,16},{16,32},{32,48},{48,64},{64,80},{80,96},{96,112},{112,128},... | collective-permute-start | bytes 2312 | tf_op jit(solution)/shard_map/ppermute | solution.py:25
  11.9 0.7 collective-permute-done.rim_ref
  12.6 0.0 copy-start.9
  12.6 0.5 copy-done.9
  13.1 3.2 %recurrence.1 = (f32[512,128]{1,0:T(8,128)}, f32[512,128]{1,0:T(8,128)}, f32[4,2,128]{2,1,0:T(2,128)}) custom-call(bf16[512,128]{1,0:T(8,128)(2,1)} %x_ref.1, bf16[3,128]{1,0:T(4,128)(2,1)} %copy-done.9, f32[4,128]{1,0:T(4,128)} %filter_ref.1, bf16[2,64,64]{2,1,0:T(8,128)(2,1)} %recur_ref.1, bf16[2,64,64]{2,1,0:T(8,128)(2,1)} %input_ref.1, ...), custom_call_target="tpu_custom_call" | custom-call | flops 1000000000 | bytes 1048576 | tf_op jit(solution)/shard_map/recurrence/pallas_call | solution.py:275
  16.3 4.5 %all-to-all-start = ((f32[4,2,128]{2,1,0:T(2,128)}), f32[4,2,128]{2,1,0:T(2,128)S(1)}, u32[]{:S(2)}, u32[]{:S(2)}) async-start(f32[4,2,128]{2,1,0:T(2,128)} %get-tuple-element.17), calls=%async_computation | async-start | bytes 8192 | tf_op jit(solution)/shard_map/all_to_all | solution.py:302
  20.9 4.1 %all-to-all-done.pieces_ref.inner_ref = f32[4,2,128]{2,1,0:T(2,128)S(1)} async-done(((f32[4,2,128]{2,1,0:T(2,128)}), f32[4,2,128]{2,1,0:T(2,128)S(1)}, u32[]{:S(2)}, u32[]{:S(2)}) %all-to-all-start) | async-done | bytes 4128 | tf_op jit(solution)/shard_map/all_to_all | solution.py:302
  25.0 0.0 copy-start.6
  25.0 0.6 copy-done.6
  25.6 1.3 inner.1
  26.9 12.5 %all-to-all-start.1 = ((f32[8,2,128]{2,1,0:T(2,128)}), f32[8,2,128]{2,1,0:T(2,128)S(1)}, u32[]{:S(2)}, u32[]{:S(2)}) async-start(f32[8,2,128]{2,1,0:T(2,128)} %inner.1), calls=%async_computation.1 | async-start | bytes 16384 | tf_op jit(solution)/shard_map/all_to_all | solution.py:312
  39.4 0.6 pad_add_fusion.place_ref
  40.0 6.0 %all-to-all-done.1.outer_ref = f32[8,2,128]{2,1,0:T(2,128)S(1)} async-done(((f32[8,2,128]{2,1,0:T(2,128)}), f32[8,2,128]{2,1,0:T(2,128)S(1)}, u32[]{:S(2)}, u32[]{:S(2)}) %all-to-all-start.1) | async-done | bytes 8224 | tf_op jit(solution)/shard_map/all_to_all | solution.py:312
  46.0 0.0 copy-start.7
  46.0 0.6 copy-done.7
  46.5 1.9 branch.1
  48.4 11.5 %all-to-all-start.2 = ((bf16[8,64,128]{2,1,0:T(8,128)(2,1)}), bf16[8,64,128]{2,1,0:T(8,128)(2,1)S(1)}, u32[]{:S(2)}, u32[]{:S(2)}) async-start(bf16[8,64,128]{2,1,0:T(8,128)(2,1)} %branch.1), calls=%async_computation.2 | async-start | bytes 262144 | tf_op jit(solution)/shard_map/all_to_all | solution.py:326
  59.9 0.0 all-gather.5.cloned.1.call-start
  59.9 13.1 %all-to-all-done.2.branch_ref = bf16[8,64,128]{2,1,0:T(8,128)(2,1)S(1)} async-done(((bf16[8,64,128]{2,1,0:T(8,128)(2,1)}), bf16[8,64,128]{2,1,0:T(8,128)(2,1)S(1)}, u32[]{:S(2)}, u32[]{:S(2)}) %all-to-all-start.2) | async-done | bytes 131104 | tf_op jit(solution)/shard_map/all_to_all | solution.py:326
  73.1 0.0 all-gather.3.cloned.1.call-done.weight_ref
  73.1 0.7 copy-done.4
  73.7 4.4 %project.1 = (f32[32,2048]{1,0:T(8,128)}, bf16[32,2048]{1,0:T(8,128)(2,1)}) custom-call(s32[1]{0:T(128)} %bitcast.side_ref, bf16[8,64,128]{2,1,0:T(8,128)(2,1)} %copy-done.4, bf16[1024,2048]{1,0:T(8,128)(2,1)} %all-gather.3.cloned.1.call-done.weight_ref), custom_call_target="tpu_custom_call" | custom-call | tf_op jit(solution)/shard_map/project/pallas_call | solution.py:331
  78.1 2.7 %collective-permute-start.1 = (bf16[32,2048]{1,0:T(8,128)(2,1)}, bf16[32,2048]{1,0:T(8,128)(2,1)S(1)}, u32[]{:S(2)}, u32[]{:S(2)}) collective-permute-start(bf16[32,2048]{1,0:T(8,128)(2,1)} %get-tuple-element.21), channel_id=1, source_target_pairs={{0,2},{1,3},{2,0},{3,1},{4,6},{5,7},{6,4},{7,5},{8,10},{9,11},{10,... | collective-permute-start | bytes 393224 | tf_op jit(solution)/shard_map/ppermute | solution.py:38
  80.9 0.0 copy-done
  80.9 0.1 constant_dynamic-slice_fusion
  80.9 0.7 copy.19.routes_ref
  81.6 1.7 slots.1
  83.3 0.9 collective-permute-done.1.got_ref
  84.2 0.7 copy-done.5
  84.8 2.3 dispatch.1
  87.2 24.3 %all_to_all.30 = bf16[32,24,256]{2,1,0:T(8,128)(2,1)S(1)} all-to-all(bf16[32,24,256]{2,1,0:T(8,128)(2,1)} %bitcast.29), channel_id=1, replica_groups=mesh['sp'=32,'tp'=16] {'sp'}, dimensions={0} | all-to-all | bytes 786432 | tf_op jit(solution)/shard_map/all_to_all | solution.py:359
  111.4 0.9 reshape.24
  112.3 0.0 all-gather.5.cloned.1.call-update
  112.4 3.5 %all-to-all-start.4 = ((bf16[8,256,128]{2,1,0:T(8,128)(2,1)}), bf16[8,256,128]{2,1,0:T(8,128)(2,1)S(1)}, u32[]{:S(2)}, u32[]{:S(2)}) async-start(bf16[8,256,128]{2,1,0:T(8,128)(2,1)} %bitcast.9), calls=%async_computation.4 | async-start | bytes 1048576 | tf_op jit(solution)/shard_map/all_to_all | solution.py:367
  115.9 0.0 reduce-scatter.2.cloned.1.call-start
  115.9 0.0 copy-done.2
  115.9 5.1 %collective-permute-start.2 = (bf16[2048,128]{1,0:T(8,128)(2,1)S(1)}, bf16[2048,128]{1,0:T(8,128)(2,1)S(1)}, u32[]{:S(2)}, u32[]{:S(2)}) collective-permute-start(bf16[2048,128]{1,0:T(8,128)(2,1)S(1)} %bitcast.24), channel_id=1, source_target_pairs={{0,1},{1,0},{2,3},{3,2},{4,5},{5,4},{6,7},{7,6},{8,9},{9,8},{10,11... | collective-permute-start | bytes 1572872 | tf_op jit(solution)/shard_map/ppermute | solution.py:43
  121.0 0.0 copy-done.3
  121.0 1.9 collective-permute-start.3
  123.0 8.7 %all-to-all-done.4 = bf16[8,256,128]{2,1,0:T(8,128)(2,1)S(1)} async-done(((bf16[8,256,128]{2,1,0:T(8,128)(2,1)}), bf16[8,256,128]{2,1,0:T(8,128)(2,1)S(1)}, u32[]{:S(2)}, u32[]{:S(2)}) %all-to-all-start.4) | async-done | bytes 524320 | tf_op jit(solution)/shard_map/all_to_all | solution.py:367
  131.7 9.7 %collective-permute-start.4 = (bf16[8,256,128]{2,1,0:T(8,128)(2,1)S(1)}, bf16[8,256,128]{2,1,0:T(8,128)(2,1)S(1)}, u32[]{:S(2)}, u32[]{:S(2)}) collective-permute-start(bf16[8,256,128]{2,1,0:T(8,128)(2,1)S(1)} %all-to-all-done.4), channel_id=1, source_target_pairs={{0,1},{1,0},{2,3},{3,2},{4,5},{5,4},{6,7},{7,6},{8,9},{9,8},{10,11... | collective-permute-start | bytes 1572872 | tf_op jit(solution)/shard_map/ppermute | solution.py:43
  141.4 0.0 collective-permute-done.2
  141.5 1.3 maximum_select_fusion.gate_ref
  142.8 0.0 collective-permute-done.3
  142.8 1.4 maximum_select_fusion.1.up_ref
  144.2 0.0 collective-permute-done.4
  144.2 0.2 maximum_select_fusion.2
  144.4 1.1 copy.17
  145.5 1.3 copy.22
  146.8 13.8 %all-gather.5.cloned.1.call-done.rows_ref = bf16[768,2048]{1,0:T(8,128)(2,1)} async-done(((bf16[96,2048]{1,0:T(8,128)(2,1)}), bf16[768,2048]{1,0:T(8,128)(2,1)}) %all-gather.5.cloned.1.call-update) | async-done | bytes 3145744 | tf_op jit(solution)/shard_map/all_gather | solution.py:362
  160.6 7.2 %experts.1 = bf16[768,2048]{1,0:T(8,128)(2,1)} custom-call(bf16[768,2048]{1,0:T(8,128)(2,1)} %all-gather.5.cloned.1.call-done.rows_ref, bf16[2048,256]{1,0:T(8,128)(2,1)} %maximum_select_fusion.gate_ref, bf16[2048,256]{1,0:T(8,128)(2,1)} %maximum_select_fusion.1.up_ref, bf16[256,2048]{1,0:T(8,128)(2,1)} %bitcast.20), custom_call_target="tpu_custom_call" | custom-call | tf_op jit(solution)/shard_map/experts/pallas_call | solution.py:377
  167.7 0.0 reduce-scatter.2.cloned.1.call-update
  167.8 41.1 %reduce-scatter.2.cloned.1.call-done = bf16[96,2048]{1,0:T(8,128)(2,1)} async-done(((bf16[768,2048]{1,0:T(8,128)(2,1)}), bf16[96,2048]{1,0:T(8,128)(2,1)}) %reduce-scatter.2.cloned.1.call-update) | async-done | bytes 393232 | tf_op jit(solution)/shard_map/reduce_scatter | solution.py:390
  208.9 1.9 reshape.27
  210.8 10.1 %all-to-all-start.5 = ((bf16[32,24,256]{2,1,0:T(8,128)(2,1)}), bf16[32,24,256]{2,1,0:T(8,128)(2,1)S(1)}, u32[]{:S(2)}, u32[]{:S(2)}) async-start(bf16[32,24,256]{2,1,0:T(8,128)(2,1)} %reshape.27), calls=%async_computation.6 | async-start | bytes 786432 | tf_op jit(solution)/shard_map/all_to_all | solution.py:394
  220.9 0.0 copy-done.8
  220.9 0.7 copy.18.weight_ref
  221.6 10.9 %all-to-all-done.5 = bf16[32,24,256]{2,1,0:T(8,128)(2,1)S(1)} async-done(((bf16[32,24,256]{2,1,0:T(8,128)(2,1)}), bf16[32,24,256]{2,1,0:T(8,128)(2,1)S(1)}, u32[]{:S(2)}, u32[]{:S(2)}) %all-to-all-start.5) | async-done | bytes 393248 | tf_op jit(solution)/shard_map/all_to_all | solution.py:394
  232.5 0.7 copy-done.1
  233.2 2.4 combine.1
  (6 shorter events, 0.0 us)
Async XLA Ops:
  6.5 74.3 %copy-start = (s32[512,2]{0,1:T(2,128)S(1)}, s32[512,2]{0,1:T(2,128)}, u32[]{:S(2)}) copy-start(s32[512,2]{0,1:T(2,128)} %param.25) | copy-start | bytes 12292
  6.5 66.5 %all-gather.3.cloned.1.call-start = ((), (), s32[]{:S(2)}) async-start(), calls=%async_computation.7 | async-start | bytes 4718592 | tf_op jit(solution)/shard_map/all_gather | solution.py:259
  7.9 4.6 %collective-permute-start = (bf16[3,128]{1,0:T(4,128)(2,1)S(1)}, bf16[3,128]{1,0:T(4,128)(2,1)S(1)}, u32[]{:S(2)}, u32[]{:S(2)}) collective-permute-start(bf16[3,128]{1,0:T(4,128)(2,1)S(1)} %slice.3), channel_id=1, source_target_pairs={{0,16},{16,32},{32,48},{48,64},{64,80},{80,96},{96,112},{112,128},... | collective-permute-start | bytes 2312 | tf_op jit(solution)/shard_map/ppermute | solution.py:25
  12.6 0.5 copy-start.9
  16.3 8.7 %all-to-all-start = ((f32[4,2,128]{2,1,0:T(2,128)}), f32[4,2,128]{2,1,0:T(2,128)S(1)}, u32[]{:S(2)}, u32[]{:S(2)}) async-start(f32[4,2,128]{2,1,0:T(2,128)} %get-tuple-element.17), calls=%async_computation | async-start | bytes 8192 | tf_op jit(solution)/shard_map/all_to_all | solution.py:302
  25.0 0.6 copy-start.6
  26.9 19.1 %all-to-all-start.1 = ((f32[8,2,128]{2,1,0:T(2,128)}), f32[8,2,128]{2,1,0:T(2,128)S(1)}, u32[]{:S(2)}, u32[]{:S(2)}) async-start(f32[8,2,128]{2,1,0:T(2,128)} %inner.1), calls=%async_computation.1 | async-start | bytes 16384 | tf_op jit(solution)/shard_map/all_to_all | solution.py:312
  46.0 0.6 copy-start.7
  48.4 24.6 %all-to-all-start.2 = ((bf16[8,64,128]{2,1,0:T(8,128)(2,1)}), bf16[8,64,128]{2,1,0:T(8,128)(2,1)S(1)}, u32[]{:S(2)}, u32[]{:S(2)}) async-start(bf16[8,64,128]{2,1,0:T(8,128)(2,1)} %branch.1), calls=%async_computation.2 | async-start | bytes 262144 | tf_op jit(solution)/shard_map/all_to_all | solution.py:326
  59.9 100.6 %all-gather.5.cloned.1.call-start = ((), (), s32[]{:S(2)}) async-start(), calls=%async_computation.8 | async-start | bytes 3538944 | tf_op jit(solution)/shard_map/all_gather | solution.py:362
  73.1 0.7 copy-start.4
  78.1 37.8 %copy-start.2 = (bf16[1,2048,128]{2,1,0:T(8,128)(2,1)S(1)}, bf16[1,2048,128]{2,1,0:T(8,128)(2,1)}, u32[]{:S(2)}) copy-start(bf16[1,2048,128]{2,1,0:T(8,128)(2,1)} %param.27) | copy-start | bytes 1572868
  78.1 42.9 %copy-start.3 = (bf16[1,2048,128]{2,1,0:T(8,128)(2,1)S(1)}, bf16[1,2048,128]{2,1,0:T(8,128)(2,1)}, u32[]{:S(2)}) copy-start(bf16[1,2048,128]{2,1,0:T(8,128)(2,1)} %param.28) | copy-start | bytes 1572868
  78.1 6.0 %collective-permute-start.1 = (bf16[32,2048]{1,0:T(8,128)(2,1)}, bf16[32,2048]{1,0:T(8,128)(2,1)S(1)}, u32[]{:S(2)}, u32[]{:S(2)}) collective-permute-start(bf16[32,2048]{1,0:T(8,128)(2,1)} %get-tuple-element.21), channel_id=1, source_target_pairs={{0,2},{1,3},{2,0},{3,1},{4,6},{5,7},{6,4},{7,5},{8,10},{9,11},{10,... | collective-permute-start | bytes 393224 | tf_op jit(solution)/shard_map/ppermute | solution.py:38
  84.2 0.7 copy-start.5
  112.4 19.3 %all-to-all-start.4 = ((bf16[8,256,128]{2,1,0:T(8,128)(2,1)}), bf16[8,256,128]{2,1,0:T(8,128)(2,1)S(1)}, u32[]{:S(2)}, u32[]{:S(2)}) async-start(bf16[8,256,128]{2,1,0:T(8,128)(2,1)} %bitcast.9), calls=%async_computation.4 | async-start | bytes 1048576 | tf_op jit(solution)/shard_map/all_to_all | solution.py:367
  115.9 93.0 %reduce-scatter.2.cloned.1.call-start = ((), (), s32[]{:S(2)}) async-start(), calls=%async_computation.9 | async-start | bytes 3538944 | tf_op jit(solution)/shard_map/reduce_scatter | solution.py:390
  115.9 25.5 %collective-permute-start.2 = (bf16[2048,128]{1,0:T(8,128)(2,1)S(1)}, bf16[2048,128]{1,0:T(8,128)(2,1)S(1)}, u32[]{:S(2)}, u32[]{:S(2)}) collective-permute-start(bf16[2048,128]{1,0:T(8,128)(2,1)S(1)} %bitcast.24), channel_id=1, source_target_pairs={{0,1},{1,0},{2,3},{3,2},{4,5},{5,4},{6,7},{7,6},{8,9},{9,8},{10,11... | collective-permute-start | bytes 1572872 | tf_op jit(solution)/shard_map/ppermute | solution.py:43
  121.0 21.7 %collective-permute-start.3 = (bf16[2048,128]{1,0:T(8,128)(2,1)S(1)}, bf16[2048,128]{1,0:T(8,128)(2,1)S(1)}, u32[]{:S(2)}, u32[]{:S(2)}) collective-permute-start(bf16[2048,128]{1,0:T(8,128)(2,1)S(1)} %bitcast.26), channel_id=1, source_target_pairs={{0,1},{1,0},{2,3},{3,2},{4,5},{5,4},{6,7},{7,6},{8,9},{9,8},{10,11... | collective-permute-start | bytes 1572872 | tf_op jit(solution)/shard_map/ppermute | solution.py:43
  131.7 12.5 %collective-permute-start.4 = (bf16[8,256,128]{2,1,0:T(8,128)(2,1)S(1)}, bf16[8,256,128]{2,1,0:T(8,128)(2,1)S(1)}, u32[]{:S(2)}, u32[]{:S(2)}) collective-permute-start(bf16[8,256,128]{2,1,0:T(8,128)(2,1)S(1)} %all-to-all-done.4), channel_id=1, source_target_pairs={{0,1},{1,0},{2,3},{3,2},{4,5},{5,4},{6,7},{7,6},{8,9},{9,8},{10,11... | collective-permute-start | bytes 1572872 | tf_op jit(solution)/shard_map/ppermute | solution.py:43
  167.7 53.2 %copy-start.8 = (f32[32,2]{0,1:T(2,128)S(1)}, f32[32,2]{0,1:T(2,128)}, u32[]{:S(2)}) copy-start(f32[32,2]{0,1:T(2,128)} %param.26) | copy-start | bytes 772
  210.8 21.7 %all-to-all-start.5 = ((bf16[32,24,256]{2,1,0:T(8,128)(2,1)}), bf16[32,24,256]{2,1,0:T(8,128)(2,1)S(1)}, u32[]{:S(2)}, u32[]{:S(2)}) async-start(bf16[32,24,256]{2,1,0:T(8,128)(2,1)} %reshape.27), calls=%async_computation.6 | async-start | bytes 786432 | tf_op jit(solution)/shard_map/all_to_all | solution.py:394
  232.5 0.7 copy-start.1
Sparse Core Ops, SparseCore 0:
  9.5 58.9 all-gather.2
  112.5 48.0 all-gather.4
  167.9 40.9 reduce-scatter.1

commit v4 on v3

--- a/solution.py
+++ b/solution.py
@@ -12,7 +12,6 @@
 CORES = 2
 CAP = 3
 PIECES = 8
-INNER = 4
 GELU_SCALE = 0.7978845608028654
 
 VMEM = pl.BlockSpec(memory_space=pltpu.VMEM)
@@ -27,15 +26,6 @@
 
 def core_groups(size):
     return [[core + CORES * y for y in range(size // CORES)] for core in range(CORES)]
-
-
-def halves_of_chips(size):
-    return [[i for i in range(size) if i // CORES % 2 == side] for side in range(2)]
-
-
-def swap_neighbours(x):
-    size = lax.axis_size("tp")
-    return lax.ppermute(x, "tp", [(i, i ^ CORES) for i in range(size)])
 
 
 def swap_cores(x):
@@ -100,35 +90,19 @@
     total_ref[:, 1:2, :] = jnp.broadcast_to(whole_b[None], (total_ref.shape[0], 1, channels))
 
 
-def inner_kernel(pieces_ref, total_ref):
-    count, _, channels = pieces_ref.shape
-    whole_a, whole_b = pieces_ref[0, 0:1, :], pieces_ref[0, 1:2, :]
-    for k in range(1, count):
-        a, b = pieces_ref[k, 0:1, :], pieces_ref[k, 1:2, :]
-        whole_b = a * whole_b + b
-        whole_a = whole_a * a
-    total_ref[:, 0:1, :] = jnp.broadcast_to(whole_a[None], (total_ref.shape[0], 1, channels))
-    total_ref[:, 1:2, :] = jnp.broadcast_to(whole_b[None], (total_ref.shape[0], 1, channels))
-
-
-def branch_kernel(place_ref, outer_ref, inner_ref, state_ref, running_ref, gate_ref, out_ref):
+def branch_kernel(place_ref, pieces_ref, state_ref, running_ref, gate_ref, out_ref):
+    place = place_ref[0]
     carry = jnp.zeros((1, state_ref.shape[1]), jnp.float32)
-    for place, pieces in ((place_ref[0], outer_ref), (place_ref[1], inner_ref)):
-        for k in range(pieces.shape[0]):
-            after = pieces[k, 0:1, :] * carry + pieces[k, 1:2, :]
-            carry = jnp.where(k < place, after, carry)
+    for k in range(pieces_ref.shape[0]):
+        after = pieces_ref[k, 0:1, :] * carry + pieces_ref[k, 1:2, :]
+        carry = jnp.where(k < place, after, carry)
     length = state_ref.shape[0] // SEGMENTS
-    half = length // CORES
     for k in range(SEGMENTS):
         rows = slice(k * length, (k + 1) * length)
         state = state_ref[rows, :] + running_ref[rows, :] * carry
         g = gate_ref[rows, :].astype(jnp.float32)
         gelu = 0.5 * g * (1.0 + jnp.tanh(GELU_SCALE * (g + 0.044715 * (g * g * g))))
-        branch = (gelu * state).astype(jnp.bfloat16)
-        for core in range(CORES):
-            out_ref[k // 2 * CORES + core, k % 2 * half : (k % 2 + 1) * half, :] = branch[
-                core * half : (core + 1) * half
-            ]
+        out_ref[rows, :] = (gelu * state).astype(jnp.bfloat16)
         carry = state[length - 1 : length, :]
 
 
@@ -247,17 +221,13 @@
     here, place = lax.axis_index("tp"), lax.axis_index("sp")
     core = here % CORES
     chips = tp // CORES
-    groups, halves = core_groups(tp), halves_of_chips(tp)
-    side = here // CORES % 2
-    outer = experts // INNER
-    inner_groups = [[k * INNER + i for i in range(INNER)] for k in range(outer)]
-    outer_groups = [[k * INNER + i for k in range(outer)] for i in range(INNER)]
+    groups = core_groups(tp)
     rows_dev, width = resid.shape
     f32, bf16 = jnp.float32, jnp.bfloat16
 
     rim = shifted(recurrent_input[tokens - taps + 1 :], "sp", 1)
     projection = lax.all_gather(
-        output_projection_weight, "tp", axis=0, axis_index_groups=halves, tiled=True
+        output_projection_weight, "tp", axis=0, axis_index_groups=groups, tiled=True
     )
 
     own_routes = lax.dynamic_slice_in_dim(routes, here * rows_dev, rows_dev, 0)
@@ -277,7 +247,7 @@
         out_shape=(
             jax.ShapeDtypeStruct((tokens, channels), f32),
             jax.ShapeDtypeStruct((tokens, channels), f32),
-            jax.ShapeDtypeStruct((INNER, 2, channels), f32),
+            jax.ShapeDtypeStruct((experts, 2, channels), f32),
         ),
         in_specs=[VMEM] * 7,
         out_specs=(VMEM,) * 3,
@@ -299,38 +269,31 @@
         token_decay_boost,
     )
 
-    inner_pieces = lax.all_to_all(
-        total, "sp", 0, 0, axis_index_groups=inner_groups, tiled=True
-    )
-    total = pl.pallas_call(
-        inner_kernel,
-        out_shape=jax.ShapeDtypeStruct((outer, 2, channels), f32),
-        in_specs=[VMEM],
-        out_specs=VMEM,
-        name="inner",
-    )(inner_pieces)
-    outer_pieces = lax.all_to_all(
-        total, "sp", 0, 0, axis_index_groups=outer_groups, tiled=True
-    )
-    peers = tp // 2
+    pieces = lax.all_to_all(total, "sp", 0, 0, tiled=True)
     branch = pl.pallas_call(
         branch_kernel,
-        out_shape=jax.ShapeDtypeStruct((peers, 2 * rows_dev, channels), bf16),
-        in_specs=[SMEM] + [VMEM] * 5,
+        out_shape=jax.ShapeDtypeStruct((tokens, channels), bf16),
+        in_specs=[SMEM] + [VMEM] * 4,
         out_specs=VMEM,
         name="branch",
-    )(
-        jnp.stack([place // INNER, place % INNER]).astype(jnp.int32),
-        outer_pieces, inner_pieces, state, running, recurrent_out_gate,
-    )
-    mine = lax.all_to_all(branch, "tp", 0, 0, axis_index_groups=halves, tiled=True)
+    )(place.astype(jnp.int32)[None], pieces, state, running, recurrent_out_gate)
+    mine = lax.all_to_all(
+        branch.reshape(chips, CORES * rows_dev, channels), "tp", 0, 0,
+        axis_index_groups=groups, tiled=True,
+    )
+    down_part = lax.optimization_barrier((down_weight[0], mine))[0]
+    hidden = gate_weight.shape[2]
+    down_own = lax.all_to_all(
+        down_part.reshape(chips, CORES * hidden, -1), "tp", 0, 0,
+        axis_index_groups=groups, tiled=True,
+    )
 
     slot_count = experts * CAP
     depth = CORES * channels
     whole = lambda *shape: pl.BlockSpec(shape, lambda k: (0,) * len(shape))
     keep, send = pl.pallas_call(
         project_kernel,
-        grid=(peers // CORES,),
+        grid=(chips // CORES,),
         out_shape=(
             jax.ShapeDtypeStruct((rows_dev, width), f32),
             jax.ShapeDtypeStruct((rows_dev, width), bf16),
@@ -343,8 +306,8 @@
         out_specs=(whole(rows_dev, width),) * 2,
         scratch_shapes=[pltpu.VMEM((2 * rows_dev, width), f32)],
         name="project",
-    )(side.astype(jnp.int32)[None], mine, projection)
-    got = swap_neighbours(send)
+    )(core.astype(jnp.int32)[None], mine, projection)
+    got = swap_cores(send)
     stream, outgoing = pl.pallas_call(
         dispatch_kernel,
         out_shape=(
@@ -360,13 +323,8 @@
     arrived = arrived.reshape(slot_count, width)
 
     rows = lax.all_gather(arrived, "tp", axis=0, axis_index_groups=groups, tiled=True)
-    arrived, down_part, gate_own, up_own = lax.optimization_barrier(
-        (arrived, down_weight[0], gate_weight[0], up_weight[0])
-    )
-    hidden = gate_own.shape[1]
-    down_own = lax.all_to_all(
-        down_part.reshape(chips, CORES * hidden, -1), "tp", 0, 0,
-        axis_index_groups=groups, tiled=True,
+    arrived, down_own, gate_own, up_own = lax.optimization_barrier(
+        (arrived, down_own, gate_weight[0], up_weight[0])
     )
     gate = natural(gate_own, swap_cores(gate_own), core, 1)
     upward = natural(up_own, swap_cores(up_own), core, 1)

time: 246 us -> 246 us (level)
  blocking collectives: 24.3 us -> 45.2 us
  starting transfers between devices: 65.6 us -> 50.8 us
  waiting for transfers between devices: 100 us -> 96.8 us
    all_to_all x0 -> x1, blocking collectives: none -> 20.9 us  [layer(): lax.all_to_all(down_part.reshape(chips, CORES * hidden, -1), 'tp', 0, 0,...]
    all_gather x1, waiting for transfers between devices: 0.01 us -> 16.6 us  [layer(): lax.all_gather(output_projection_weight, 'tp', axis=0, axis_index_groups=...]
    all_to_all x4 -> x2, waiting for transfers between devices: 32 us -> 18.1 us  [the longest x1 9.41 us: layer(): lax.all_to_all(branch.reshape(chips, CORES * rows_dev, channels), 'tp', 0...]
    all_to_all x4 -> x2, starting transfers between devices: 32.1 us -> 21 us  [the longest x1 14.2 us: layer(): pieces = lax.all_to_all(total, 'sp', 0, 0, tiled=True)]
    all_gather x1, waiting for transfers between devices: 13.8 us -> 9.61 us  [layer(): lax.all_gather(arrived, 'tp', axis=0, axis_index_groups=groups, tiled=True)]
    ppermute x1 -> x0, starting transfers between devices: 2.7 us -> none  [swap_neighbours(): return lax.ppermute(x, 'tp', [(i, i ^ CORES) for i in range(size)])]
    pallas_call x3 -> x2, Pallas kernels: 7.59 us -> 6.33 us  [the longest x1 4.42 us: layer(): pl.pallas_call(project_kernel, grid=(chips // CORES,), out_shape=(jax.Sha...]
    ppermute x3 -> x4, starting transfers between devices: 16.8 us -> 15.7 us  [swap_cores(): return lax.ppermute(x, 'tp', [(i, i ^ 1) for i in range(size)])]
  transfers between devices with their start and end apart: 13 -> 11, of which waited for: 9 -> 7; matrix products, arithmetic and copies ran while one was open for 3% -> 3% of each run, Pallas kernels for 3% -> 3%
where the time goes in v4:
time: 246 us; the launch traced here: 242 us
  waiting for transfers between devices  96.8 us (39%)
  starting transfers between devices  50.8 us (21%)
  blocking collectives  45.2 us (18%)
  Pallas kernels  23.1 us (9%)
  between operations  13.3 us (5%)
  local copies, waits for them, and re-layouts  10 us (4%)
  other arithmetic  2.94 us (1%)
    reduce_scatter x1, waiting for transfers between devices, layer(): lax.psum_scatter(summed, 'tp', scatter_dimension=0, axis_index_groups=gro...  40.2 us
    all_to_all x1, blocking collectives, layer(): arrived = lax.all_to_all(outgoing.reshape(packed), 'sp', 0, 0, tiled=True)  24.3 us
    all_to_all x1, blocking collectives, layer(): lax.all_to_all(down_part.reshape(chips, CORES * hidden, -1), 'tp', 0, 0,...  20.9 us
    all_gather x1, waiting for transfers between devices, layer(): lax.all_gather(output_projection_weight, 'tp', axis=0, axis_index_groups=...  16.6 us
    ppermute x4, starting transfers between devices, swap_cores(): return lax.ppermute(x, 'tp', [(i, i ^ 1) for i in range(size)])  15.7 us
    all_to_all x1, starting transfers between devices, layer(): pieces = lax.all_to_all(total, 'sp', 0, 0, tiled=True)  14.2 us
    all_to_all x1, waiting for transfers between devices, layer(): returned = lax.all_to_all(result.reshape(packed), 'sp', 0, 0, tiled=True)  10.9 us
    all_to_all x1, starting transfers between devices, layer(): returned = lax.all_to_all(result.reshape(packed), 'sp', 0, 0, tiled=True)  10.1 us
  transfers between devices with their start and end apart: 11, of which 7 were waited for; matrix products, arithmetic and copies ran while one was open for 3% of the time, Pallas kernels for 3%

profile of v4, /device:TPU:1, one launch (start us, length us, event | category | flops | bytes accessed | tf_op | source)
XLA Modules:
  0.0 242.2 jit_solution(1414138817666817708)
XLA Ops:
  6.5 0.0 copy-start
  6.5 0.0 all-gather.3.cloned.1.call-start
  6.5 0.7 all-gather.3.cloned.1.call-update
  7.3 0.7 slice.3
  7.9 3.9 %collective-permute-start = (bf16[3,128]{1,0:T(4,128)(2,1)S(1)}, bf16[3,128]{1,0:T(4,128)(2,1)S(1)}, u32[]{:S(2)}, u32[]{:S(2)}) collective-permute-start(bf16[3,128]{1,0:T(4,128)(2,1)S(1)} %slice.3), channel_id=1, source_target_pairs={{0,16},{16,32},{32,48},{48,64},{64,80},{80,96},{96,112},{112,128},... | collective-permute-start | bytes 2312 | tf_op jit(solution)/shard_map/ppermute | solution.py:24
  11.9 0.7 collective-permute-done.rim_ref
  12.6 0.0 copy-start.9
  12.6 0.6 copy-done.9
  13.2 3.2 %recurrence.1 = (f32[512,128]{1,0:T(8,128)}, f32[512,128]{1,0:T(8,128)}, f32[32,2,128]{2,1,0:T(2,128)}) custom-call(bf16[512,128]{1,0:T(8,128)(2,1)} %x_ref.1, bf16[3,128]{1,0:T(4,128)(2,1)} %copy-done.9, f32[4,128]{1,0:T(4,128)} %filter_ref.1, bf16[2,64,64]{2,1,0:T(8,128)(2,1)} %recur_ref.1, bf16[2,64,64]{2,1,0:T(8,128)(2,1)} %input_ref.1, ...), custom_call_target="tpu_custom_call" | custom-call | flops 1000000000 | bytes 1048576 | tf_op jit(solution)/shard_map/recurrence/pallas_call | solution.py:245
  16.4 14.2 %all-to-all-start = ((f32[32,2,128]{2,1,0:T(2,128)}), f32[32,2,128]{2,1,0:T(2,128)S(1)}, u32[]{:S(2)}, u32[]{:S(2)}) async-start(f32[32,2,128]{2,1,0:T(2,128)} %get-tuple-element.18), calls=%async_computation | async-start | bytes 65536 | tf_op jit(solution)/shard_map/all_to_all | solution.py:272
  30.6 8.7 %all-to-all-done.pieces_ref = f32[32,2,128]{2,1,0:T(2,128)S(1)} async-done(((f32[32,2,128]{2,1,0:T(2,128)}), f32[32,2,128]{2,1,0:T(2,128)S(1)}, u32[]{:S(2)}, u32[]{:S(2)}) %all-to-all-start) | async-done | bytes 32800 | tf_op jit(solution)/shard_map/all_to_all | solution.py:272
  39.3 0.0 copy-start.6
  39.3 0.6 copy-done.6
  39.9 1.9 branch.1
  41.8 6.8 %all-to-all-start.1 = ((bf16[8,64,128]{2,1,0:T(8,128)(2,1)}), bf16[8,64,128]{2,1,0:T(8,128)(2,1)S(1)}, u32[]{:S(2)}, u32[]{:S(2)}) async-start(bf16[8,64,128]{2,1,0:T(8,128)(2,1)} %bitcast.30), calls=%async_computation.1 | async-start | bytes 262144 | tf_op jit(solution)/shard_map/all_to_all | solution.py:280
  48.6 0.0 all-gather.5.cloned.1.call-start
  48.7 9.4 %all-to-all-done.1.branch_ref = bf16[8,64,128]{2,1,0:T(8,128)(2,1)S(1)} async-done(((bf16[8,64,128]{2,1,0:T(8,128)(2,1)}), bf16[8,64,128]{2,1,0:T(8,128)(2,1)S(1)}, u32[]{:S(2)}, u32[]{:S(2)}) %all-to-all-start.1) | async-done | bytes 131104 | tf_op jit(solution)/shard_map/all_to_all | solution.py:280
  58.1 0.0 copy-start.4
  58.1 16.6 %all-gather.3.cloned.1.call-done.weight_ref = bf16[1024,2048]{1,0:T(8,128)(2,1)} async-done(((bf16[128,2048]{1,0:T(8,128)(2,1)}), bf16[1024,2048]{1,0:T(8,128)(2,1)}) %all-gather.3.cloned.1.call-update) | async-done | bytes 4194320 | tf_op jit(solution)/shard_map/all_gather | solution.py:229
  74.6 0.0 copy-done.4
  74.6 4.4 %project.1 = (f32[32,2048]{1,0:T(8,128)}, bf16[32,2048]{1,0:T(8,128)(2,1)}) custom-call(s32[1]{0:T(128)} %bitcast.side_ref, bf16[8,64,128]{2,1,0:T(8,128)(2,1)} %copy-done.4, bf16[1024,2048]{1,0:T(8,128)(2,1)} %all-gather.3.cloned.1.call-done.weight_ref), custom_call_target="tpu_custom_call" | custom-call | tf_op jit(solution)/shard_map/project/pallas_call | solution.py:294
  79.1 0.0 copy-start.5
  79.1 0.0 copy-start.2
  79.1 0.0 copy-start.3
  79.1 2.9 %collective-permute-start.1 = (bf16[32,2048]{1,0:T(8,128)(2,1)}, bf16[32,2048]{1,0:T(8,128)(2,1)S(1)}, u32[]{:S(2)}, u32[]{:S(2)}) collective-permute-start(bf16[32,2048]{1,0:T(8,128)(2,1)} %get-tuple-element.22), channel_id=1, source_target_pairs={{0,1},{1,0},{2,3},{3,2},{4,5},{5,4},{6,7},{7,6},{8,9},{9,8},{10,11... | collective-permute-start | bytes 393224 | tf_op jit(solution)/shard_map/ppermute | solution.py:33
  82.0 0.0 copy-done
  82.0 0.1 constant_dynamic-slice_fusion
  82.0 0.7 copy.19.routes_ref
  82.7 1.7 slots.1
  84.4 0.0 collective-permute-done.1.got_ref
  84.4 0.0 copy-start.7
  84.4 0.7 copy-done.7
  85.1 2.3 dispatch.1
  87.4 24.3 %all_to_all.25 = bf16[32,24,256]{2,1,0:T(8,128)(2,1)S(1)} all-to-all(bf16[32,24,256]{2,1,0:T(8,128)(2,1)} %bitcast.31), channel_id=1, replica_groups=mesh['sp'=32,'tp'=16] {'sp'}, dimensions={0} | all-to-all | bytes 786432 | tf_op jit(solution)/shard_map/all_to_all | solution.py:322
  111.7 0.9 reshape.28
  112.6 0.0 all-gather.5.cloned.1.call-update
  112.7 0.0 reduce-scatter.2.cloned.1.call-start
  112.7 0.0 copy-done.5
  112.7 20.9 %all_to_all.26 = bf16[8,256,128]{2,1,0:T(8,128)(2,1)S(1)} all-to-all(bf16[8,256,128]{2,1,0:T(8,128)(2,1)S(1)} %bitcast.29), channel_id=1, replica_groups={{0,2,4,6,8,10,12,14},{1,3,5,7,9,11,13,15},{16,18,20,22,24,26,28,30},{17..., dimensions={0} | all-to-all | bytes 1048576 | tf_op jit(solution)/shard_map/all_to_all | solution.py:286
  133.7 8.5 %collective-permute-start.4 = (bf16[8,256,128]{2,1,0:T(8,128)(2,1)S(1)}, bf16[8,256,128]{2,1,0:T(8,128)(2,1)S(1)}, u32[]{:S(2)}, u32[]{:S(2)}) collective-permute-start(bf16[8,256,128]{2,1,0:T(8,128)(2,1)S(1)} %all_to_all.26), channel_id=1, source_target_pairs={{0,1},{1,0},{2,3},{3,2},{4,5},{5,4},{6,7},{7,6},{8,9},{9,8},{10,11... | collective-permute-start | bytes 1572872 | tf_op jit(solution)/shard_map/ppermute | solution.py:33
  142.1 0.0 copy-done.2
  142.1 1.9 collective-permute-start.2
  144.1 0.0 copy-done.3
  144.1 2.4 collective-permute-start.3
  146.5 0.0 collective-permute-done.4
  146.5 0.2 maximum_select_fusion.2
  146.7 1.1 copy.17
  147.8 1.3 copy.22
  149.1 0.0 collective-permute-done.2
  149.1 1.3 maximum_select_fusion.gate_ref
  150.4 0.0 collective-permute-done.3
  150.4 1.4 maximum_select_fusion.1.up_ref
  151.8 9.6 %all-gather.5.cloned.1.call-done.rows_ref = bf16[768,2048]{1,0:T(8,128)(2,1)} async-done(((bf16[96,2048]{1,0:T(8,128)(2,1)}), bf16[768,2048]{1,0:T(8,128)(2,1)}) %all-gather.5.cloned.1.call-update) | async-done | bytes 3145744 | tf_op jit(solution)/shard_map/all_gather | solution.py:325
  161.5 7.2 %experts.1 = bf16[768,2048]{1,0:T(8,128)(2,1)} custom-call(bf16[768,2048]{1,0:T(8,128)(2,1)} %all-gather.5.cloned.1.call-done.rows_ref, bf16[2048,256]{1,0:T(8,128)(2,1)} %maximum_select_fusion.gate_ref, bf16[2048,256]{1,0:T(8,128)(2,1)} %maximum_select_fusion.1.up_ref, bf16[256,2048]{1,0:T(8,128)(2,1)} %bitcast.20), custom_call_target="tpu_custom_call" | custom-call | tf_op jit(solution)/shard_map/experts/pallas_call | solution.py:335
  168.6 0.0 copy-start.8
  168.6 0.0 reduce-scatter.2.cloned.1.call-update
  168.7 40.2 %reduce-scatter.2.cloned.1.call-done = bf16[96,2048]{1,0:T(8,128)(2,1)} async-done(((bf16[768,2048]{1,0:T(8,128)(2,1)}), bf16[96,2048]{1,0:T(8,128)(2,1)}) %reduce-scatter.2.cloned.1.call-update) | async-done | bytes 393232 | tf_op jit(solution)/shard_map/reduce_scatter | solution.py:348
  208.9 1.9 reshape.31
  210.8 10.1 %all-to-all-start.4 = ((bf16[32,24,256]{2,1,0:T(8,128)(2,1)}), bf16[32,24,256]{2,1,0:T(8,128)(2,1)S(1)}, u32[]{:S(2)}, u32[]{:S(2)}) async-start(bf16[32,24,256]{2,1,0:T(8,128)(2,1)} %reshape.31), calls=%async_computation.5 | async-start | bytes 786432 | tf_op jit(solution)/shard_map/all_to_all | solution.py:352
  220.9 0.0 copy-done.8
  221.0 0.7 copy.18.weight_ref
  221.6 10.9 %all-to-all-done.4 = bf16[32,24,256]{2,1,0:T(8,128)(2,1)S(1)} async-done(((bf16[32,24,256]{2,1,0:T(8,128)(2,1)}), bf16[32,24,256]{2,1,0:T(8,128)(2,1)S(1)}, u32[]{:S(2)}, u32[]{:S(2)}) %all-to-all-start.4) | async-done | bytes 393248 | tf_op jit(solution)/shard_map/all_to_all | solution.py:352
  232.5 0.8 copy-done.1
  233.3 2.4 combine.1
  (1 shorter events, 0.0 us)
Async XLA Ops:
  6.5 75.4 %copy-start = (s32[512,2]{0,1:T(2,128)S(1)}, s32[512,2]{0,1:T(2,128)}, u32[]{:S(2)}) copy-start(s32[512,2]{0,1:T(2,128)} %param.25) | copy-start | bytes 12292
  6.5 68.1 %all-gather.3.cloned.1.call-start = ((), (), s32[]{:S(2)}) async-start(), calls=%async_computation.6 | async-start | bytes 4718592 | tf_op jit(solution)/shard_map/all_gather | solution.py:229
  7.9 4.6 %collective-permute-start = (bf16[3,128]{1,0:T(4,128)(2,1)S(1)}, bf16[3,128]{1,0:T(4,128)(2,1)S(1)}, u32[]{:S(2)}, u32[]{:S(2)}) collective-permute-start(bf16[3,128]{1,0:T(4,128)(2,1)S(1)} %slice.3), channel_id=1, source_target_pairs={{0,16},{16,32},{32,48},{48,64},{64,80},{80,96},{96,112},{112,128},... | collective-permute-start | bytes 2312 | tf_op jit(solution)/shard_map/ppermute | solution.py:24
  12.6 0.6 copy-start.9
  16.4 22.9 %all-to-all-start = ((f32[32,2,128]{2,1,0:T(2,128)}), f32[32,2,128]{2,1,0:T(2,128)S(1)}, u32[]{:S(2)}, u32[]{:S(2)}) async-start(f32[32,2,128]{2,1,0:T(2,128)} %get-tuple-element.18), calls=%async_computation | async-start | bytes 65536 | tf_op jit(solution)/shard_map/all_to_all | solution.py:272
  39.3 0.6 copy-start.6
  41.8 16.3 %all-to-all-start.1 = ((bf16[8,64,128]{2,1,0:T(8,128)(2,1)}), bf16[8,64,128]{2,1,0:T(8,128)(2,1)S(1)}, u32[]{:S(2)}, u32[]{:S(2)}) async-start(bf16[8,64,128]{2,1,0:T(8,128)(2,1)} %bitcast.30), calls=%async_computation.1 | async-start | bytes 262144 | tf_op jit(solution)/shard_map/all_to_all | solution.py:280
  48.6 112.9 %all-gather.5.cloned.1.call-start = ((), (), s32[]{:S(2)}) async-start(), calls=%async_computation.7 | async-start | bytes 3538944 | tf_op jit(solution)/shard_map/all_gather | solution.py:325
  58.1 16.6 %copy-start.4 = (bf16[8,64,128]{2,1,0:T(8,128)(2,1)}, bf16[8,64,128]{2,1,0:T(8,128)(2,1)S(1)}, u32[]{:S(2)}) copy-start(bf16[8,64,128]{2,1,0:T(8,128)(2,1)S(1)} %all-to-all-done.1.branch_ref) | copy-start | bytes 393220
  79.1 33.7 %copy-start.5 = (bf16[1,2048,128]{2,1,0:T(8,128)(2,1)S(1)}, bf16[1,2048,128]{2,1,0:T(8,128)(2,1)}, u32[]{:S(2)}) copy-start(bf16[1,2048,128]{2,1,0:T(8,128)(2,1)} %param.29) | copy-start | bytes 1572868
  79.1 63.1 %copy-start.2 = (bf16[1,2048,128]{2,1,0:T(8,128)(2,1)S(1)}, bf16[1,2048,128]{2,1,0:T(8,128)(2,1)}, u32[]{:S(2)}) copy-start(bf16[1,2048,128]{2,1,0:T(8,128)(2,1)} %param.27) | copy-start | bytes 1572868
  79.1 65.0 %copy-start.3 = (bf16[1,2048,128]{2,1,0:T(8,128)(2,1)S(1)}, bf16[1,2048,128]{2,1,0:T(8,128)(2,1)}, u32[]{:S(2)}) copy-start(bf16[1,2048,128]{2,1,0:T(8,128)(2,1)} %param.28) | copy-start | bytes 1572868
  79.1 5.4 %collective-permute-start.1 = (bf16[32,2048]{1,0:T(8,128)(2,1)}, bf16[32,2048]{1,0:T(8,128)(2,1)S(1)}, u32[]{:S(2)}, u32[]{:S(2)}) collective-permute-start(bf16[32,2048]{1,0:T(8,128)(2,1)} %get-tuple-element.22), channel_id=1, source_target_pairs={{0,1},{1,0},{2,3},{3,2},{4,5},{5,4},{6,7},{7,6},{8,9},{9,8},{10,11... | collective-permute-start | bytes 393224 | tf_op jit(solution)/shard_map/ppermute | solution.py:33
  84.4 0.7 copy-start.7
  112.7 96.2 %reduce-scatter.2.cloned.1.call-start = ((), (), s32[]{:S(2)}) async-start(), calls=%async_computation.8 | async-start | bytes 3538944 | tf_op jit(solution)/shard_map/reduce_scatter | solution.py:348
  133.7 12.8 %collective-permute-start.4 = (bf16[8,256,128]{2,1,0:T(8,128)(2,1)S(1)}, bf16[8,256,128]{2,1,0:T(8,128)(2,1)S(1)}, u32[]{:S(2)}, u32[]{:S(2)}) collective-permute-start(bf16[8,256,128]{2,1,0:T(8,128)(2,1)S(1)} %all_to_all.26), channel_id=1, source_target_pairs={{0,1},{1,0},{2,3},{3,2},{4,5},{5,4},{6,7},{7,6},{8,9},{9,8},{10,11... | collective-permute-start | bytes 1572872 | tf_op jit(solution)/shard_map/ppermute | solution.py:33
  142.1 6.9 %collective-permute-start.2 = (bf16[2048,128]{1,0:T(8,128)(2,1)S(1)}, bf16[2048,128]{1,0:T(8,128)(2,1)S(1)}, u32[]{:S(2)}, u32[]{:S(2)}) collective-permute-start(bf16[2048,128]{1,0:T(8,128)(2,1)S(1)} %bitcast.24), channel_id=1, source_target_pairs={{0,1},{1,0},{2,3},{3,2},{4,5},{5,4},{6,7},{7,6},{8,9},{9,8},{10,11... | collective-permute-start | bytes 1572872 | tf_op jit(solution)/shard_map/ppermute | solution.py:33
  144.1 6.3 %collective-permute-start.3 = (bf16[2048,128]{1,0:T(8,128)(2,1)S(1)}, bf16[2048,128]{1,0:T(8,128)(2,1)S(1)}, u32[]{:S(2)}, u32[]{:S(2)}) collective-permute-start(bf16[2048,128]{1,0:T(8,128)(2,1)S(1)} %bitcast.26), channel_id=1, source_target_pairs={{0,1},{1,0},{2,3},{3,2},{4,5},{5,4},{6,7},{7,6},{8,9},{9,8},{10,11... | collective-permute-start | bytes 1572872 | tf_op jit(solution)/shard_map/ppermute | solution.py:33
  168.6 52.3 %copy-start.8 = (f32[32,2]{0,1:T(2,128)S(1)}, f32[32,2]{0,1:T(2,128)}, u32[]{:S(2)}) copy-start(f32[32,2]{0,1:T(2,128)} %param.26) | copy-start | bytes 772
  210.8 21.7 %all-to-all-start.4 = ((bf16[32,24,256]{2,1,0:T(8,128)(2,1)}), bf16[32,24,256]{2,1,0:T(8,128)(2,1)S(1)}, u32[]{:S(2)}, u32[]{:S(2)}) async-start(bf16[32,24,256]{2,1,0:T(8,128)(2,1)} %reshape.31), calls=%async_computation.5 | async-start | bytes 786432 | tf_op jit(solution)/shard_map/all_to_all | solution.py:352
  232.5 0.8 copy-start.1
Sparse Core Ops, SparseCore 0:
  9.4 65.1 all-gather.2
  112.8 48.6 all-gather.4
  168.8 40.0 reduce-scatter.1

commit v5 on v4

--- a/solution.py
+++ b/solution.py
@@ -90,20 +90,23 @@
     total_ref[:, 1:2, :] = jnp.broadcast_to(whole_b[None], (total_ref.shape[0], 1, channels))
 
 
-def branch_kernel(place_ref, pieces_ref, state_ref, running_ref, gate_ref, out_ref):
-    place = place_ref[0]
+def branch_kernel(place_ref, pieces_ref, state_ref, running_ref, gate_ref, keep_ref, send_ref):
+    place, core = place_ref[0], place_ref[1]
     carry = jnp.zeros((1, state_ref.shape[1]), jnp.float32)
     for k in range(pieces_ref.shape[0]):
         after = pieces_ref[k, 0:1, :] * carry + pieces_ref[k, 1:2, :]
         carry = jnp.where(k < place, after, carry)
     length = state_ref.shape[0] // SEGMENTS
+    half = length // CORES
     for k in range(SEGMENTS):
-        rows = slice(k * length, (k + 1) * length)
-        state = state_ref[rows, :] + running_ref[rows, :] * carry
-        g = gate_ref[rows, :].astype(jnp.float32)
-        gelu = 0.5 * g * (1.0 + jnp.tanh(GELU_SCALE * (g + 0.044715 * (g * g * g))))
-        out_ref[rows, :] = (gelu * state).astype(jnp.bfloat16)
-        carry = state[length - 1 : length, :]
+        for out, side in ((keep_ref, core), (send_ref, 1 - core)):
+            rows = pl.ds(pl.multiple_of(k * length + side * half, half), half)
+            state = state_ref[rows, :] + running_ref[rows, :] * carry
+            g = gate_ref[rows, :].astype(jnp.float32)
+            gelu = 0.5 * g * (1.0 + jnp.tanh(GELU_SCALE * (g + 0.044715 * (g * g * g))))
+            out[k * half : (k + 1) * half, :] = (gelu * state).astype(jnp.bfloat16)
+        last = (k + 1) * length - 1
+        carry = running_ref[last : last + 1, :] * carry + state_ref[last : last + 1, :]
 
 
 def slots_kernel(routes_ref, column_ref, line_ref):
@@ -129,30 +132,11 @@
         )
 
 
-def project_kernel(side_ref, branch_ref, weight_ref, keep_ref, send_ref, total):
-    step = pl.program_id(0)
-    branch = jnp.concatenate([branch_ref[k] for k in range(branch_ref.shape[0])], axis=1)
-    term = jnp.dot(branch, weight_ref[...], preferred_element_type=jnp.float32)
-
-    @pl.when(step == 0)
-    def _():
-        total[...] = term
-
-    @pl.when(step > 0)
-    def _():
-        total[...] += term
-
-    @pl.when(step == pl.num_programs(0) - 1)
-    def _():
-        side, rows = side_ref[0], keep_ref.shape[0]
-        keep_ref[...] = total[pl.ds(pl.multiple_of(side * rows, rows), rows), :]
-        other = pl.ds(pl.multiple_of((1 - side) * rows, rows), rows)
-        send_ref[...] = total[other, :].astype(jnp.bfloat16)
-
-
-def dispatch_kernel(keep_ref, got_ref, resid_ref, gain_ref, line_ref, stream_ref, out_ref):
+def dispatch_kernel(parts_ref, resid_ref, gain_ref, line_ref, stream_ref, out_ref):
     rows, width = resid_ref.shape
-    projected = keep_ref[...] + got_ref[...].astype(jnp.float32)
+    projected = parts_ref[0].astype(jnp.float32)
+    for k in range(1, parts_ref.shape[0]):
+        projected = projected + parts_ref[k].astype(jnp.float32)
     stream = (resid_ref[...].astype(jnp.float32) + projected).astype(jnp.bfloat16)
     stream_ref[...] = stream
     wide = stream.astype(jnp.float32)
@@ -226,9 +210,7 @@
     f32, bf16 = jnp.float32, jnp.bfloat16
 
     rim = shifted(recurrent_input[tokens - taps + 1 :], "sp", 1)
-    projection = lax.all_gather(
-        output_projection_weight, "tp", axis=0, axis_index_groups=groups, tiled=True
-    )
+    projection_other = swap_cores(output_projection_weight)
 
     own_routes = lax.dynamic_slice_in_dim(routes, here * rows_dev, rows_dev, 0)
     column, line = pl.pallas_call(
@@ -270,61 +252,45 @@
     )
 
     pieces = lax.all_to_all(total, "sp", 0, 0, tiled=True)
-    branch = pl.pallas_call(
+    keep, send = pl.pallas_call(
         branch_kernel,
-        out_shape=jax.ShapeDtypeStruct((tokens, channels), bf16),
+        out_shape=(jax.ShapeDtypeStruct((tokens // CORES, channels), bf16),) * 2,
         in_specs=[SMEM] + [VMEM] * 4,
-        out_specs=VMEM,
+        out_specs=(VMEM,) * 2,
+        cost_estimate=pl.CostEstimate(flops=10**9, bytes_accessed=2**20, transcendentals=0),
         name="branch",
-    )(place.astype(jnp.int32)[None], pieces, state, running, recurrent_out_gate)
-    mine = lax.all_to_all(
-        branch.reshape(chips, CORES * rows_dev, channels), "tp", 0, 0,
-        axis_index_groups=groups, tiled=True,
-    )
-    down_part = lax.optimization_barrier((down_weight[0], mine))[0]
-    hidden = gate_weight.shape[2]
-    down_own = lax.all_to_all(
-        down_part.reshape(chips, CORES * hidden, -1), "tp", 0, 0,
-        axis_index_groups=groups, tiled=True,
-    )
-
+    )(jnp.stack([place, core]).astype(jnp.int32), pieces, state, running, recurrent_out_gate)
+    got = swap_cores(send)
+    both = jnp.concatenate([keep, got], axis=1)
+    projection = jnp.concatenate([output_projection_weight, projection_other], axis=0)
+    partial = jnp.dot(both, projection, preferred_element_type=f32).astype(bf16)
+    parts = lax.all_to_all(
+        partial.reshape(chips, rows_dev, width), "tp", 0, 0, axis_index_groups=groups, tiled=True
+    )
     slot_count = experts * CAP
-    depth = CORES * channels
     whole = lambda *shape: pl.BlockSpec(shape, lambda k: (0,) * len(shape))
-    keep, send = pl.pallas_call(
-        project_kernel,
-        grid=(chips // CORES,),
-        out_shape=(
-            jax.ShapeDtypeStruct((rows_dev, width), f32),
-            jax.ShapeDtypeStruct((rows_dev, width), bf16),
-        ),
-        in_specs=[
-            SMEM,
-            pl.BlockSpec((CORES, 2 * rows_dev, channels), lambda k: (k, 0, 0)),
-            pl.BlockSpec((depth, width), lambda k: (k, 0)),
-        ],
-        out_specs=(whole(rows_dev, width),) * 2,
-        scratch_shapes=[pltpu.VMEM((2 * rows_dev, width), f32)],
-        name="project",
-    )(core.astype(jnp.int32)[None], mine, projection)
-    got = swap_cores(send)
     stream, outgoing = pl.pallas_call(
         dispatch_kernel,
         out_shape=(
             jax.ShapeDtypeStruct((rows_dev, width), bf16),
             jax.ShapeDtypeStruct((slot_count * PIECES, width // PIECES), bf16),
         ),
-        in_specs=[VMEM] * 5,
+        in_specs=[VMEM] * 4,
         out_specs=(VMEM,) * 2,
         name="dispatch",
-    )(keep, got, resid, expert_norm_gain[None, :], line)
+    )(parts, resid, expert_norm_gain[None, :], line)
     packed = (experts, CAP * PIECES, width // PIECES)
     arrived = lax.all_to_all(outgoing.reshape(packed), "sp", 0, 0, tiled=True)
     arrived = arrived.reshape(slot_count, width)
 
     rows = lax.all_gather(arrived, "tp", axis=0, axis_index_groups=groups, tiled=True)
-    arrived, down_own, gate_own, up_own = lax.optimization_barrier(
-        (arrived, down_own, gate_weight[0], up_weight[0])
+    arrived, down_part, gate_own, up_own = lax.optimization_barrier(
+        (arrived, down_weight[0], gate_weight[0], up_weight[0])
+    )
+    hidden = gate_own.shape[1]
+    down_own = lax.all_to_all(
+        down_part.reshape(chips, CORES * hidden, -1), "tp", 0, 0,
+        axis_index_groups=groups, tiled=True,
     )
     gate = natural(gate_own, swap_cores(gate_own), core, 1)
     upward = natural(up_own, swap_cores(up_own), core, 1)

time: 246 us -> 244 us (level)
  blocking collectives: 45.2 us -> 17.8 us
  waiting for transfers between devices: 96.8 us -> 115 us
  starting transfers between devices: 50.8 us -> 57.9 us
  Pallas kernels: 23.1 us -> 19.1 us
    all_to_all x1 -> x2, waiting for transfers between devices: 9.41 us -> 40.6 us  [the longest x1 26.7 us: layer(): lax.all_to_all(partial.reshape(chips, rows_dev, width), 'tp', 0, 0, axis_...]
    all_to_all x1 -> x0, blocking collectives: 20.9 us -> none  [layer(): lax.all_to_all(down_part.reshape(chips, CORES * hidden, -1), 'tp', 0, 0,...]
    all_gather x1 -> x0, waiting for transfers between devices: 16.6 us -> none  [layer(): lax.all_gather(output_projection_weight, 'tp', axis=0, axis_index_groups=...]
    ppermute x4 -> x5, starting transfers between devices: 15.7 us -> 25.4 us  [swap_cores(): return lax.ppermute(x, 'tp', [(i, i ^ 1) for i in range(size)])]
    all_to_all x1, blocking collectives: 24.3 us -> 17.8 us  [layer(): arrived = lax.all_to_all(outgoing.reshape(packed), 'sp', 0, 0, tiled=True)]
    pallas_call x2 -> x1, Pallas kernels: 6.33 us -> 1.9 us  [layer(): pl.pallas_call(branch_kernel, out_shape=(jax.ShapeDtypeStruct((tokens //...]
    all_gather x1, waiting for transfers between devices: 9.61 us -> 13.3 us  [layer(): lax.all_gather(arrived, 'tp', axis=0, axis_index_groups=groups, tiled=True)]
    all_to_all x1 -> x2, starting transfers between devices: 6.83 us -> 10.3 us  [the longest x1 6.82 us: layer(): lax.all_to_all(partial.reshape(chips, rows_dev, width), 'tp', 0, 0, axis_...]
  transfers between devices with their start and end apart: 11 -> 12, of which waited for: 7 -> 8; matrix products, arithmetic and copies ran while one was open for 3% -> 3% of each run, Pallas kernels for 3% -> 3%
where the time goes in v5:
time: 244 us; the launch traced here: 240 us
  waiting for transfers between devices  115 us (47%)
  starting transfers between devices  57.9 us (24%)
  Pallas kernels  19.1 us (8%)
  blocking collectives  17.8 us (7%)
  between operations  13.6 us (6%)
  local copies, waits for them, and re-layouts  10.4 us (4%)
  other arithmetic  3.6 us (1%)
    reduce_scatter x1, waiting for transfers between devices, layer(): lax.psum_scatter(summed, 'tp', scatter_dimension=0, axis_index_groups=gro...  40.6 us
    all_to_all x1, waiting for transfers between devices, layer(): lax.all_to_all(partial.reshape(chips, rows_dev, width), 'tp', 0, 0, axis_...  26.7 us
    ppermute x5, starting transfers between devices, swap_cores(): return lax.ppermute(x, 'tp', [(i, i ^ 1) for i in range(size)])  25.4 us
    all_to_all x1, blocking collectives, layer(): arrived = lax.all_to_all(outgoing.reshape(packed), 'sp', 0, 0, tiled=True)  17.8 us
    all_to_all x1, waiting for transfers between devices, layer(): lax.all_to_all(down_part.reshape(chips, CORES * hidden, -1), 'tp', 0, 0,...  13.8 us
    all_gather x1, waiting for transfers between devices, layer(): lax.all_gather(arrived, 'tp', axis=0, axis_index_groups=groups, tiled=True)  13.3 us
    all_to_all x1, waiting for transfers between devices, layer(): returned = lax.all_to_all(result.reshape(packed), 'sp', 0, 0, tiled=True)  10.9 us
    all_to_all x1, starting transfers between devices, layer(): pieces = lax.all_to_all(total, 'sp', 0, 0, tiled=True)  10.8 us
  transfers between devices with their start and end apart: 12, of which 8 were waited for; matrix products, arithmetic and copies ran while one was open for 3% of the time, Pallas kernels for 3%

profile of v5, /device:TPU:1, one launch (start us, length us, event | category | flops | bytes accessed | tf_op | source)
XLA Modules:
  0.0 239.9 jit_solution(10213969269246702549)
XLA Ops:
  6.5 0.0 copy-start
  6.5 8.9 %collective-permute-start.2 = (bf16[128,2048]{1,0:T(8,128)(2,1)}, bf16[128,2048]{1,0:T(8,128)(2,1)S(1)}, u32[]{:S(2)}, u32[]{:S(2)}) collective-permute-start(bf16[128,2048]{1,0:T(8,128)(2,1)} %param.23), channel_id=1, source_target_pairs={{0,1},{1,0},{2,3},{3,2},{4,5},{5,4},{6,7},{7,6},{8,9},{9,8},{10,11... | collective-permute-start | bytes 1572872 | tf_op jit(solution)/shard_map/ppermute | solution.py:33
  15.4 0.7 slice.3
  16.1 1.3 collective-permute-start
  17.4 0.7 collective-permute-done.rim_ref
  18.1 0.0 copy-start.8
  18.1 0.6 copy-done.8
  18.7 3.2 %recurrence.1 = (f32[512,128]{1,0:T(8,128)}, f32[512,128]{1,0:T(8,128)}, f32[32,2,128]{2,1,0:T(2,128)}) custom-call(bf16[512,128]{1,0:T(8,128)(2,1)} %x_ref.1, bf16[3,128]{1,0:T(4,128)(2,1)} %copy-done.8, f32[4,128]{1,0:T(4,128)} %filter_ref.1, bf16[2,64,64]{2,1,0:T(8,128)(2,1)} %recur_ref.1, bf16[2,64,64]{2,1,0:T(8,128)(2,1)} %input_ref.1, ...), custom_call_target="tpu_custom_call" | custom-call | flops 1000000000 | bytes 1048576 | tf_op jit(solution)/shard_map/recurrence/pallas_call | solution.py:227
  21.9 0.0 copy-start.7
  21.9 10.8 %all-to-all-start = ((f32[32,2,128]{2,1,0:T(2,128)}), f32[32,2,128]{2,1,0:T(2,128)S(1)}, u32[]{:S(2)}, u32[]{:S(2)}) async-start(f32[32,2,128]{2,1,0:T(2,128)} %get-tuple-element.17), calls=%async_computation | async-start | bytes 65536 | tf_op jit(solution)/shard_map/all_to_all | solution.py:254
  32.7 0.7 pad_add_fusion.place_ref
  33.4 8.0 %all-to-all-done.pieces_ref = f32[32,2,128]{2,1,0:T(2,128)S(1)} async-done(((f32[32,2,128]{2,1,0:T(2,128)}), f32[32,2,128]{2,1,0:T(2,128)S(1)}, u32[]{:S(2)}, u32[]{:S(2)}) %all-to-all-start) | async-done | bytes 32800 | tf_op jit(solution)/shard_map/all_to_all | solution.py:254
  41.4 0.0 copy-start.5
  41.4 0.6 copy-done.5
  42.0 1.9 branch.1
  43.9 4.5 %collective-permute-start.1 = (bf16[256,128]{1,0:T(8,128)(2,1)}, bf16[256,128]{1,0:T(8,128)(2,1)S(1)}, u32[]{:S(2)}, u32[]{:S(2)}) collective-permute-start(bf16[256,128]{1,0:T(8,128)(2,1)} %get-tuple-element.21), channel_id=1, source_target_pairs={{0,1},{1,0},{2,3},{3,2},{4,5},{5,4},{6,7},{7,6},{8,9},{9,8},{10,11... | collective-permute-start | bytes 196616 | tf_op jit(solution)/shard_map/ppermute | solution.py:33
  48.4 1.1 collective-permute-done.1
  49.5 0.0 collective-permute-done.2
  49.5 0.0 copy-done.7
  49.5 2.3 convolution_convert_fusion
  51.8 6.8 %all-to-all-start.1 = ((bf16[8,32,2048]{2,1,0:T(8,128)(2,1)}), bf16[8,32,2048]{2,1,0:T(8,128)(2,1)S(1)}, u32[]{:S(2)}, u32[]{:S(2)}) async-start(bf16[8,32,2048]{2,1,0:T(8,128)(2,1)} %bitcast.3), calls=%async_computation.1 | async-start | bytes 2097152 | tf_op jit(solution)/shard_map/all_to_all | solution.py:267
  58.6 0.0 all-gather.2.cloned.1.call-start
  58.7 0.0 copy-done
  58.7 0.1 constant_dynamic-slice_fusion
  58.8 0.7 copy.19.routes_ref
  59.5 1.7 slots.1
  61.1 26.7 %all-to-all-done.1.parts_ref = bf16[8,32,2048]{2,1,0:T(8,128)(2,1)S(1)} async-done(((bf16[8,32,2048]{2,1,0:T(8,128)(2,1)}), bf16[8,32,2048]{2,1,0:T(8,128)(2,1)S(1)}, u32[]{:S(2)}, u32[]{:S(2)}) %all-to-all-start.1) | async-done | bytes 1048608 | tf_op jit(solution)/shard_map/all_to_all | solution.py:267
  87.9 0.0 copy-start.1
  87.9 1.0 copy-done.1
  88.9 0.0 copy-start.3
  88.9 0.0 copy-start.4
  88.9 2.7 %dispatch.1 = (bf16[32,2048]{1,0:T(8,128)(2,1)}, bf16[768,256]{1,0:T(8,128)(2,1)}) custom-call(bf16[8,32,2048]{2,1,0:T(8,128)(2,1)} %copy-done.1, bf16[32,2048]{1,0:T(8,128)(2,1)} %resid_ref.1, f32[1,2048]{1,0:T(1,128)} %bitcast.30, s32[2,256]{1,0:T(2,128)} %get-tuple-element.22.line_ref), custom_call_target="tpu_custom_call" | custom-call | tf_op jit(solution)/shard_map/dispatch/pallas_call | solution.py:272
  91.6 17.8 %all_to_all.25 = bf16[32,24,256]{2,1,0:T(8,128)(2,1)S(1)} all-to-all(bf16[32,24,256]{2,1,0:T(8,128)(2,1)} %bitcast.29), channel_id=1, replica_groups=mesh['sp'=32,'tp'=16] {'sp'}, dimensions={0} | all-to-all | bytes 786432 | tf_op jit(solution)/shard_map/all_to_all | solution.py:283
  109.4 0.9 reshape.28
  110.4 0.0 all-gather.2.cloned.1.call-update
  110.4 3.5 %all-to-all-start.3 = ((bf16[8,256,128]{2,1,0:T(8,128)(2,1)}), bf16[8,256,128]{2,1,0:T(8,128)(2,1)S(1)}, u32[]{:S(2)}, u32[]{:S(2)}) async-start(bf16[8,256,128]{2,1,0:T(8,128)(2,1)} %bitcast.9), calls=%async_computation.3 | async-start | bytes 1048576 | tf_op jit(solution)/shard_map/all_to_all | solution.py:291
  113.9 0.0 reduce-scatter.2.cloned.1.call-start
  114.0 0.0 copy-done.3
  114.0 4.2 %collective-permute-start.3 = (bf16[2048,128]{1,0:T(8,128)(2,1)S(1)}, bf16[2048,128]{1,0:T(8,128)(2,1)S(1)}, u32[]{:S(2)}, u32[]{:S(2)}) collective-permute-start(bf16[2048,128]{1,0:T(8,128)(2,1)S(1)} %bitcast.24), channel_id=1, source_target_pairs={{0,1},{1,0},{2,3},{3,2},{4,5},{5,4},{6,7},{7,6},{8,9},{9,8},{10,11... | collective-permute-start | bytes 1572872 | tf_op jit(solution)/shard_map/ppermute | solution.py:33
  118.2 0.0 copy-done.4
  118.2 1.9 collective-permute-start.4
  120.1 13.8 %all-to-all-done.3 = bf16[8,256,128]{2,1,0:T(8,128)(2,1)S(1)} async-done(((bf16[8,256,128]{2,1,0:T(8,128)(2,1)}), bf16[8,256,128]{2,1,0:T(8,128)(2,1)S(1)}, u32[]{:S(2)}, u32[]{:S(2)}) %all-to-all-start.3) | async-done | bytes 524320 | tf_op jit(solution)/shard_map/all_to_all | solution.py:291
  133.9 5.9 %collective-permute-start.5 = (bf16[8,256,128]{2,1,0:T(8,128)(2,1)S(1)}, bf16[8,256,128]{2,1,0:T(8,128)(2,1)S(1)}, u32[]{:S(2)}, u32[]{:S(2)}) collective-permute-start(bf16[8,256,128]{2,1,0:T(8,128)(2,1)S(1)} %all-to-all-done.3), channel_id=1, source_target_pairs={{0,1},{1,0},{2,3},{3,2},{4,5},{5,4},{6,7},{7,6},{8,9},{9,8},{10,11... | collective-permute-start | bytes 1572872 | tf_op jit(solution)/shard_map/ppermute | solution.py:33
  139.9 0.0 collective-permute-done.3
  139.9 1.3 maximum_select_fusion.gate_ref
  141.2 0.0 collective-permute-done.4
  141.2 1.4 maximum_select_fusion.1.up_ref
  142.7 0.0 collective-permute-done.5
  142.7 0.2 maximum_select_fusion.2
  142.8 1.1 copy.17
  143.9 1.3 copy.22
  145.3 13.3 %all-gather.2.cloned.1.call-done.rows_ref = bf16[768,2048]{1,0:T(8,128)(2,1)} async-done(((bf16[96,2048]{1,0:T(8,128)(2,1)}), bf16[768,2048]{1,0:T(8,128)(2,1)}) %all-gather.2.cloned.1.call-update) | async-done | bytes 3145744 | tf_op jit(solution)/shard_map/all_gather | solution.py:286
  158.6 7.2 %experts.1 = bf16[768,2048]{1,0:T(8,128)(2,1)} custom-call(bf16[768,2048]{1,0:T(8,128)(2,1)} %all-gather.2.cloned.1.call-done.rows_ref, bf16[2048,256]{1,0:T(8,128)(2,1)} %maximum_select_fusion.gate_ref, bf16[2048,256]{1,0:T(8,128)(2,1)} %maximum_select_fusion.1.up_ref, bf16[256,2048]{1,0:T(8,128)(2,1)} %bitcast.20), custom_call_target="tpu_custom_call" | custom-call | tf_op jit(solution)/shard_map/experts/pallas_call | solution.py:301
  165.8 0.0 copy-start.6
  165.8 0.0 reduce-scatter.2.cloned.1.call-update
  165.8 40.6 %reduce-scatter.2.cloned.1.call-done = bf16[96,2048]{1,0:T(8,128)(2,1)} async-done(((bf16[768,2048]{1,0:T(8,128)(2,1)}), bf16[96,2048]{1,0:T(8,128)(2,1)}) %reduce-scatter.2.cloned.1.call-update) | async-done | bytes 393232 | tf_op jit(solution)/shard_map/reduce_scatter | solution.py:314
  206.4 1.9 reshape.31
  208.3 10.0 %all-to-all-start.4 = ((bf16[32,24,256]{2,1,0:T(8,128)(2,1)}), bf16[32,24,256]{2,1,0:T(8,128)(2,1)S(1)}, u32[]{:S(2)}, u32[]{:S(2)}) async-start(bf16[32,24,256]{2,1,0:T(8,128)(2,1)} %reshape.31), calls=%async_computation.5 | async-start | bytes 786432 | tf_op jit(solution)/shard_map/all_to_all | solution.py:318
  218.3 0.0 copy-done.6
  218.3 0.7 copy.18.weight_ref
  219.0 10.9 %all-to-all-done.4 = bf16[32,24,256]{2,1,0:T(8,128)(2,1)S(1)} async-done(((bf16[32,24,256]{2,1,0:T(8,128)(2,1)}), bf16[32,24,256]{2,1,0:T(8,128)(2,1)S(1)}, u32[]{:S(2)}, u32[]{:S(2)}) %all-to-all-start.4) | async-done | bytes 393248 | tf_op jit(solution)/shard_map/all_to_all | solution.py:318
  229.9 0.0 copy-start.2
  229.9 0.8 copy-done.2
  230.6 2.4 %combine.1 = bf16[32,2048]{1,0:T(8,128)(2,1)} custom-call(bf16[32,2048]{1,0:T(8,128)(2,1)} %get-tuple-element.23.stream_ref, bf16[768,256]{1,0:T(8,128)(2,1)} %bitcast.23, s32[64,1]{1,0:T(8,128)} %get-tuple-element.28.column_ref, f32[32,2]{1,0:T(8,128)} %copy.18.weight_ref), custom_call_target="tpu_custom_call" | custom-call | tf_op jit(solution)/shard_map/combine/pallas_call | solution.py:319
Async XLA Ops:
  6.5 52.1 %copy-start = (s32[512,2]{0,1:T(2,128)S(1)}, s32[512,2]{0,1:T(2,128)}, u32[]{:S(2)}) copy-start(s32[512,2]{0,1:T(2,128)} %param.25) | copy-start | bytes 12292
  6.5 43.0 %collective-permute-start.2 = (bf16[128,2048]{1,0:T(8,128)(2,1)}, bf16[128,2048]{1,0:T(8,128)(2,1)S(1)}, u32[]{:S(2)}, u32[]{:S(2)}) collective-permute-start(bf16[128,2048]{1,0:T(8,128)(2,1)} %param.23), channel_id=1, source_target_pairs={{0,1},{1,0},{2,3},{3,2},{4,5},{5,4},{6,7},{7,6},{8,9},{9,8},{10,11... | collective-permute-start | bytes 1572872 | tf_op jit(solution)/shard_map/ppermute | solution.py:33
  16.1 2.0 collective-permute-start
  18.1 0.6 copy-start.8
  21.9 27.6 %copy-start.7 = (bf16[128,2048]{1,0:T(8,128)(2,1)S(1)}, bf16[128,2048]{1,0:T(8,128)(2,1)}, u32[]{:S(2)}) copy-start(bf16[128,2048]{1,0:T(8,128)(2,1)} %param.23) | copy-start | bytes 1572868
  21.9 19.5 %all-to-all-start = ((f32[32,2,128]{2,1,0:T(2,128)}), f32[32,2,128]{2,1,0:T(2,128)S(1)}, u32[]{:S(2)}, u32[]{:S(2)}) async-start(f32[32,2,128]{2,1,0:T(2,128)} %get-tuple-element.17), calls=%async_computation | async-start | bytes 65536 | tf_op jit(solution)/shard_map/all_to_all | solution.py:254
  41.4 0.6 copy-start.5
  43.9 5.6 %collective-permute-start.1 = (bf16[256,128]{1,0:T(8,128)(2,1)}, bf16[256,128]{1,0:T(8,128)(2,1)S(1)}, u32[]{:S(2)}, u32[]{:S(2)}) collective-permute-start(bf16[256,128]{1,0:T(8,128)(2,1)} %get-tuple-element.21), channel_id=1, source_target_pairs={{0,1},{1,0},{2,3},{3,2},{4,5},{5,4},{6,7},{7,6},{8,9},{9,8},{10,11... | collective-permute-start | bytes 196616 | tf_op jit(solution)/shard_map/ppermute | solution.py:33
  51.8 36.1 %all-to-all-start.1 = ((bf16[8,32,2048]{2,1,0:T(8,128)(2,1)}), bf16[8,32,2048]{2,1,0:T(8,128)(2,1)S(1)}, u32[]{:S(2)}, u32[]{:S(2)}) async-start(bf16[8,32,2048]{2,1,0:T(8,128)(2,1)} %bitcast.3), calls=%async_computation.1 | async-start | bytes 2097152 | tf_op jit(solution)/shard_map/all_to_all | solution.py:267
  58.6 99.9 %all-gather.2.cloned.1.call-start = ((), (), s32[]{:S(2)}) async-start(), calls=%async_computation.6 | async-start | bytes 3538944 | tf_op jit(solution)/shard_map/all_gather | solution.py:286
  87.9 1.0 copy-start.1
  88.9 25.1 %copy-start.3 = (bf16[1,2048,128]{2,1,0:T(8,128)(2,1)S(1)}, bf16[1,2048,128]{2,1,0:T(8,128)(2,1)}, u32[]{:S(2)}) copy-start(bf16[1,2048,128]{2,1,0:T(8,128)(2,1)} %param.27) | copy-start | bytes 1572868
  88.9 29.3 %copy-start.4 = (bf16[1,2048,128]{2,1,0:T(8,128)(2,1)S(1)}, bf16[1,2048,128]{2,1,0:T(8,128)(2,1)}, u32[]{:S(2)}) copy-start(bf16[1,2048,128]{2,1,0:T(8,128)(2,1)} %param.28) | copy-start | bytes 1572868
  110.4 23.6 %all-to-all-start.3 = ((bf16[8,256,128]{2,1,0:T(8,128)(2,1)}), bf16[8,256,128]{2,1,0:T(8,128)(2,1)S(1)}, u32[]{:S(2)}, u32[]{:S(2)}) async-start(bf16[8,256,128]{2,1,0:T(8,128)(2,1)} %bitcast.9), calls=%async_computation.3 | async-start | bytes 1048576 | tf_op jit(solution)/shard_map/all_to_all | solution.py:291
  113.9 92.5 %reduce-scatter.2.cloned.1.call-start = ((), (), s32[]{:S(2)}) async-start(), calls=%async_computation.7 | async-start | bytes 3538944 | tf_op jit(solution)/shard_map/reduce_scatter | solution.py:314
  114.0 25.9 %collective-permute-start.3 = (bf16[2048,128]{1,0:T(8,128)(2,1)S(1)}, bf16[2048,128]{1,0:T(8,128)(2,1)S(1)}, u32[]{:S(2)}, u32[]{:S(2)}) collective-permute-start(bf16[2048,128]{1,0:T(8,128)(2,1)S(1)} %bitcast.24), channel_id=1, source_target_pairs={{0,1},{1,0},{2,3},{3,2},{4,5},{5,4},{6,7},{7,6},{8,9},{9,8},{10,11... | collective-permute-start | bytes 1572872 | tf_op jit(solution)/shard_map/ppermute | solution.py:33
  118.2 23.0 %collective-permute-start.4 = (bf16[2048,128]{1,0:T(8,128)(2,1)S(1)}, bf16[2048,128]{1,0:T(8,128)(2,1)S(1)}, u32[]{:S(2)}, u32[]{:S(2)}) collective-permute-start(bf16[2048,128]{1,0:T(8,128)(2,1)S(1)} %bitcast.26), channel_id=1, source_target_pairs={{0,1},{1,0},{2,3},{3,2},{4,5},{5,4},{6,7},{7,6},{8,9},{9,8},{10,11... | collective-permute-start | bytes 1572872 | tf_op jit(solution)/shard_map/ppermute | solution.py:33
  133.9 8.7 %collective-permute-start.5 = (bf16[8,256,128]{2,1,0:T(8,128)(2,1)S(1)}, bf16[8,256,128]{2,1,0:T(8,128)(2,1)S(1)}, u32[]{:S(2)}, u32[]{:S(2)}) collective-permute-start(bf16[8,256,128]{2,1,0:T(8,128)(2,1)S(1)} %all-to-all-done.3), channel_id=1, source_target_pairs={{0,1},{1,0},{2,3},{3,2},{4,5},{5,4},{6,7},{7,6},{8,9},{9,8},{10,11... | collective-permute-start | bytes 1572872 | tf_op jit(solution)/shard_map/ppermute | solution.py:33
  165.8 52.6 %copy-start.6 = (f32[32,2]{0,1:T(2,128)S(1)}, f32[32,2]{0,1:T(2,128)}, u32[]{:S(2)}) copy-start(f32[32,2]{0,1:T(2,128)} %param.26) | copy-start | bytes 772
  208.3 21.5 %all-to-all-start.4 = ((bf16[32,24,256]{2,1,0:T(8,128)(2,1)}), bf16[32,24,256]{2,1,0:T(8,128)(2,1)S(1)}, u32[]{:S(2)}, u32[]{:S(2)}) async-start(bf16[32,24,256]{2,1,0:T(8,128)(2,1)} %reshape.31), calls=%async_computation.5 | async-start | bytes 786432 | tf_op jit(solution)/shard_map/all_to_all | solution.py:318
  229.9 0.8 copy-start.2
Sparse Core Ops, SparseCore 0:
  110.5 48.0 all-gather.1
  165.9 40.4 reduce-scatter.1

commit v6 on v5

--- a/solution.py
+++ b/solution.py
@@ -11,6 +11,8 @@
 SEGMENTS = 8
 CORES = 2
 CAP = 3
+QUAD = 4
+EXPERT_STEPS = 2
 PIECES = 8
 GELU_SCALE = 0.7978845608028654
 
@@ -90,8 +92,8 @@
     total_ref[:, 1:2, :] = jnp.broadcast_to(whole_b[None], (total_ref.shape[0], 1, channels))
 
 
-def branch_kernel(place_ref, pieces_ref, state_ref, running_ref, gate_ref, keep_ref, send_ref):
-    place, core = place_ref[0], place_ref[1]
+def branch_kernel(place_ref, pieces_ref, state_ref, running_ref, gate_ref, out_ref):
+    place = place_ref[0]
     carry = jnp.zeros((1, state_ref.shape[1]), jnp.float32)
     for k in range(pieces_ref.shape[0]):
         after = pieces_ref[k, 0:1, :] * carry + pieces_ref[k, 1:2, :]
@@ -99,14 +101,23 @@
     length = state_ref.shape[0] // SEGMENTS
     half = length // CORES
     for k in range(SEGMENTS):
-        for out, side in ((keep_ref, core), (send_ref, 1 - core)):
-            rows = pl.ds(pl.multiple_of(k * length + side * half, half), half)
-            state = state_ref[rows, :] + running_ref[rows, :] * carry
-            g = gate_ref[rows, :].astype(jnp.float32)
-            gelu = 0.5 * g * (1.0 + jnp.tanh(GELU_SCALE * (g + 0.044715 * (g * g * g))))
-            out[k * half : (k + 1) * half, :] = (gelu * state).astype(jnp.bfloat16)
-        last = (k + 1) * length - 1
-        carry = running_ref[last : last + 1, :] * carry + state_ref[last : last + 1, :]
+        rows = slice(k * length, (k + 1) * length)
+        state = state_ref[rows, :] + running_ref[rows, :] * carry
+        g = gate_ref[rows, :].astype(jnp.float32)
+        gelu = 0.5 * g * (1.0 + jnp.tanh(GELU_SCALE * (g + 0.044715 * (g * g * g))))
+        branch = (gelu * state).astype(jnp.bfloat16)
+        for core in range(CORES):
+            at = k * CORES + core
+            low = at // QUAD * half
+            out_ref[at % QUAD, low : low + half, :] = branch[core * half : (core + 1) * half]
+        carry = state[length - 1 : length, :]
+
+
+def project_kernel(branch_ref, weight_ref, out_ref):
+    branch = jnp.concatenate([branch_ref[k] for k in range(branch_ref.shape[0])], axis=1)
+    out_ref[...] = jnp.dot(branch, weight_ref[...], preferred_element_type=jnp.float32).astype(
+        jnp.bfloat16
+    )
 
 
 def slots_kernel(routes_ref, column_ref, line_ref):
@@ -210,7 +221,11 @@
     f32, bf16 = jnp.float32, jnp.bfloat16
 
     rim = shifted(recurrent_input[tokens - taps + 1 :], "sp", 1)
-    projection_other = swap_cores(output_projection_weight)
+    quads = [[k * QUAD + i for i in range(QUAD)] for k in range(tp // QUAD)]
+    strides = [[k * QUAD + i for k in range(tp // QUAD)] for i in range(QUAD)]
+    projection = lax.all_gather(
+        output_projection_weight, "tp", axis=0, axis_index_groups=quads, tiled=True
+    )
 
     own_routes = lax.dynamic_slice_in_dim(routes, here * rows_dev, rows_dev, 0)
     column, line = pl.pallas_call(
@@ -252,20 +267,29 @@
     )
 
     pieces = lax.all_to_all(total, "sp", 0, 0, tiled=True)
-    keep, send = pl.pallas_call(
+    branch = pl.pallas_call(
         branch_kernel,
-        out_shape=(jax.ShapeDtypeStruct((tokens // CORES, channels), bf16),) * 2,
+        out_shape=jax.ShapeDtypeStruct((QUAD, tokens // QUAD, channels), bf16),
         in_specs=[SMEM] + [VMEM] * 4,
-        out_specs=(VMEM,) * 2,
-        cost_estimate=pl.CostEstimate(flops=10**9, bytes_accessed=2**20, transcendentals=0),
+        out_specs=VMEM,
         name="branch",
-    )(jnp.stack([place, core]).astype(jnp.int32), pieces, state, running, recurrent_out_gate)
-    got = swap_cores(send)
-    both = jnp.concatenate([keep, got], axis=1)
-    projection = jnp.concatenate([output_projection_weight, projection_other], axis=0)
-    partial = jnp.dot(both, projection, preferred_element_type=f32).astype(bf16)
+    )(place.astype(jnp.int32)[None], pieces, state, running, recurrent_out_gate)
+    mine = lax.all_to_all(branch, "tp", 0, 0, axis_index_groups=quads, tiled=True)
+    cut = width // 2
+    partial = pl.pallas_call(
+        project_kernel,
+        grid=(width // cut,),
+        out_shape=jax.ShapeDtypeStruct((tokens // QUAD, width), bf16),
+        in_specs=[
+            pl.BlockSpec(mine.shape, lambda k: (0, 0, 0)),
+            pl.BlockSpec((QUAD * channels, cut), lambda k: (0, k)),
+        ],
+        out_specs=pl.BlockSpec((tokens // QUAD, cut), lambda k: (0, k)),
+        name="project",
+    )(mine, projection)
     parts = lax.all_to_all(
-        partial.reshape(chips, rows_dev, width), "tp", 0, 0, axis_index_groups=groups, tiled=True
+        partial.reshape(tp // QUAD, rows_dev, width), "tp", 0, 0,
+        axis_index_groups=strides, tiled=True,
     )
     slot_count = experts * CAP
     whole = lambda *shape: pl.BlockSpec(shape, lambda k: (0,) * len(shape))
@@ -297,10 +321,10 @@
     down = natural(down_own[:, None], swap_cores(down_own)[:, None], core, 1)
     down = jnp.moveaxis(down.reshape(tp, CORES * hidden, -1), 0, 1).reshape(CORES * hidden, width)
     depth = CORES * hidden
-    block = rows.shape[0] // 4
+    block = rows.shape[0] // EXPERT_STEPS
     summed = pl.pallas_call(
         expert_kernel,
-        grid=(4,),
+        grid=(EXPERT_STEPS,),
         out_shape=jax.ShapeDtypeStruct(rows.shape, bf16),
         in_specs=[
             pl.BlockSpec((block, width), lambda k: (k, 0)),

time: 244 us -> 236 us (0.967)
  waiting for transfers between devices: 115 us -> 96.4 us
  blocking collectives: 17.8 us -> 29.4 us
    all_to_all x1, waiting for transfers between devices: 26.7 us -> 11.1 us  [layer(): lax.all_to_all(partial.reshape(tp // QUAD, rows_dev, width), 'tp', 0, 0,...]
    all_to_all x0 -> x1, blocking collectives: none -> 10.8 us  [layer(): lax.all_to_all(branch, 'tp', 0, 0, axis_index_groups=quads, tiled=True)]
    ppermute x5 -> x3, starting transfers between devices: 25.4 us -> 16.2 us  [swap_cores(): return lax.ppermute(x, 'tp', [(i, i ^ 1) for i in range(size)])]
    all_to_all x1, waiting for transfers between devices: 13.8 us -> 9.38 us  [layer(): lax.all_to_all(down_part.reshape(chips, CORES * hidden, -1), 'tp', 0, 0,...]
    all_to_all x1, starting transfers between devices: 3.51 us -> 7.9 us  [layer(): lax.all_to_all(down_part.reshape(chips, CORES * hidden, -1), 'tp', 0, 0,...]
    all_to_all x1, starting transfers between devices: 10.8 us -> 14.2 us  [layer(): pieces = lax.all_to_all(total, 'sp', 0, 0, tiled=True)]
    ppermute x1, starting transfers between devices: 1.28 us -> 3.92 us  [shifted(): return lax.ppermute(block, axis, route)]
    pallas_call x2 -> x3, Pallas kernels: 9.09 us -> 11 us  [the longest x1 6.45 us: layer(): pl.pallas_call(expert_kernel, grid=(EXPERT_STEPS,), out_shape=jax.ShapeDt...]
  transfers between devices with their start and end apart: 12 -> 11, of which waited for: 8 -> 7; matrix products, arithmetic and copies ran while one was open for 3% -> 3% of each run, Pallas kernels for 3% -> 3%
where the time goes in v6:
time: 236 us; the launch traced here: 232 us
  waiting for transfers between devices  96.4 us (41%)
  starting transfers between devices  58.9 us (25%)
  blocking collectives  29.4 us (12%)
  Pallas kernels  20.7 us (9%)
  between operations  13.2 us (6%)
  local copies, waits for them, and re-layouts  10.2 us (4%)
  other arithmetic  2.94 us (1%)
    reduce_scatter x1, waiting for transfers between devices, layer(): lax.psum_scatter(summed, 'tp', scatter_dimension=0, axis_index_groups=gro...  41.1 us
    all_to_all x1, blocking collectives, layer(): arrived = lax.all_to_all(outgoing.reshape(packed), 'sp', 0, 0, tiled=True)  18.5 us
    ppermute x3, starting transfers between devices, swap_cores(): return lax.ppermute(x, 'tp', [(i, i ^ 1) for i in range(size)])  16.2 us
    all_to_all x1, starting transfers between devices, layer(): pieces = lax.all_to_all(total, 'sp', 0, 0, tiled=True)  14.2 us
    all_gather x1, waiting for transfers between devices, layer(): lax.all_gather(arrived, 'tp', axis=0, axis_index_groups=groups, tiled=True)  13.7 us
    all_to_all x1, waiting for transfers between devices, layer(): lax.all_to_all(partial.reshape(tp // QUAD, rows_dev, width), 'tp', 0, 0,...  11.1 us
    all_to_all x1, waiting for transfers between devices, layer(): returned = lax.all_to_all(result.reshape(packed), 'sp', 0, 0, tiled=True)  10.9 us
    all_to_all x1, blocking collectives, layer(): lax.all_to_all(branch, 'tp', 0, 0, axis_index_groups=quads, tiled=True)  10.8 us
  transfers between devices with their start and end apart: 11, of which 7 were waited for; matrix products, arithmetic and copies ran while one was open for 3% of the time, Pallas kernels for 3%

profile of v6, /device:TPU:1, one launch (start us, length us, event | category | flops | bytes accessed | tf_op | source)
XLA Modules:
  0.0 231.7 jit_solution(803163123271115408)
XLA Ops:
  6.5 0.0 copy-start
  6.5 0.0 all-gather.3.cloned.1.call-start
  6.5 0.7 all-gather.3.cloned.1.call-update
  7.3 0.7 slice.3
  7.9 3.9 %collective-permute-start = (bf16[3,128]{1,0:T(4,128)(2,1)S(1)}, bf16[3,128]{1,0:T(4,128)(2,1)S(1)}, u32[]{:S(2)}, u32[]{:S(2)}) collective-permute-start(bf16[3,128]{1,0:T(4,128)(2,1)S(1)} %slice.3), channel_id=1, source_target_pairs={{0,16},{16,32},{32,48},{48,64},{64,80},{80,96},{96,112},{112,128},... | collective-permute-start | bytes 2312 | tf_op jit(solution)/shard_map/ppermute | solution.py:26
  11.9 0.7 collective-permute-done.rim_ref
  12.6 0.0 copy-start.7
  12.6 0.6 copy-done.7
  13.2 3.2 %recurrence.1 = (f32[512,128]{1,0:T(8,128)}, f32[512,128]{1,0:T(8,128)}, f32[32,2,128]{2,1,0:T(2,128)}) custom-call(bf16[512,128]{1,0:T(8,128)(2,1)} %x_ref.1, bf16[3,128]{1,0:T(4,128)(2,1)} %copy-done.7, f32[4,128]{1,0:T(4,128)} %filter_ref.1, bf16[2,64,64]{2,1,0:T(8,128)(2,1)} %recur_ref.1, bf16[2,64,64]{2,1,0:T(8,128)(2,1)} %input_ref.1, ...), custom_call_target="tpu_custom_call" | custom-call | flops 1000000000 | bytes 1048576 | tf_op jit(solution)/shard_map/recurrence/pallas_call | solution.py:242
  16.4 14.2 %all-to-all-start = ((f32[32,2,128]{2,1,0:T(2,128)}), f32[32,2,128]{2,1,0:T(2,128)S(1)}, u32[]{:S(2)}, u32[]{:S(2)}) async-start(f32[32,2,128]{2,1,0:T(2,128)} %get-tuple-element.15), calls=%async_computation | async-start | bytes 65536 | tf_op jit(solution)/shard_map/all_to_all | solution.py:269
  30.6 8.7 %all-to-all-done.pieces_ref = f32[32,2,128]{2,1,0:T(2,128)S(1)} async-done(((f32[32,2,128]{2,1,0:T(2,128)}), f32[32,2,128]{2,1,0:T(2,128)S(1)}, u32[]{:S(2)}, u32[]{:S(2)}) %all-to-all-start) | async-done | bytes 32800 | tf_op jit(solution)/shard_map/all_to_all | solution.py:269
  39.3 0.0 copy-start.5
  39.3 0.6 copy-done.5
  39.9 1.9 branch.1
  41.8 10.8 %all_to_all.30.branch_ref = bf16[4,128,128]{2,1,0:T(8,128)(2,1)} all-to-all(bf16[4,128,128]{2,1,0:T(8,128)(2,1)} %branch.1), channel_id=1, replica_groups={{0,1,2,3},{4,5,6,7},{8,9,10,11},{12,13,14,15},{16,17,18,19},{20,21,22,2..., dimensions={0} | all-to-all | bytes 262144 | tf_op jit(solution)/shard_map/all_to_all | solution.py:277
  52.6 0.0 all-gather.3.cloned.1.call-done.weight_ref
  52.6 2.6 %project.1 = bf16[128,2048]{1,0:T(8,128)(2,1)} custom-call(bf16[4,128,128]{2,1,0:T(8,128)(2,1)} %all_to_all.30.branch_ref, bf16[512,2048]{1,0:T(8,128)(2,1)} %all-gather.3.cloned.1.call-done.weight_ref), custom_call_target="tpu_custom_call" | custom-call | tf_op jit(solution)/shard_map/project/pallas_call | solution.py:279
  55.2 6.8 %all-to-all-start.2 = ((bf16[4,32,2048]{2,1,0:T(8,128)(2,1)}), bf16[4,32,2048]{2,1,0:T(8,128)(2,1)S(1)}, u32[]{:S(2)}, u32[]{:S(2)}) async-start(bf16[4,32,2048]{2,1,0:T(8,128)(2,1)} %bitcast.22), calls=%async_computation.2 | async-start | bytes 1048576 | tf_op jit(solution)/shard_map/all_to_all | solution.py:290
  62.0 0.0 copy-start.3
  62.0 0.0 copy-start.4
  62.0 0.0 all-gather.5.cloned.1.call-start
  62.1 0.0 copy-done
  62.1 0.1 constant_dynamic-slice_fusion
  62.2 0.7 copy.19.routes_ref
  62.9 1.7 slots.1
  64.6 11.1 %all-to-all-done.2.parts_ref = bf16[4,32,2048]{2,1,0:T(8,128)(2,1)S(1)} async-done(((bf16[4,32,2048]{2,1,0:T(8,128)(2,1)}), bf16[4,32,2048]{2,1,0:T(8,128)(2,1)S(1)}, u32[]{:S(2)}, u32[]{:S(2)}) %all-to-all-start.2) | async-done | bytes 524320 | tf_op jit(solution)/shard_map/all_to_all | solution.py:290
  75.7 0.0 copy-start.1
  75.7 0.8 copy-done.1
  76.5 2.4 %dispatch.1 = (bf16[32,2048]{1,0:T(8,128)(2,1)}, bf16[768,256]{1,0:T(8,128)(2,1)}) custom-call(bf16[4,32,2048]{2,1,0:T(8,128)(2,1)} %copy-done.1, bf16[32,2048]{1,0:T(8,128)(2,1)} %resid_ref.1, f32[1,2048]{1,0:T(1,128)} %bitcast.30, s32[2,256]{1,0:T(2,128)} %get-tuple-element.18.line_ref), custom_call_target="tpu_custom_call" | custom-call | tf_op jit(solution)/shard_map/dispatch/pallas_call | solution.py:296
  78.9 18.5 %all_to_all.31 = bf16[32,24,256]{2,1,0:T(8,128)(2,1)S(1)} all-to-all(bf16[32,24,256]{2,1,0:T(8,128)(2,1)} %bitcast.29), channel_id=1, replica_groups=mesh['sp'=32,'tp'=16] {'sp'}, dimensions={0} | all-to-all | bytes 786432 | tf_op jit(solution)/shard_map/all_to_all | solution.py:307
  97.5 0.9 reshape.28
  98.4 0.0 all-gather.5.cloned.1.call-update
  98.4 7.9 %all-to-all-start.4 = ((bf16[8,256,128]{2,1,0:T(8,128)(2,1)}), bf16[8,256,128]{2,1,0:T(8,128)(2,1)S(1)}, u32[]{:S(2)}, u32[]{:S(2)}) async-start(bf16[8,256,128]{2,1,0:T(8,128)(2,1)} %bitcast.8), calls=%async_computation.4 | async-start | bytes 1048576 | tf_op jit(solution)/shard_map/all_to_all | solution.py:315
  106.3 0.0 reduce-scatter.2.cloned.1.call-start
  106.4 0.0 copy-done.3
  106.4 4.8 %collective-permute-start.1 = (bf16[2048,128]{1,0:T(8,128)(2,1)S(1)}, bf16[2048,128]{1,0:T(8,128)(2,1)S(1)}, u32[]{:S(2)}, u32[]{:S(2)}) collective-permute-start(bf16[2048,128]{1,0:T(8,128)(2,1)S(1)} %bitcast.24), channel_id=1, source_target_pairs={{0,1},{1,0},{2,3},{3,2},{4,5},{5,4},{6,7},{7,6},{8,9},{9,8},{10,11... | collective-permute-start | bytes 1572872 | tf_op jit(solution)/shard_map/ppermute | solution.py:35
  111.1 0.0 copy-done.4
  111.1 1.9 collective-permute-start.2
  113.1 9.4 %all-to-all-done.4 = bf16[8,256,128]{2,1,0:T(8,128)(2,1)S(1)} async-done(((bf16[8,256,128]{2,1,0:T(8,128)(2,1)}), bf16[8,256,128]{2,1,0:T(8,128)(2,1)S(1)}, u32[]{:S(2)}, u32[]{:S(2)}) %all-to-all-start.4) | async-done | bytes 524320 | tf_op jit(solution)/shard_map/all_to_all | solution.py:315
  122.5 9.5 %collective-permute-start.3 = (bf16[8,256,128]{2,1,0:T(8,128)(2,1)S(1)}, bf16[8,256,128]{2,1,0:T(8,128)(2,1)S(1)}, u32[]{:S(2)}, u32[]{:S(2)}) collective-permute-start(bf16[8,256,128]{2,1,0:T(8,128)(2,1)S(1)} %all-to-all-done.4), channel_id=1, source_target_pairs={{0,1},{1,0},{2,3},{3,2},{4,5},{5,4},{6,7},{7,6},{8,9},{9,8},{10,11... | collective-permute-start | bytes 1572872 | tf_op jit(solution)/shard_map/ppermute | solution.py:35
  132.0 0.0 collective-permute-done.1
  132.0 1.3 maximum_select_fusion.gate_ref
  133.3 0.0 collective-permute-done.2
  133.3 1.4 maximum_select_fusion.1.up_ref
  134.7 0.0 collective-permute-done.3
  134.7 0.2 maximum_select_fusion.2
  134.9 1.1 copy.17
  136.0 1.3 copy.22
  137.3 13.7 %all-gather.5.cloned.1.call-done.rows_ref = bf16[768,2048]{1,0:T(8,128)(2,1)} async-done(((bf16[96,2048]{1,0:T(8,128)(2,1)}), bf16[768,2048]{1,0:T(8,128)(2,1)}) %all-gather.5.cloned.1.call-update) | async-done | bytes 3145744 | tf_op jit(solution)/shard_map/all_gather | solution.py:310
  151.1 6.5 %experts.1 = bf16[768,2048]{1,0:T(8,128)(2,1)} custom-call(bf16[768,2048]{1,0:T(8,128)(2,1)} %all-gather.5.cloned.1.call-done.rows_ref, bf16[2048,256]{1,0:T(8,128)(2,1)} %maximum_select_fusion.gate_ref, bf16[2048,256]{1,0:T(8,128)(2,1)} %maximum_select_fusion.1.up_ref, bf16[256,2048]{1,0:T(8,128)(2,1)} %bitcast.19), custom_call_target="tpu_custom_call" | custom-call | tf_op jit(solution)/shard_map/experts/pallas_call | solution.py:325
  157.5 0.0 copy-start.6
  157.5 0.0 reduce-scatter.2.cloned.1.call-update
  157.5 41.1 %reduce-scatter.2.cloned.1.call-done = bf16[96,2048]{1,0:T(8,128)(2,1)} async-done(((bf16[768,2048]{1,0:T(8,128)(2,1)}), bf16[96,2048]{1,0:T(8,128)(2,1)}) %reduce-scatter.2.cloned.1.call-update) | async-done | bytes 393232 | tf_op jit(solution)/shard_map/reduce_scatter | solution.py:338
  198.7 1.9 reshape.31
  200.6 9.8 %all-to-all-start.5 = ((bf16[32,24,256]{2,1,0:T(8,128)(2,1)}), bf16[32,24,256]{2,1,0:T(8,128)(2,1)S(1)}, u32[]{:S(2)}, u32[]{:S(2)}) async-start(bf16[32,24,256]{2,1,0:T(8,128)(2,1)} %reshape.31), calls=%async_computation.6 | async-start | bytes 786432 | tf_op jit(solution)/shard_map/all_to_all | solution.py:342
  210.5 0.0 copy-done.6
  210.5 0.7 copy.18.weight_ref
  211.2 10.9 %all-to-all-done.5 = bf16[32,24,256]{2,1,0:T(8,128)(2,1)S(1)} async-done(((bf16[32,24,256]{2,1,0:T(8,128)(2,1)}), bf16[32,24,256]{2,1,0:T(8,128)(2,1)S(1)}, u32[]{:S(2)}, u32[]{:S(2)}) %all-to-all-start.5) | async-done | bytes 393248 | tf_op jit(solution)/shard_map/all_to_all | solution.py:342
  222.0 0.0 copy-start.2
  222.0 0.8 copy-done.2
  222.8 2.4 %combine.1 = bf16[32,2048]{1,0:T(8,128)(2,1)} custom-call(bf16[32,2048]{1,0:T(8,128)(2,1)} %get-tuple-element.19.stream_ref, bf16[768,256]{1,0:T(8,128)(2,1)} %bitcast.23, s32[64,1]{1,0:T(8,128)} %get-tuple-element.24.column_ref, f32[32,2]{1,0:T(8,128)} %copy.18.weight_ref), custom_call_target="tpu_custom_call" | custom-call | tf_op jit(solution)/shard_map/combine/pallas_call | solution.py:343
Async XLA Ops:
  6.5 55.6 %copy-start = (s32[512,2]{0,1:T(2,128)S(1)}, s32[512,2]{0,1:T(2,128)}, u32[]{:S(2)}) copy-start(s32[512,2]{0,1:T(2,128)} %param.25) | copy-start | bytes 12292
  6.5 46.1 %all-gather.3.cloned.1.call-start = ((), (), s32[]{:S(2)}) async-start(), calls=%async_computation.7 | async-start | bytes 2621440 | tf_op jit(solution)/shard_map/all_gather | solution.py:226
  7.9 4.6 %collective-permute-start = (bf16[3,128]{1,0:T(4,128)(2,1)S(1)}, bf16[3,128]{1,0:T(4,128)(2,1)S(1)}, u32[]{:S(2)}, u32[]{:S(2)}) collective-permute-start(bf16[3,128]{1,0:T(4,128)(2,1)S(1)} %slice.3), channel_id=1, source_target_pairs={{0,16},{16,32},{32,48},{48,64},{64,80},{80,96},{96,112},{112,128},... | collective-permute-start | bytes 2312 | tf_op jit(solution)/shard_map/ppermute | solution.py:26
  12.6 0.6 copy-start.7
  16.4 22.9 %all-to-all-start = ((f32[32,2,128]{2,1,0:T(2,128)}), f32[32,2,128]{2,1,0:T(2,128)S(1)}, u32[]{:S(2)}, u32[]{:S(2)}) async-start(f32[32,2,128]{2,1,0:T(2,128)} %get-tuple-element.15), calls=%async_computation | async-start | bytes 65536 | tf_op jit(solution)/shard_map/all_to_all | solution.py:269
  39.3 0.6 copy-start.5
  55.2 20.5 %all-to-all-start.2 = ((bf16[4,32,2048]{2,1,0:T(8,128)(2,1)}), bf16[4,32,2048]{2,1,0:T(8,128)(2,1)S(1)}, u32[]{:S(2)}, u32[]{:S(2)}) async-start(bf16[4,32,2048]{2,1,0:T(8,128)(2,1)} %bitcast.22), calls=%async_computation.2 | async-start | bytes 1048576 | tf_op jit(solution)/shard_map/all_to_all | solution.py:290
  62.0 44.3 %copy-start.3 = (bf16[1,2048,128]{2,1,0:T(8,128)(2,1)S(1)}, bf16[1,2048,128]{2,1,0:T(8,128)(2,1)}, u32[]{:S(2)}) copy-start(bf16[1,2048,128]{2,1,0:T(8,128)(2,1)} %param.27) | copy-start | bytes 1572868
  62.0 49.1 %copy-start.4 = (bf16[1,2048,128]{2,1,0:T(8,128)(2,1)S(1)}, bf16[1,2048,128]{2,1,0:T(8,128)(2,1)}, u32[]{:S(2)}) copy-start(bf16[1,2048,128]{2,1,0:T(8,128)(2,1)} %param.28) | copy-start | bytes 1572868
  62.0 89.0 %all-gather.5.cloned.1.call-start = ((), (), s32[]{:S(2)}) async-start(), calls=%async_computation.8 | async-start | bytes 3538944 | tf_op jit(solution)/shard_map/all_gather | solution.py:310
  75.7 0.8 copy-start.1
  98.4 24.0 %all-to-all-start.4 = ((bf16[8,256,128]{2,1,0:T(8,128)(2,1)}), bf16[8,256,128]{2,1,0:T(8,128)(2,1)S(1)}, u32[]{:S(2)}, u32[]{:S(2)}) async-start(bf16[8,256,128]{2,1,0:T(8,128)(2,1)} %bitcast.8), calls=%async_computation.4 | async-start | bytes 1048576 | tf_op jit(solution)/shard_map/all_to_all | solution.py:315
  106.3 92.4 %reduce-scatter.2.cloned.1.call-start = ((), (), s32[]{:S(2)}) async-start(), calls=%async_computation.9 | async-start | bytes 3538944 | tf_op jit(solution)/shard_map/reduce_scatter | solution.py:338
  106.4 25.6 %collective-permute-start.1 = (bf16[2048,128]{1,0:T(8,128)(2,1)S(1)}, bf16[2048,128]{1,0:T(8,128)(2,1)S(1)}, u32[]{:S(2)}, u32[]{:S(2)}) collective-permute-start(bf16[2048,128]{1,0:T(8,128)(2,1)S(1)} %bitcast.24), channel_id=1, source_target_pairs={{0,1},{1,0},{2,3},{3,2},{4,5},{5,4},{6,7},{7,6},{8,9},{9,8},{10,11... | collective-permute-start | bytes 1572872 | tf_op jit(solution)/shard_map/ppermute | solution.py:35
  111.1 22.2 %collective-permute-start.2 = (bf16[2048,128]{1,0:T(8,128)(2,1)S(1)}, bf16[2048,128]{1,0:T(8,128)(2,1)S(1)}, u32[]{:S(2)}, u32[]{:S(2)}) collective-permute-start(bf16[2048,128]{1,0:T(8,128)(2,1)S(1)} %bitcast.26), channel_id=1, source_target_pairs={{0,1},{1,0},{2,3},{3,2},{4,5},{5,4},{6,7},{7,6},{8,9},{9,8},{10,11... | collective-permute-start | bytes 1572872 | tf_op jit(solution)/shard_map/ppermute | solution.py:35
  122.5 12.3 %collective-permute-start.3 = (bf16[8,256,128]{2,1,0:T(8,128)(2,1)S(1)}, bf16[8,256,128]{2,1,0:T(8,128)(2,1)S(1)}, u32[]{:S(2)}, u32[]{:S(2)}) collective-permute-start(bf16[8,256,128]{2,1,0:T(8,128)(2,1)S(1)} %all-to-all-done.4), channel_id=1, source_target_pairs={{0,1},{1,0},{2,3},{3,2},{4,5},{5,4},{6,7},{7,6},{8,9},{9,8},{10,11... | collective-permute-start | bytes 1572872 | tf_op jit(solution)/shard_map/ppermute | solution.py:35
  157.5 52.9 %copy-start.6 = (f32[32,2]{0,1:T(2,128)S(1)}, f32[32,2]{0,1:T(2,128)}, u32[]{:S(2)}) copy-start(f32[32,2]{0,1:T(2,128)} %param.26) | copy-start | bytes 772
  200.6 21.4 %all-to-all-start.5 = ((bf16[32,24,256]{2,1,0:T(8,128)(2,1)}), bf16[32,24,256]{2,1,0:T(8,128)(2,1)S(1)}, u32[]{:S(2)}, u32[]{:S(2)}) async-start(bf16[32,24,256]{2,1,0:T(8,128)(2,1)} %reshape.31), calls=%async_computation.6 | async-start | bytes 786432 | tf_op jit(solution)/shard_map/all_to_all | solution.py:342
  222.0 0.8 copy-start.2
Sparse Core Ops, SparseCore 0:
  9.4 40.3 all-gather.2
  98.5 52.4 all-gather.4
  157.7 40.9 reduce-scatter.1

commit v7 on v6

--- a/solution.py
+++ b/solution.py
@@ -120,7 +120,8 @@
     )
 
 
-def slots_kernel(routes_ref, column_ref, line_ref):
+def slots_kernel(routes_ref, weight_ref, column_ref, line_ref, pair_ref):
+    pair_ref[...] = weight_ref[...]
     rows = routes_ref.shape[0]
     experts = 32
     number = lax.broadcasted_iota(jnp.int32, (rows, experts), 1)
@@ -177,11 +178,18 @@
     rows, width = stream_ref.shape
     piece = width // PIECES
     spot = lax.broadcasted_iota(jnp.int32, (2 * rows, returned_ref.shape[0]), 1)
+    offset = spot - column_ref[...]
+    pick = jnp.concatenate([(offset == k).astype(jnp.float32) for k in range(PIECES)], axis=0)
+    chosen = jnp.dot(
+        pick.astype(jnp.bfloat16), returned_ref[...], preferred_element_type=jnp.float32
+    )
     for k in range(PIECES):
-        pick = (column_ref[...] + k == spot).astype(jnp.float32).astype(jnp.bfloat16)
-        chosen = jnp.dot(pick, returned_ref[...], preferred_element_type=jnp.float32)
         lanes = slice(k * piece, (k + 1) * piece)
-        total = weight_ref[:, 0:1] * chosen[:rows] + weight_ref[:, 1:2] * chosen[rows:]
+        low = 2 * rows * k
+        total = (
+            weight_ref[:, 0:1] * chosen[low : low + rows]
+            + weight_ref[:, 1:2] * chosen[low + rows : low + 2 * rows]
+        )
         out_ref[:, lanes] = (stream_ref[:, lanes].astype(jnp.float32) + total).astype(jnp.bfloat16)
 
 
@@ -227,18 +235,6 @@
         output_projection_weight, "tp", axis=0, axis_index_groups=quads, tiled=True
     )
 
-    own_routes = lax.dynamic_slice_in_dim(routes, here * rows_dev, rows_dev, 0)
-    column, line = pl.pallas_call(
-        slots_kernel,
-        out_shape=(
-            jax.ShapeDtypeStruct((2 * rows_dev, 1), jnp.int32),
-            jax.ShapeDtypeStruct((2, PIECES * rows_dev), jnp.int32),
-        ),
-        in_specs=[VMEM],
-        out_specs=(VMEM,) * 2,
-        name="slots",
-    )(own_routes)
-
     state, running, total = pl.pallas_call(
         recurrence_kernel,
         out_shape=(
@@ -267,6 +263,19 @@
     )
 
     pieces = lax.all_to_all(total, "sp", 0, 0, tiled=True)
+    own_routes = lax.dynamic_slice_in_dim(routes, here * rows_dev, rows_dev, 0)
+    own_routes, pair = lax.optimization_barrier((own_routes, expert_pair_weight, total))[:2]
+    column, line, pair = pl.pallas_call(
+        slots_kernel,
+        out_shape=(
+            jax.ShapeDtypeStruct((2 * rows_dev, 1), jnp.int32),
+            jax.ShapeDtypeStruct((2, PIECES * rows_dev), jnp.int32),
+            jax.ShapeDtypeStruct(pair.shape, f32),
+        ),
+        in_specs=[VMEM] * 2,
+        out_specs=(VMEM,) * 3,
+        name="slots",
+    )(own_routes, pair)
     branch = pl.pallas_call(
         branch_kernel,
         out_shape=jax.ShapeDtypeStruct((QUAD, tokens // QUAD, channels), bf16),
@@ -346,7 +355,7 @@
         in_specs=[VMEM] * 4,
         out_specs=VMEM,
         name="combine",
-    )(stream, returned.reshape(slot_count * PIECES, width // PIECES), column, expert_pair_weight)
+    )(stream, returned.reshape(slot_count * PIECES, width // PIECES), column, pair)
 
 
 def solution(mesh):

time: 236 us -> 234 us (level)
  blocking collectives: 29.4 us -> 50.5 us
  waiting for transfers between devices: 96.4 us -> 84.7 us
  starting transfers between devices: 58.9 us -> 49.1 us
    all_to_all x0 -> x1, blocking collectives: none -> 21.2 us  [layer(): returned = lax.all_to_all(result.reshape(packed), 'sp', 0, 0, tiled=True)]
    all_to_all x1 -> x0, waiting for transfers between devices: 10.9 us -> none  [layer(): returned = lax.all_to_all(result.reshape(packed), 'sp', 0, 0, tiled=True)]
    all_to_all x1 -> x0, starting transfers between devices: 9.84 us -> none  [layer(): returned = lax.all_to_all(result.reshape(packed), 'sp', 0, 0, tiled=True)]
    unnamed x19 -> x15, local copies, waits for them, and re-layouts: 5.47 us -> 3.37 us
  transfers between devices with their start and end apart: 11 -> 10, of which waited for: 7 -> 6; matrix products, arithmetic and copies ran while one was open for 3% -> 3% of each run, Pallas kernels for 3% -> 3%
where the time goes in v7:
time: 234 us; the launch traced here: 230 us
  waiting for transfers between devices  84.7 us (36%)
  blocking collectives  50.5 us (22%)
  starting transfers between devices  49.1 us (21%)
  Pallas kernels  20.4 us (9%)
  between operations  13.2 us (6%)
  local copies, waits for them, and re-layouts  8.69 us (4%)
  other arithmetic  2.94 us (1%)
    reduce_scatter x1, waiting for transfers between devices, layer(): lax.psum_scatter(summed, 'tp', scatter_dimension=0, axis_index_groups=gro...  41.1 us
    all_to_all x1, blocking collectives, layer(): returned = lax.all_to_all(result.reshape(packed), 'sp', 0, 0, tiled=True)  21.2 us
    all_to_all x1, blocking collectives, layer(): arrived = lax.all_to_all(outgoing.reshape(packed), 'sp', 0, 0, tiled=True)  18.4 us
    ppermute x3, starting transfers between devices, swap_cores(): return lax.ppermute(x, 'tp', [(i, i ^ 1) for i in range(size)])  16.2 us
    all_to_all x1, starting transfers between devices, layer(): pieces = lax.all_to_all(total, 'sp', 0, 0, tiled=True)  14.2 us
    all_gather x1, waiting for transfers between devices, layer(): lax.all_gather(arrived, 'tp', axis=0, axis_index_groups=groups, tiled=True)  13.7 us
    all_to_all x1, blocking collectives, layer(): lax.all_to_all(branch, 'tp', 0, 0, axis_index_groups=quads, tiled=True)  11 us
    all_to_all x1, waiting for transfers between devices, layer(): lax.all_to_all(partial.reshape(tp // QUAD, rows_dev, width), 'tp', 0, 0,...  10.5 us
  transfers between devices with their start and end apart: 10, of which 6 were waited for; matrix products, arithmetic and copies ran while one was open for 3% of the time, Pallas kernels for 3%

profile of v7, /device:TPU:1, one launch (start us, length us, event | category | flops | bytes accessed | tf_op | source)
XLA Modules:
  0.0 229.6 jit_solution(15106947931344381547)
XLA Ops:
  6.5 0.0 copy-start
  6.5 0.0 all-gather.3.cloned.1.call-start
  6.5 0.7 all-gather.3.cloned.1.call-update
  7.3 0.7 slice.3
  7.9 3.9 %collective-permute-start = (bf16[3,128]{1,0:T(4,128)(2,1)S(1)}, bf16[3,128]{1,0:T(4,128)(2,1)S(1)}, u32[]{:S(2)}, u32[]{:S(2)}) collective-permute-start(bf16[3,128]{1,0:T(4,128)(2,1)S(1)} %slice.3), channel_id=1, source_target_pairs={{0,16},{16,32},{32,48},{48,64},{64,80},{80,96},{96,112},{112,128},... | collective-permute-start | bytes 2312 | tf_op jit(solution)/shard_map/ppermute | solution.py:26
  11.9 0.7 collective-permute-done.rim_ref
  12.6 0.0 copy-start.6
  12.6 0.6 copy-done.6
  13.2 3.2 %recurrence.1 = (f32[512,128]{1,0:T(8,128)}, f32[512,128]{1,0:T(8,128)}, f32[32,2,128]{2,1,0:T(2,128)}) custom-call(bf16[512,128]{1,0:T(8,128)(2,1)} %x_ref.1, bf16[3,128]{1,0:T(4,128)(2,1)} %copy-done.6, f32[4,128]{1,0:T(4,128)} %filter_ref.1, bf16[2,64,64]{2,1,0:T(8,128)(2,1)} %recur_ref.1, bf16[2,64,64]{2,1,0:T(8,128)(2,1)} %input_ref.1, ...), custom_call_target="tpu_custom_call" | custom-call | flops 1000000000 | bytes 1048576 | tf_op jit(solution)/shard_map/recurrence/pallas_call | solution.py:238
  16.4 14.2 %all-to-all-start = ((f32[32,2,128]{2,1,0:T(2,128)}), f32[32,2,128]{2,1,0:T(2,128)S(1)}, u32[]{:S(2)}, u32[]{:S(2)}) async-start(f32[32,2,128]{2,1,0:T(2,128)} %get-tuple-element.18), calls=%async_computation | async-start | bytes 65536 | tf_op jit(solution)/shard_map/all_to_all | solution.py:265
  30.6 8.7 %all-to-all-done.pieces_ref = f32[32,2,128]{2,1,0:T(2,128)S(1)} async-done(((f32[32,2,128]{2,1,0:T(2,128)}), f32[32,2,128]{2,1,0:T(2,128)S(1)}, u32[]{:S(2)}, u32[]{:S(2)}) %all-to-all-start) | async-done | bytes 32800 | tf_op jit(solution)/shard_map/all_to_all | solution.py:265
  39.3 0.0 copy-start.4
  39.3 0.6 copy-done.4
  39.9 1.9 branch.1
  41.8 0.0 copy-start.5
  41.8 11.0 %all_to_all.30.branch_ref = bf16[4,128,128]{2,1,0:T(8,128)(2,1)} all-to-all(bf16[4,128,128]{2,1,0:T(8,128)(2,1)} %branch.1), channel_id=1, replica_groups={{0,1,2,3},{4,5,6,7},{8,9,10,11},{12,13,14,15},{16,17,18,19},{20,21,22,2..., dimensions={0} | all-to-all | bytes 262144 | tf_op jit(solution)/shard_map/all_to_all | solution.py:286
  52.7 0.0 all-gather.3.cloned.1.call-done.weight_ref
  52.8 2.6 %project.1 = bf16[128,2048]{1,0:T(8,128)(2,1)} custom-call(bf16[4,128,128]{2,1,0:T(8,128)(2,1)} %all_to_all.30.branch_ref, bf16[512,2048]{1,0:T(8,128)(2,1)} %all-gather.3.cloned.1.call-done.weight_ref), custom_call_target="tpu_custom_call" | custom-call | tf_op jit(solution)/shard_map/project/pallas_call | solution.py:288
  55.4 6.8 %all-to-all-start.2 = ((bf16[4,32,2048]{2,1,0:T(8,128)(2,1)}), bf16[4,32,2048]{2,1,0:T(8,128)(2,1)S(1)}, u32[]{:S(2)}, u32[]{:S(2)}) async-start(bf16[4,32,2048]{2,1,0:T(8,128)(2,1)} %bitcast.22), calls=%async_computation.2 | async-start | bytes 1048576 | tf_op jit(solution)/shard_map/all_to_all | solution.py:299
  62.2 0.0 copy-start.2
  62.2 0.0 copy-start.3
  62.2 0.0 all-gather.5.cloned.1.call-start
  62.2 0.0 copy-done
  62.3 0.1 constant_dynamic-slice_fusion
  62.3 0.7 copy.19.routes_ref
  63.0 0.0 copy-done.5
  63.0 0.7 copy.17.weight_ref
  63.7 1.7 slots.1
  65.4 10.5 %all-to-all-done.2.parts_ref = bf16[4,32,2048]{2,1,0:T(8,128)(2,1)S(1)} async-done(((bf16[4,32,2048]{2,1,0:T(8,128)(2,1)}), bf16[4,32,2048]{2,1,0:T(8,128)(2,1)S(1)}, u32[]{:S(2)}, u32[]{:S(2)}) %all-to-all-start.2) | async-done | bytes 524320 | tf_op jit(solution)/shard_map/all_to_all | solution.py:299
  75.9 0.0 copy-start.1
  75.9 0.8 copy-done.1
  76.7 2.4 %dispatch.1 = (bf16[32,2048]{1,0:T(8,128)(2,1)}, bf16[768,256]{1,0:T(8,128)(2,1)}) custom-call(bf16[4,32,2048]{2,1,0:T(8,128)(2,1)} %copy-done.1, bf16[32,2048]{1,0:T(8,128)(2,1)} %resid_ref.1, f32[1,2048]{1,0:T(1,128)} %bitcast.30, s32[2,256]{1,0:T(2,128)} %get-tuple-element.23.line_ref), custom_call_target="tpu_custom_call" | custom-call | tf_op jit(solution)/shard_map/dispatch/pallas_call | solution.py:305
  79.1 18.4 %all_to_all.31 = bf16[32,24,256]{2,1,0:T(8,128)(2,1)S(1)} all-to-all(bf16[32,24,256]{2,1,0:T(8,128)(2,1)} %bitcast.29), channel_id=1, replica_groups=mesh['sp'=32,'tp'=16] {'sp'}, dimensions={0} | all-to-all | bytes 786432 | tf_op jit(solution)/shard_map/all_to_all | solution.py:316
  97.5 0.9 reshape.28
  98.4 0.0 all-gather.5.cloned.1.call-update
  98.4 7.9 %all-to-all-start.4 = ((bf16[8,256,128]{2,1,0:T(8,128)(2,1)}), bf16[8,256,128]{2,1,0:T(8,128)(2,1)S(1)}, u32[]{:S(2)}, u32[]{:S(2)}) async-start(bf16[8,256,128]{2,1,0:T(8,128)(2,1)} %bitcast.8), calls=%async_computation.4 | async-start | bytes 1048576 | tf_op jit(solution)/shard_map/all_to_all | solution.py:324
  106.3 0.0 reduce-scatter.2.cloned.1.call-start
  106.4 0.0 copy-done.2
  106.4 4.8 %collective-permute-start.1 = (bf16[2048,128]{1,0:T(8,128)(2,1)S(1)}, bf16[2048,128]{1,0:T(8,128)(2,1)S(1)}, u32[]{:S(2)}, u32[]{:S(2)}) collective-permute-start(bf16[2048,128]{1,0:T(8,128)(2,1)S(1)} %bitcast.24), channel_id=1, source_target_pairs={{0,1},{1,0},{2,3},{3,2},{4,5},{5,4},{6,7},{7,6},{8,9},{9,8},{10,11... | collective-permute-start | bytes 1572872 | tf_op jit(solution)/shard_map/ppermute | solution.py:35
  111.1 0.0 copy-done.3
  111.1 1.9 collective-permute-start.2
  113.1 9.4 %all-to-all-done.4 = bf16[8,256,128]{2,1,0:T(8,128)(2,1)S(1)} async-done(((bf16[8,256,128]{2,1,0:T(8,128)(2,1)}), bf16[8,256,128]{2,1,0:T(8,128)(2,1)S(1)}, u32[]{:S(2)}, u32[]{:S(2)}) %all-to-all-start.4) | async-done | bytes 524320 | tf_op jit(solution)/shard_map/all_to_all | solution.py:324
  122.5 9.5 %collective-permute-start.3 = (bf16[8,256,128]{2,1,0:T(8,128)(2,1)S(1)}, bf16[8,256,128]{2,1,0:T(8,128)(2,1)S(1)}, u32[]{:S(2)}, u32[]{:S(2)}) collective-permute-start(bf16[8,256,128]{2,1,0:T(8,128)(2,1)S(1)} %all-to-all-done.4), channel_id=1, source_target_pairs={{0,1},{1,0},{2,3},{3,2},{4,5},{5,4},{6,7},{7,6},{8,9},{9,8},{10,11... | collective-permute-start | bytes 1572872 | tf_op jit(solution)/shard_map/ppermute | solution.py:35
  132.0 0.0 collective-permute-done.1
  132.0 1.3 maximum_select_fusion.gate_ref
  133.3 0.0 collective-permute-done.2
  133.3 1.4 maximum_select_fusion.1.up_ref
  134.7 0.0 collective-permute-done.3
  134.8 0.2 maximum_select_fusion.2
  134.9 1.1 copy.18
  136.0 1.3 copy.22
  137.4 13.7 %all-gather.5.cloned.1.call-done.rows_ref = bf16[768,2048]{1,0:T(8,128)(2,1)} async-done(((bf16[96,2048]{1,0:T(8,128)(2,1)}), bf16[768,2048]{1,0:T(8,128)(2,1)}) %all-gather.5.cloned.1.call-update) | async-done | bytes 3145744 | tf_op jit(solution)/shard_map/all_gather | solution.py:319
  151.1 6.5 %experts.1 = bf16[768,2048]{1,0:T(8,128)(2,1)} custom-call(bf16[768,2048]{1,0:T(8,128)(2,1)} %all-gather.5.cloned.1.call-done.rows_ref, bf16[2048,256]{1,0:T(8,128)(2,1)} %maximum_select_fusion.gate_ref, bf16[2048,256]{1,0:T(8,128)(2,1)} %maximum_select_fusion.1.up_ref, bf16[256,2048]{1,0:T(8,128)(2,1)} %bitcast.19), custom_call_target="tpu_custom_call" | custom-call | tf_op jit(solution)/shard_map/experts/pallas_call | solution.py:334
  157.5 0.0 reduce-scatter.2.cloned.1.call-update
  157.5 41.1 %reduce-scatter.2.cloned.1.call-done = bf16[96,2048]{1,0:T(8,128)(2,1)} async-done(((bf16[768,2048]{1,0:T(8,128)(2,1)}), bf16[96,2048]{1,0:T(8,128)(2,1)}) %reduce-scatter.2.cloned.1.call-update) | async-done | bytes 393232 | tf_op jit(solution)/shard_map/reduce_scatter | solution.py:347
  198.6 1.2 reshape.31
  199.8 21.2 %all_to_all.32 = bf16[32,24,256]{2,1,0:T(8,128)(2,1)} all-to-all(bf16[32,24,256]{2,1,0:T(8,128)(2,1)S(1)} %reshape.31), channel_id=1, replica_groups=mesh['sp'=32,'tp'=16] {'sp'}, dimensions={0} | all-to-all | bytes 786432 | tf_op jit(solution)/shard_map/all_to_all | solution.py:351
  221.0 2.1 combine.1
Async XLA Ops:
  6.5 55.7 %copy-start = (s32[512,2]{0,1:T(2,128)S(1)}, s32[512,2]{0,1:T(2,128)}, u32[]{:S(2)}) copy-start(s32[512,2]{0,1:T(2,128)} %param.25) | copy-start | bytes 12292
  6.5 46.2 %all-gather.3.cloned.1.call-start = ((), (), s32[]{:S(2)}) async-start(), calls=%async_computation.7 | async-start | bytes 2621440 | tf_op jit(solution)/shard_map/all_gather | solution.py:234
  7.9 4.6 %collective-permute-start = (bf16[3,128]{1,0:T(4,128)(2,1)S(1)}, bf16[3,128]{1,0:T(4,128)(2,1)S(1)}, u32[]{:S(2)}, u32[]{:S(2)}) collective-permute-start(bf16[3,128]{1,0:T(4,128)(2,1)S(1)} %slice.3), channel_id=1, source_target_pairs={{0,16},{16,32},{32,48},{48,64},{64,80},{80,96},{96,112},{112,128},... | collective-permute-start | bytes 2312 | tf_op jit(solution)/shard_map/ppermute | solution.py:26
  12.6 0.6 copy-start.6
  16.4 22.9 %all-to-all-start = ((f32[32,2,128]{2,1,0:T(2,128)}), f32[32,2,128]{2,1,0:T(2,128)S(1)}, u32[]{:S(2)}, u32[]{:S(2)}) async-start(f32[32,2,128]{2,1,0:T(2,128)} %get-tuple-element.18), calls=%async_computation | async-start | bytes 65536 | tf_op jit(solution)/shard_map/all_to_all | solution.py:265
  39.3 0.6 copy-start.4
  41.8 21.2 %copy-start.5 = (f32[32,2]{0,1:T(2,128)S(1)}, f32[32,2]{0,1:T(2,128)}, u32[]{:S(2)}) copy-start(f32[32,2]{0,1:T(2,128)} %param.26) | copy-start | bytes 772
  55.4 20.5 %all-to-all-start.2 = ((bf16[4,32,2048]{2,1,0:T(8,128)(2,1)}), bf16[4,32,2048]{2,1,0:T(8,128)(2,1)S(1)}, u32[]{:S(2)}, u32[]{:S(2)}) async-start(bf16[4,32,2048]{2,1,0:T(8,128)(2,1)} %bitcast.22), calls=%async_computation.2 | async-start | bytes 1048576 | tf_op jit(solution)/shard_map/all_to_all | solution.py:299
  62.2 44.2 %copy-start.2 = (bf16[1,2048,128]{2,1,0:T(8,128)(2,1)S(1)}, bf16[1,2048,128]{2,1,0:T(8,128)(2,1)}, u32[]{:S(2)}) copy-start(bf16[1,2048,128]{2,1,0:T(8,128)(2,1)} %param.27) | copy-start | bytes 1572868
  62.2 48.9 %copy-start.3 = (bf16[1,2048,128]{2,1,0:T(8,128)(2,1)S(1)}, bf16[1,2048,128]{2,1,0:T(8,128)(2,1)}, u32[]{:S(2)}) copy-start(bf16[1,2048,128]{2,1,0:T(8,128)(2,1)} %param.28) | copy-start | bytes 1572868
  62.2 88.9 %all-gather.5.cloned.1.call-start = ((), (), s32[]{:S(2)}) async-start(), calls=%async_computation.8 | async-start | bytes 3538944 | tf_op jit(solution)/shard_map/all_gather | solution.py:319
  75.9 0.8 copy-start.1
  98.4 24.0 %all-to-all-start.4 = ((bf16[8,256,128]{2,1,0:T(8,128)(2,1)}), bf16[8,256,128]{2,1,0:T(8,128)(2,1)S(1)}, u32[]{:S(2)}, u32[]{:S(2)}) async-start(bf16[8,256,128]{2,1,0:T(8,128)(2,1)} %bitcast.8), calls=%async_computation.4 | async-start | bytes 1048576 | tf_op jit(solution)/shard_map/all_to_all | solution.py:324
  106.3 92.3 %reduce-scatter.2.cloned.1.call-start = ((), (), s32[]{:S(2)}) async-start(), calls=%async_computation.9 | async-start | bytes 3538944 | tf_op jit(solution)/shard_map/reduce_scatter | solution.py:347
  106.4 25.6 %collective-permute-start.1 = (bf16[2048,128]{1,0:T(8,128)(2,1)S(1)}, bf16[2048,128]{1,0:T(8,128)(2,1)S(1)}, u32[]{:S(2)}, u32[]{:S(2)}) collective-permute-start(bf16[2048,128]{1,0:T(8,128)(2,1)S(1)} %bitcast.24), channel_id=1, source_target_pairs={{0,1},{1,0},{2,3},{3,2},{4,5},{5,4},{6,7},{7,6},{8,9},{9,8},{10,11... | collective-permute-start | bytes 1572872 | tf_op jit(solution)/shard_map/ppermute | solution.py:35
  111.1 22.2 %collective-permute-start.2 = (bf16[2048,128]{1,0:T(8,128)(2,1)S(1)}, bf16[2048,128]{1,0:T(8,128)(2,1)S(1)}, u32[]{:S(2)}, u32[]{:S(2)}) collective-permute-start(bf16[2048,128]{1,0:T(8,128)(2,1)S(1)} %bitcast.26), channel_id=1, source_target_pairs={{0,1},{1,0},{2,3},{3,2},{4,5},{5,4},{6,7},{7,6},{8,9},{9,8},{10,11... | collective-permute-start | bytes 1572872 | tf_op jit(solution)/shard_map/ppermute | solution.py:35
  122.5 12.3 %collective-permute-start.3 = (bf16[8,256,128]{2,1,0:T(8,128)(2,1)S(1)}, bf16[8,256,128]{2,1,0:T(8,128)(2,1)S(1)}, u32[]{:S(2)}, u32[]{:S(2)}) collective-permute-start(bf16[8,256,128]{2,1,0:T(8,128)(2,1)S(1)} %all-to-all-done.4), channel_id=1, source_target_pairs={{0,1},{1,0},{2,3},{3,2},{4,5},{5,4},{6,7},{7,6},{8,9},{9,8},{10,11... | collective-permute-start | bytes 1572872 | tf_op jit(solution)/shard_map/ppermute | solution.py:35
Sparse Core Ops, SparseCore 0:
  9.4 40.3 all-gather.2
  98.5 52.4 all-gather.4
  157.7 40.8 reduce-scatter.1

commit v8 on v7

--- a/solution.py
+++ b/solution.py
@@ -11,6 +11,7 @@
 SEGMENTS = 8
 CORES = 2
 CAP = 3
+RIM = 16
 QUAD = 4
 EXPERT_STEPS = 2
 PIECES = 8
@@ -40,6 +41,11 @@
     for k in (6, 5, 4, 3, 2):
         series = 1.0 + x * (1.0 / k) * series
     return jnp.where(x > -0.35, -x * series, 1.0 - jnp.exp(x))
+
+
+def log_one_plus(x):
+    series = 1.0 - x * (1.0 / 2.0 - x * (1.0 / 3.0 - x * (1.0 / 4.0 - x * (1.0 / 5.0))))
+    return jnp.where(x < 0.02, x * series, jnp.log1p(x))
 
 
 def recurrence_kernel(
@@ -55,7 +61,7 @@
             low = k * wide
             gates[low : low + wide, at + low : at + low + wide] = matrix[k]
     lead = 8
-    ext[lead - taps + 1 : lead, :] = rim_ref[...].astype(jnp.float32)
+    ext[0:lead, :] = rim_ref[RIM - lead : RIM, :].astype(jnp.float32)
     ext[lead : lead + tokens, :] = x_ref[...].astype(jnp.float32)
     first = lead - taps + 1
     mixed = ext[first : first + tokens, :] * filter_ref[0:1, :]
@@ -65,7 +71,7 @@
     logits = jnp.dot(smoothed, gates[...], preferred_element_type=jnp.float32)
     both = jax.nn.sigmoid(logits)
     minus_raw = -raw_ref[...]
-    soft = jnp.maximum(minus_raw, 0.0) + jnp.log1p(jnp.exp(-jnp.abs(minus_raw)))
+    soft = jnp.maximum(minus_raw, 0.0) + log_one_plus(jnp.exp(-jnp.abs(minus_raw)))
     log_decay = both[:, :channels] * (-RECURRENT_SCALE * soft) + boost_ref[...]
     decay[...] = jnp.exp(log_decay)
     drive[...] = jnp.sqrt(minus_expm1(2.0 * log_decay)) * (
@@ -219,7 +225,6 @@
     down_weight,
 ):
     tokens, channels = recurrent_input.shape
-    taps = filter_weight.shape[0]
     tp, experts = lax.axis_size("tp"), lax.axis_size("sp")
     here, place = lax.axis_index("tp"), lax.axis_index("sp")
     core = here % CORES
@@ -228,22 +233,29 @@
     rows_dev, width = resid.shape
     f32, bf16 = jnp.float32, jnp.bfloat16
 
-    rim = shifted(recurrent_input[tokens - taps + 1 :], "sp", 1)
+    before = shifted(recurrent_input[tokens - RIM :], "sp", 1)
     quads = [[k * QUAD + i for i in range(QUAD)] for k in range(tp // QUAD)]
     strides = [[k * QUAD + i for k in range(tp // QUAD)] for i in range(QUAD)]
     projection = lax.all_gather(
         output_projection_weight, "tp", axis=0, axis_index_groups=quads, tiled=True
     )
 
+    whole = lambda *shape: pl.BlockSpec(shape, lambda k: (0,) * len(shape))
+    operands = (
+        recurrent_input,
+        before,
+        filter_weight,
+        recurrence_gate_matrix,
+        input_gate_matrix,
+        channel_decay_raw[None, :],
+        token_decay_boost,
+    )
+    shapes = ((tokens, channels), (tokens, channels), (experts, 2, channels))
     state, running, total = pl.pallas_call(
         recurrence_kernel,
-        out_shape=(
-            jax.ShapeDtypeStruct((tokens, channels), f32),
-            jax.ShapeDtypeStruct((tokens, channels), f32),
-            jax.ShapeDtypeStruct((experts, 2, channels), f32),
-        ),
-        in_specs=[VMEM] * 7,
-        out_specs=(VMEM,) * 3,
+        out_shape=tuple(jax.ShapeDtypeStruct(shape, f32) for shape in shapes),
+        in_specs=[VMEM] * len(operands),
+        out_specs=(VMEM,) * len(shapes),
         scratch_shapes=[
             pltpu.VMEM((tokens + 8, channels), f32),
             pltpu.VMEM((tokens, channels), f32),
@@ -252,15 +264,7 @@
         ],
         cost_estimate=pl.CostEstimate(flops=10**9, bytes_accessed=2**20, transcendentals=0),
         name="recurrence",
-    )(
-        recurrent_input,
-        rim,
-        filter_weight,
-        recurrence_gate_matrix,
-        input_gate_matrix,
-        channel_decay_raw[None, :],
-        token_decay_boost,
-    )
+    )(*operands)
 
     pieces = lax.all_to_all(total, "sp", 0, 0, tiled=True)
     own_routes = lax.dynamic_slice_in_dim(routes, here * rows_dev, rows_dev, 0)
@@ -301,7 +305,6 @@
         axis_index_groups=strides, tiled=True,
     )
     slot_count = experts * CAP
-    whole = lambda *shape: pl.BlockSpec(shape, lambda k: (0,) * len(shape))
     stream, outgoing = pl.pallas_call(
         dispatch_kernel,
         out_shape=(

time: 234 us -> 234 us (level)
  no operation moved by 1% of the time
where the time goes in v8:
time: 234 us; the launch traced here: 230 us
  waiting for transfers between devices  84.8 us (36%)
  blocking collectives  50.5 us (22%)
  starting transfers between devices  49.1 us (21%)
  Pallas kernels  20.4 us (9%)
  between operations  13.2 us (6%)
  local copies, waits for them, and re-layouts  8.7 us (4%)
  other arithmetic  2.94 us (1%)
    reduce_scatter x1, waiting for transfers between devices, layer(): lax.psum_scatter(summed, 'tp', scatter_dimension=0, axis_index_groups=gro...  41.1 us
    all_to_all x1, blocking collectives, layer(): returned = lax.all_to_all(result.reshape(packed), 'sp', 0, 0, tiled=True)  21.2 us
    all_to_all x1, blocking collectives, layer(): arrived = lax.all_to_all(outgoing.reshape(packed), 'sp', 0, 0, tiled=True)  18.3 us
    ppermute x3, starting transfers between devices, swap_cores(): return lax.ppermute(x, 'tp', [(i, i ^ 1) for i in range(size)])  16.2 us
    all_to_all x1, starting transfers between devices, layer(): pieces = lax.all_to_all(total, 'sp', 0, 0, tiled=True)  14.2 us
    all_gather x1, waiting for transfers between devices, layer(): lax.all_gather(arrived, 'tp', axis=0, axis_index_groups=groups, tiled=True)  13.7 us
    all_to_all x1, blocking collectives, layer(): lax.all_to_all(branch, 'tp', 0, 0, axis_index_groups=quads, tiled=True)  11 us
    all_to_all x1, waiting for transfers between devices, layer(): lax.all_to_all(partial.reshape(tp // QUAD, rows_dev, width), 'tp', 0, 0,...  10.5 us
  transfers between devices with their start and end apart: 10, of which 6 were waited for; matrix products, arithmetic and copies ran while one was open for 3% of the time, Pallas kernels for 3%

profile of v8, /device:TPU:1, one launch (start us, length us, event | category | flops | bytes accessed | tf_op | source)
XLA Modules:
  0.0 229.6 jit_solution(15543267760345584723)
XLA Ops:
  6.5 0.0 copy-start
  6.5 0.0 all-gather.3.cloned.1.call-start
  6.5 0.7 all-gather.3.cloned.1.call-update
  7.3 0.7 slice.3
  8.0 3.9 %collective-permute-start = (bf16[16,128]{1,0:T(8,128)(2,1)S(1)}, bf16[16,128]{1,0:T(8,128)(2,1)S(1)}, u32[]{:S(2)}, u32[]{:S(2)}) collective-permute-start(bf16[16,128]{1,0:T(8,128)(2,1)S(1)} %slice.3), channel_id=1, source_target_pairs={{0,16},{16,32},{32,48},{48,64},{64,80},{80,96},{96,112},{112,128},... | collective-permute-start | bytes 12296 | tf_op jit(solution)/shard_map/ppermute | solution.py:27
  11.9 0.7 collective-permute-done.rim_ref
  12.6 0.0 copy-start.6
  12.6 0.6 copy-done.6
  13.2 3.2 %recurrence.1 = (f32[512,128]{1,0:T(8,128)}, f32[512,128]{1,0:T(8,128)}, f32[32,2,128]{2,1,0:T(2,128)}) custom-call(bf16[512,128]{1,0:T(8,128)(2,1)} %x_ref.1, bf16[16,128]{1,0:T(8,128)(2,1)} %copy-done.6, f32[4,128]{1,0:T(4,128)} %filter_ref.1, bf16[2,64,64]{2,1,0:T(8,128)(2,1)} %recur_ref.1, bf16[2,64,64]{2,1,0:T(8,128)(2,1)} %input_ref.1, ...), custom_call_target="tpu_custom_call" | custom-call | flops 1000000000 | bytes 1048576 | tf_op jit(solution)/shard_map/recurrence/pallas_call | solution.py:254
  16.4 14.2 %all-to-all-start = ((f32[32,2,128]{2,1,0:T(2,128)}), f32[32,2,128]{2,1,0:T(2,128)S(1)}, u32[]{:S(2)}, u32[]{:S(2)}) async-start(f32[32,2,128]{2,1,0:T(2,128)} %get-tuple-element.18), calls=%async_computation | async-start | bytes 65536 | tf_op jit(solution)/shard_map/all_to_all | solution.py:269
  30.6 8.7 %all-to-all-done.pieces_ref = f32[32,2,128]{2,1,0:T(2,128)S(1)} async-done(((f32[32,2,128]{2,1,0:T(2,128)}), f32[32,2,128]{2,1,0:T(2,128)S(1)}, u32[]{:S(2)}, u32[]{:S(2)}) %all-to-all-start) | async-done | bytes 32800 | tf_op jit(solution)/shard_map/all_to_all | solution.py:269
  39.3 0.0 copy-start.4
  39.3 0.6 copy-done.4
  39.9 1.9 branch.1
  41.8 0.0 copy-start.5
  41.8 11.0 %all_to_all.30.branch_ref = bf16[4,128,128]{2,1,0:T(8,128)(2,1)} all-to-all(bf16[4,128,128]{2,1,0:T(8,128)(2,1)} %branch.1), channel_id=1, replica_groups={{0,1,2,3},{4,5,6,7},{8,9,10,11},{12,13,14,15},{16,17,18,19},{20,21,22,2..., dimensions={0} | all-to-all | bytes 262144 | tf_op jit(solution)/shard_map/all_to_all | solution.py:290
  52.8 0.0 all-gather.3.cloned.1.call-done.weight_ref
  52.8 2.6 %project.1 = bf16[128,2048]{1,0:T(8,128)(2,1)} custom-call(bf16[4,128,128]{2,1,0:T(8,128)(2,1)} %all_to_all.30.branch_ref, bf16[512,2048]{1,0:T(8,128)(2,1)} %all-gather.3.cloned.1.call-done.weight_ref), custom_call_target="tpu_custom_call" | custom-call | tf_op jit(solution)/shard_map/project/pallas_call | solution.py:292
  55.4 6.8 %all-to-all-start.2 = ((bf16[4,32,2048]{2,1,0:T(8,128)(2,1)}), bf16[4,32,2048]{2,1,0:T(8,128)(2,1)S(1)}, u32[]{:S(2)}, u32[]{:S(2)}) async-start(bf16[4,32,2048]{2,1,0:T(8,128)(2,1)} %bitcast.22), calls=%async_computation.2 | async-start | bytes 1048576 | tf_op jit(solution)/shard_map/all_to_all | solution.py:303
  62.2 0.0 copy-start.2
  62.2 0.0 copy-start.3
  62.2 0.0 all-gather.5.cloned.1.call-start
  62.3 0.0 copy-done
  62.3 0.1 constant_dynamic-slice_fusion
  62.4 0.7 copy.19.routes_ref
  63.1 0.0 copy-done.5
  63.1 0.7 copy.17.weight_ref
  63.8 1.7 slots.1
  65.5 10.5 %all-to-all-done.2.parts_ref = bf16[4,32,2048]{2,1,0:T(8,128)(2,1)S(1)} async-done(((bf16[4,32,2048]{2,1,0:T(8,128)(2,1)}), bf16[4,32,2048]{2,1,0:T(8,128)(2,1)S(1)}, u32[]{:S(2)}, u32[]{:S(2)}) %all-to-all-start.2) | async-done | bytes 524320 | tf_op jit(solution)/shard_map/all_to_all | solution.py:303
  75.9 0.0 copy-start.1
  75.9 0.8 copy-done.1
  76.7 2.4 %dispatch.1 = (bf16[32,2048]{1,0:T(8,128)(2,1)}, bf16[768,256]{1,0:T(8,128)(2,1)}) custom-call(bf16[4,32,2048]{2,1,0:T(8,128)(2,1)} %copy-done.1, bf16[32,2048]{1,0:T(8,128)(2,1)} %resid_ref.1, f32[1,2048]{1,0:T(1,128)} %bitcast.30, s32[2,256]{1,0:T(2,128)} %get-tuple-element.23.line_ref), custom_call_target="tpu_custom_call" | custom-call | tf_op jit(solution)/shard_map/dispatch/pallas_call | solution.py:308
  79.1 18.3 %all_to_all.31 = bf16[32,24,256]{2,1,0:T(8,128)(2,1)S(1)} all-to-all(bf16[32,24,256]{2,1,0:T(8,128)(2,1)} %bitcast.29), channel_id=1, replica_groups=mesh['sp'=32,'tp'=16] {'sp'}, dimensions={0} | all-to-all | bytes 786432 | tf_op jit(solution)/shard_map/all_to_all | solution.py:319
  97.5 0.9 reshape.28
  98.4 0.0 all-gather.5.cloned.1.call-update
  98.4 7.9 %all-to-all-start.4 = ((bf16[8,256,128]{2,1,0:T(8,128)(2,1)}), bf16[8,256,128]{2,1,0:T(8,128)(2,1)S(1)}, u32[]{:S(2)}, u32[]{:S(2)}) async-start(bf16[8,256,128]{2,1,0:T(8,128)(2,1)} %bitcast.8), calls=%async_computation.4 | async-start | bytes 1048576 | tf_op jit(solution)/shard_map/all_to_all | solution.py:327
  106.3 0.0 reduce-scatter.2.cloned.1.call-start
  106.4 0.0 copy-done.2
  106.4 4.8 %collective-permute-start.1 = (bf16[2048,128]{1,0:T(8,128)(2,1)S(1)}, bf16[2048,128]{1,0:T(8,128)(2,1)S(1)}, u32[]{:S(2)}, u32[]{:S(2)}) collective-permute-start(bf16[2048,128]{1,0:T(8,128)(2,1)S(1)} %bitcast.24), channel_id=1, source_target_pairs={{0,1},{1,0},{2,3},{3,2},{4,5},{5,4},{6,7},{7,6},{8,9},{9,8},{10,11... | collective-permute-start | bytes 1572872 | tf_op jit(solution)/shard_map/ppermute | solution.py:36
  111.1 0.0 copy-done.3
  111.1 1.9 collective-permute-start.2
  113.1 9.4 %all-to-all-done.4 = bf16[8,256,128]{2,1,0:T(8,128)(2,1)S(1)} async-done(((bf16[8,256,128]{2,1,0:T(8,128)(2,1)}), bf16[8,256,128]{2,1,0:T(8,128)(2,1)S(1)}, u32[]{:S(2)}, u32[]{:S(2)}) %all-to-all-start.4) | async-done | bytes 524320 | tf_op jit(solution)/shard_map/all_to_all | solution.py:327
  122.5 9.5 %collective-permute-start.3 = (bf16[8,256,128]{2,1,0:T(8,128)(2,1)S(1)}, bf16[8,256,128]{2,1,0:T(8,128)(2,1)S(1)}, u32[]{:S(2)}, u32[]{:S(2)}) collective-permute-start(bf16[8,256,128]{2,1,0:T(8,128)(2,1)S(1)} %all-to-all-done.4), channel_id=1, source_target_pairs={{0,1},{1,0},{2,3},{3,2},{4,5},{5,4},{6,7},{7,6},{8,9},{9,8},{10,11... | collective-permute-start | bytes 1572872 | tf_op jit(solution)/shard_map/ppermute | solution.py:36
  132.0 0.0 collective-permute-done.1
  132.0 1.3 maximum_select_fusion.gate_ref
  133.3 0.0 collective-permute-done.2
  133.3 1.4 maximum_select_fusion.1.up_ref
  134.7 0.0 collective-permute-done.3
  134.8 0.2 maximum_select_fusion.2
  134.9 1.1 copy.18
  136.0 1.3 copy.22
  137.4 13.7 %all-gather.5.cloned.1.call-done.rows_ref = bf16[768,2048]{1,0:T(8,128)(2,1)} async-done(((bf16[96,2048]{1,0:T(8,128)(2,1)}), bf16[768,2048]{1,0:T(8,128)(2,1)}) %all-gather.5.cloned.1.call-update) | async-done | bytes 3145744 | tf_op jit(solution)/shard_map/all_gather | solution.py:322
  151.1 6.5 %experts.1 = bf16[768,2048]{1,0:T(8,128)(2,1)} custom-call(bf16[768,2048]{1,0:T(8,128)(2,1)} %all-gather.5.cloned.1.call-done.rows_ref, bf16[2048,256]{1,0:T(8,128)(2,1)} %maximum_select_fusion.gate_ref, bf16[2048,256]{1,0:T(8,128)(2,1)} %maximum_select_fusion.1.up_ref, bf16[256,2048]{1,0:T(8,128)(2,1)} %bitcast.19), custom_call_target="tpu_custom_call" | custom-call | tf_op jit(solution)/shard_map/experts/pallas_call | solution.py:337
  157.5 0.0 reduce-scatter.2.cloned.1.call-update
  157.5 41.1 %reduce-scatter.2.cloned.1.call-done = bf16[96,2048]{1,0:T(8,128)(2,1)} async-done(((bf16[768,2048]{1,0:T(8,128)(2,1)}), bf16[96,2048]{1,0:T(8,128)(2,1)}) %reduce-scatter.2.cloned.1.call-update) | async-done | bytes 393232 | tf_op jit(solution)/shard_map/reduce_scatter | solution.py:350
  198.6 1.2 reshape.31
  199.8 21.2 %all_to_all.32 = bf16[32,24,256]{2,1,0:T(8,128)(2,1)} all-to-all(bf16[32,24,256]{2,1,0:T(8,128)(2,1)S(1)} %reshape.31), channel_id=1, replica_groups=mesh['sp'=32,'tp'=16] {'sp'}, dimensions={0} | all-to-all | bytes 786432 | tf_op jit(solution)/shard_map/all_to_all | solution.py:354
  221.0 2.1 combine.1
Async XLA Ops:
  6.5 55.8 %copy-start = (s32[512,2]{0,1:T(2,128)S(1)}, s32[512,2]{0,1:T(2,128)}, u32[]{:S(2)}) copy-start(s32[512,2]{0,1:T(2,128)} %param.25) | copy-start | bytes 12292
  6.5 46.2 %all-gather.3.cloned.1.call-start = ((), (), s32[]{:S(2)}) async-start(), calls=%async_computation.7 | async-start | bytes 2621440 | tf_op jit(solution)/shard_map/all_gather | solution.py:239
  8.0 4.7 %collective-permute-start = (bf16[16,128]{1,0:T(8,128)(2,1)S(1)}, bf16[16,128]{1,0:T(8,128)(2,1)S(1)}, u32[]{:S(2)}, u32[]{:S(2)}) collective-permute-start(bf16[16,128]{1,0:T(8,128)(2,1)S(1)} %slice.3), channel_id=1, source_target_pairs={{0,16},{16,32},{32,48},{48,64},{64,80},{80,96},{96,112},{112,128},... | collective-permute-start | bytes 12296 | tf_op jit(solution)/shard_map/ppermute | solution.py:27
  12.6 0.6 copy-start.6
  16.4 22.9 %all-to-all-start = ((f32[32,2,128]{2,1,0:T(2,128)}), f32[32,2,128]{2,1,0:T(2,128)S(1)}, u32[]{:S(2)}, u32[]{:S(2)}) async-start(f32[32,2,128]{2,1,0:T(2,128)} %get-tuple-element.18), calls=%async_computation | async-start | bytes 65536 | tf_op jit(solution)/shard_map/all_to_all | solution.py:269
  39.3 0.6 copy-start.4
  41.8 21.2 %copy-start.5 = (f32[32,2]{0,1:T(2,128)S(1)}, f32[32,2]{0,1:T(2,128)}, u32[]{:S(2)}) copy-start(f32[32,2]{0,1:T(2,128)} %param.26) | copy-start | bytes 772
  55.4 20.5 %all-to-all-start.2 = ((bf16[4,32,2048]{2,1,0:T(8,128)(2,1)}), bf16[4,32,2048]{2,1,0:T(8,128)(2,1)S(1)}, u32[]{:S(2)}, u32[]{:S(2)}) async-start(bf16[4,32,2048]{2,1,0:T(8,128)(2,1)} %bitcast.22), calls=%async_computation.2 | async-start | bytes 1048576 | tf_op jit(solution)/shard_map/all_to_all | solution.py:303
  62.2 44.1 %copy-start.2 = (bf16[1,2048,128]{2,1,0:T(8,128)(2,1)S(1)}, bf16[1,2048,128]{2,1,0:T(8,128)(2,1)}, u32[]{:S(2)}) copy-start(bf16[1,2048,128]{2,1,0:T(8,128)(2,1)} %param.27) | copy-start | bytes 1572868
  62.2 48.9 %copy-start.3 = (bf16[1,2048,128]{2,1,0:T(8,128)(2,1)S(1)}, bf16[1,2048,128]{2,1,0:T(8,128)(2,1)}, u32[]{:S(2)}) copy-start(bf16[1,2048,128]{2,1,0:T(8,128)(2,1)} %param.28) | copy-start | bytes 1572868
  62.2 88.8 %all-gather.5.cloned.1.call-start = ((), (), s32[]{:S(2)}) async-start(), calls=%async_computation.8 | async-start | bytes 3538944 | tf_op jit(solution)/shard_map/all_gather | solution.py:322
  75.9 0.8 copy-start.1
  98.4 24.0 %all-to-all-start.4 = ((bf16[8,256,128]{2,1,0:T(8,128)(2,1)}), bf16[8,256,128]{2,1,0:T(8,128)(2,1)S(1)}, u32[]{:S(2)}, u32[]{:S(2)}) async-start(bf16[8,256,128]{2,1,0:T(8,128)(2,1)} %bitcast.8), calls=%async_computation.4 | async-start | bytes 1048576 | tf_op jit(solution)/shard_map/all_to_all | solution.py:327
  106.3 92.3 %reduce-scatter.2.cloned.1.call-start = ((), (), s32[]{:S(2)}) async-start(), calls=%async_computation.9 | async-start | bytes 3538944 | tf_op jit(solution)/shard_map/reduce_scatter | solution.py:350
  106.4 25.6 %collective-permute-start.1 = (bf16[2048,128]{1,0:T(8,128)(2,1)S(1)}, bf16[2048,128]{1,0:T(8,128)(2,1)S(1)}, u32[]{:S(2)}, u32[]{:S(2)}) collective-permute-start(bf16[2048,128]{1,0:T(8,128)(2,1)S(1)} %bitcast.24), channel_id=1, source_target_pairs={{0,1},{1,0},{2,3},{3,2},{4,5},{5,4},{6,7},{7,6},{8,9},{9,8},{10,11... | collective-permute-start | bytes 1572872 | tf_op jit(solution)/shard_map/ppermute | solution.py:36
  111.1 22.2 %collective-permute-start.2 = (bf16[2048,128]{1,0:T(8,128)(2,1)S(1)}, bf16[2048,128]{1,0:T(8,128)(2,1)S(1)}, u32[]{:S(2)}, u32[]{:S(2)}) collective-permute-start(bf16[2048,128]{1,0:T(8,128)(2,1)S(1)} %bitcast.26), channel_id=1, source_target_pairs={{0,1},{1,0},{2,3},{3,2},{4,5},{5,4},{6,7},{7,6},{8,9},{9,8},{10,11... | collective-permute-start | bytes 1572872 | tf_op jit(solution)/shard_map/ppermute | solution.py:36
  122.5 12.3 %collective-permute-start.3 = (bf16[8,256,128]{2,1,0:T(8,128)(2,1)S(1)}, bf16[8,256,128]{2,1,0:T(8,128)(2,1)S(1)}, u32[]{:S(2)}, u32[]{:S(2)}) collective-permute-start(bf16[8,256,128]{2,1,0:T(8,128)(2,1)S(1)} %all-to-all-done.4), channel_id=1, source_target_pairs={{0,1},{1,0},{2,3},{3,2},{4,5},{5,4},{6,7},{7,6},{8,9},{9,8},{10,11... | collective-permute-start | bytes 1572872 | tf_op jit(solution)/shard_map/ppermute | solution.py:36
Sparse Core Ops, SparseCore 0:
  9.4 40.3 all-gather.2
  98.5 52.4 all-gather.4
  157.7 40.8 reduce-scatter.1

commit v9 on v8

--- a/solution.py
+++ b/solution.py
@@ -228,7 +228,6 @@
     tp, experts = lax.axis_size("tp"), lax.axis_size("sp")
     here, place = lax.axis_index("tp"), lax.axis_index("sp")
     core = here % CORES
-    chips = tp // CORES
     groups = core_groups(tp)
     rows_dev, width = resid.shape
     f32, bf16 = jnp.float32, jnp.bfloat16
@@ -267,6 +266,7 @@
     )(*operands)
 
     pieces = lax.all_to_all(total, "sp", 0, 0, tiled=True)
+    down_all = lax.all_gather(down_weight[0], "tp", axis_index_groups=groups)
     own_routes = lax.dynamic_slice_in_dim(routes, here * rows_dev, rows_dev, 0)
     own_routes, pair = lax.optimization_barrier((own_routes, expert_pair_weight, total))[:2]
     column, line, pair = pl.pallas_call(
@@ -320,13 +320,12 @@
     arrived = arrived.reshape(slot_count, width)
 
     rows = lax.all_gather(arrived, "tp", axis=0, axis_index_groups=groups, tiled=True)
-    arrived, down_part, gate_own, up_own = lax.optimization_barrier(
-        (arrived, down_weight[0], gate_weight[0], up_weight[0])
+    arrived, down_all, gate_own, up_own = lax.optimization_barrier(
+        (arrived, down_all, gate_weight[0], up_weight[0])
     )
     hidden = gate_own.shape[1]
-    down_own = lax.all_to_all(
-        down_part.reshape(chips, CORES * hidden, -1), "tp", 0, 0,
-        axis_index_groups=groups, tiled=True,
+    down_own = lax.dynamic_slice_in_dim(
+        down_all, here // CORES * CORES * hidden, CORES * hidden, 1
     )
     gate = natural(gate_own, swap_cores(gate_own), core, 1)
     upward = natural(up_own, swap_cores(up_own), core, 1)

time: 234 us -> 250 us (1.068)
  waiting for transfers between devices: 84.8 us -> 120 us
  starting transfers between devices: 49.1 us -> 31.8 us
  blocking collectives: 50.5 us -> 47.6 us
    all_gather x0 -> x1, waiting for transfers between devices: none -> 21.1 us  [layer(): down_all = lax.all_gather(down_weight[0], 'tp', axis_index_groups=groups)]
    all_gather x1, waiting for transfers between devices: 13.7 us -> 30.5 us  [layer(): lax.all_gather(arrived, 'tp', axis=0, axis_index_groups=groups, tiled=True)]
    ppermute x3, starting transfers between devices: 16.2 us -> 6.73 us  [swap_cores(): return lax.ppermute(x, 'tp', [(i, i ^ 1) for i in range(size)])]
    all_to_all x1 -> x0, waiting for transfers between devices: 9.38 us -> none  [layer(): lax.all_to_all(down_part.reshape(chips, CORES * hidden, -1), 'tp', 0, 0,...]
    all_to_all x1 -> x0, starting transfers between devices: 7.9 us -> none  [layer(): lax.all_to_all(down_part.reshape(chips, CORES * hidden, -1), 'tp', 0, 0,...]
    reduce_scatter x1, waiting for transfers between devices: 41.1 us -> 46.2 us  [layer(): lax.psum_scatter(summed, 'tp', scatter_dimension=0, axis_index_groups=gro...]
    all_to_all x1, blocking collectives: 18.3 us -> 15.3 us  [layer(): arrived = lax.all_to_all(outgoing.reshape(packed), 'sp', 0, 0, tiled=True)]
  transfers between devices with their start and end apart: 10 -> 10, of which waited for: 6 -> 6; matrix products, arithmetic and copies ran while one was open for 3% -> 4% of each run, Pallas kernels for 3% -> 5%
where the time goes in v9:
time: 250 us; the launch traced here: 246 us
  waiting for transfers between devices  120 us (48%)
  blocking collectives  47.6 us (19%)
  starting transfers between devices  31.8 us (13%)
  Pallas kernels  20.3 us (8%)
  between operations  13.3 us (5%)
  local copies, waits for them, and re-layouts  9.79 us (4%)
  other arithmetic  2.88 us (1%)
    reduce_scatter x1, waiting for transfers between devices, layer(): lax.psum_scatter(summed, 'tp', scatter_dimension=0, axis_index_groups=gro...  46.2 us
    all_gather x1, waiting for transfers between devices, layer(): lax.all_gather(arrived, 'tp', axis=0, axis_index_groups=groups, tiled=True)  30.5 us
    all_to_all x1, blocking collectives, layer(): returned = lax.all_to_all(result.reshape(packed), 'sp', 0, 0, tiled=True)  21.3 us
    all_gather x1, waiting for transfers between devices, layer(): down_all = lax.all_gather(down_weight[0], 'tp', axis_index_groups=groups)  21.1 us
    all_to_all x1, blocking collectives, layer(): arrived = lax.all_to_all(outgoing.reshape(packed), 'sp', 0, 0, tiled=True)  15.3 us
    all_to_all x1, starting transfers between devices, layer(): pieces = lax.all_to_all(total, 'sp', 0, 0, tiled=True)  14.2 us
    all_to_all x1, waiting for transfers between devices, layer(): lax.all_to_all(partial.reshape(tp // QUAD, rows_dev, width), 'tp', 0, 0,...  11.5 us
    all_to_all x1, blocking collectives, layer(): lax.all_to_all(branch, 'tp', 0, 0, axis_index_groups=quads, tiled=True)  11 us
  transfers between devices with their start and end apart: 10, of which 6 were waited for; matrix products, arithmetic and copies ran while one was open for 4% of the time, Pallas kernels for 5%

profile of v9, /device:TPU:1, one launch (start us, length us, event | category | flops | bytes accessed | tf_op | source)
XLA Modules:
  0.0 245.9 jit_solution(9128766457550350644)
XLA Ops:
  6.5 0.0 copy-start
  6.5 0.0 all-gather.4.cloned.1.call-start
  6.5 0.7 all-gather.4.cloned.1.call-update
  7.3 0.0 all-gather.8.cloned.1.call-start
  7.3 0.7 all-gather.8.cloned.1.call-update
  8.0 0.7 slice.3
  8.7 3.9 %collective-permute-start = (bf16[16,128]{1,0:T(8,128)(2,1)S(1)}, bf16[16,128]{1,0:T(8,128)(2,1)S(1)}, u32[]{:S(2)}, u32[]{:S(2)}) collective-permute-start(bf16[16,128]{1,0:T(8,128)(2,1)S(1)} %slice.3), channel_id=1, source_target_pairs={{0,16},{16,32},{32,48},{48,64},{64,80},{80,96},{96,112},{112,128},... | collective-permute-start | bytes 12296 | tf_op jit(solution)/shard_map/ppermute | solution.py:27
  12.6 0.7 collective-permute-done.rim_ref
  13.4 0.0 copy-start.6
  13.4 0.6 copy-done.6
  14.0 3.2 %recurrence.1 = (f32[512,128]{1,0:T(8,128)}, f32[512,128]{1,0:T(8,128)}, f32[32,2,128]{2,1,0:T(2,128)}) custom-call(bf16[512,128]{1,0:T(8,128)(2,1)} %x_ref.1, bf16[16,128]{1,0:T(8,128)(2,1)} %copy-done.6, f32[4,128]{1,0:T(4,128)} %filter_ref.1, bf16[2,64,64]{2,1,0:T(8,128)(2,1)} %recur_ref.1, bf16[2,64,64]{2,1,0:T(8,128)(2,1)} %input_ref.1, ...), custom_call_target="tpu_custom_call" | custom-call | flops 1000000000 | bytes 1048576 | tf_op jit(solution)/shard_map/recurrence/pallas_call | solution.py:253
  17.1 14.2 %all-to-all-start = ((f32[32,2,128]{2,1,0:T(2,128)}), f32[32,2,128]{2,1,0:T(2,128)S(1)}, u32[]{:S(2)}, u32[]{:S(2)}) async-start(f32[32,2,128]{2,1,0:T(2,128)} %get-tuple-element.18), calls=%async_computation | async-start | bytes 65536 | tf_op jit(solution)/shard_map/all_to_all | solution.py:268
  31.4 8.7 %all-to-all-done.pieces_ref = f32[32,2,128]{2,1,0:T(2,128)S(1)} async-done(((f32[32,2,128]{2,1,0:T(2,128)}), f32[32,2,128]{2,1,0:T(2,128)S(1)}, u32[]{:S(2)}, u32[]{:S(2)}) %all-to-all-start) | async-done | bytes 32800 | tf_op jit(solution)/shard_map/all_to_all | solution.py:268
  40.1 0.0 copy-start.4
  40.1 0.6 copy-done.4
  40.7 1.9 branch.1
  42.6 0.0 copy-start.5
  42.6 11.0 %all_to_all.25.branch_ref = bf16[4,128,128]{2,1,0:T(8,128)(2,1)} all-to-all(bf16[4,128,128]{2,1,0:T(8,128)(2,1)} %branch.1), channel_id=1, replica_groups={{0,1,2,3},{4,5,6,7},{8,9,10,11},{12,13,14,15},{16,17,18,19},{20,21,22,2..., dimensions={0} | all-to-all | bytes 262144 | tf_op jit(solution)/shard_map/all_to_all | solution.py:290
  53.5 0.0 all-gather.4.cloned.1.call-done.weight_ref
  53.5 2.6 %project.1 = bf16[128,2048]{1,0:T(8,128)(2,1)} custom-call(bf16[4,128,128]{2,1,0:T(8,128)(2,1)} %all_to_all.25.branch_ref, bf16[512,2048]{1,0:T(8,128)(2,1)} %all-gather.4.cloned.1.call-done.weight_ref), custom_call_target="tpu_custom_call" | custom-call | tf_op jit(solution)/shard_map/project/pallas_call | solution.py:292
  56.1 6.8 %all-to-all-start.2 = ((bf16[4,32,2048]{2,1,0:T(8,128)(2,1)}), bf16[4,32,2048]{2,1,0:T(8,128)(2,1)S(1)}, u32[]{:S(2)}, u32[]{:S(2)}) async-start(bf16[4,32,2048]{2,1,0:T(8,128)(2,1)} %bitcast.20), calls=%async_computation.2 | async-start | bytes 1048576 | tf_op jit(solution)/shard_map/all_to_all | solution.py:303
  62.9 0.0 copy-start.2
  62.9 0.0 copy-start.3
  62.9 0.0 all-gather.6.cloned.1.call-start
  63.0 0.0 copy-done
  63.0 0.1 constant_dynamic-slice_fusion.1
  63.1 0.7 copy.24.routes_ref
  63.8 0.0 copy-done.5
  63.8 0.7 copy.22.weight_ref
  64.5 1.7 slots.1
  66.2 11.5 %all-to-all-done.2.parts_ref = bf16[4,32,2048]{2,1,0:T(8,128)(2,1)S(1)} async-done(((bf16[4,32,2048]{2,1,0:T(8,128)(2,1)}), bf16[4,32,2048]{2,1,0:T(8,128)(2,1)S(1)}, u32[]{:S(2)}, u32[]{:S(2)}) %all-to-all-start.2) | async-done | bytes 524320 | tf_op jit(solution)/shard_map/all_to_all | solution.py:303
  77.7 0.0 copy-start.1
  77.7 0.8 copy-done.1
  78.5 2.4 dispatch.1
  80.9 15.3 %all_to_all.26 = bf16[32,24,256]{2,1,0:T(8,128)(2,1)S(1)} all-to-all(bf16[32,24,256]{2,1,0:T(8,128)(2,1)} %bitcast.27), channel_id=1, replica_groups=mesh['sp'=32,'tp'=16] {'sp'}, dimensions={0} | all-to-all | bytes 786432 | tf_op jit(solution)/shard_map/all_to_all | solution.py:319
  96.2 0.9 reshape.25
  97.2 0.0 all-gather.6.cloned.1.call-update
  97.2 0.0 reduce-scatter.2.cloned.1.call-start
  97.3 21.1 %all-gather.8.cloned.1.call-done = bf16[8,2048,128]{2,1,0:T(8,128)(2,1)} async-done(((bf16[1,2048,128]{2,1,0:T(8,128)(2,1)}), bf16[8,2048,128]{2,1,0:T(8,128)(2,1)}) %all-gather.8.cloned.1.call-update) | async-done | bytes 4194320 | tf_op jit(solution)/shard_map/all_gather | solution.py:269
  118.4 1.1 constant_dynamic-slice_fusion
  119.5 2.4 collective-permute-start.3
  121.9 0.0 copy-done.2
  121.9 1.9 collective-permute-start.1
  123.8 0.0 copy-done.3
  123.8 2.4 collective-permute-start.2
  126.2 1.1 fusion
  127.3 0.0 collective-permute-done.3
  127.4 0.1 maximum_select_fusion.2
  127.5 1.4 copy.27
  128.8 0.0 collective-permute-done.1
  128.8 1.3 maximum_select_fusion.gate_ref
  130.2 0.0 collective-permute-done.2
  130.2 1.4 maximum_select_fusion.1.up_ref
  131.6 30.5 %all-gather.6.cloned.1.call-done.rows_ref = bf16[768,2048]{1,0:T(8,128)(2,1)} async-done(((bf16[96,2048]{1,0:T(8,128)(2,1)}), bf16[768,2048]{1,0:T(8,128)(2,1)}) %all-gather.6.cloned.1.call-update) | async-done | bytes 3145744 | tf_op jit(solution)/shard_map/all_gather | solution.py:322
  162.1 6.4 %experts.1 = bf16[768,2048]{1,0:T(8,128)(2,1)} custom-call(bf16[768,2048]{1,0:T(8,128)(2,1)} %all-gather.6.cloned.1.call-done.rows_ref, bf16[2048,256]{1,0:T(8,128)(2,1)} %maximum_select_fusion.gate_ref, bf16[2048,256]{1,0:T(8,128)(2,1)} %maximum_select_fusion.1.up_ref, bf16[256,2048]{1,0:T(8,128)(2,1)} %bitcast.18), custom_call_target="tpu_custom_call" | custom-call | tf_op jit(solution)/shard_map/experts/pallas_call | solution.py:336
  168.5 0.0 reduce-scatter.2.cloned.1.call-update
  168.5 46.2 %reduce-scatter.2.cloned.1.call-done = bf16[96,2048]{1,0:T(8,128)(2,1)} async-done(((bf16[768,2048]{1,0:T(8,128)(2,1)}), bf16[96,2048]{1,0:T(8,128)(2,1)}) %reduce-scatter.2.cloned.1.call-update) | async-done | bytes 393232 | tf_op jit(solution)/shard_map/reduce_scatter | solution.py:349
  214.8 1.2 reshape.27
  216.0 21.3 %all_to_all.27 = bf16[32,24,256]{2,1,0:T(8,128)(2,1)} all-to-all(bf16[32,24,256]{2,1,0:T(8,128)(2,1)S(1)} %reshape.27), channel_id=1, replica_groups=mesh['sp'=32,'tp'=16] {'sp'}, dimensions={0} | all-to-all | bytes 786432 | tf_op jit(solution)/shard_map/all_to_all | solution.py:353
  237.3 2.1 combine.1
Async XLA Ops:
  6.5 56.5 %copy-start = (s32[512,2]{0,1:T(2,128)S(1)}, s32[512,2]{0,1:T(2,128)}, u32[]{:S(2)}) copy-start(s32[512,2]{0,1:T(2,128)} %param.25) | copy-start | bytes 12292
  6.5 47.0 %all-gather.4.cloned.1.call-start = ((), (), s32[]{:S(2)}) async-start(), calls=%async_computation.6 | async-start | bytes 2621440 | tf_op jit(solution)/shard_map/all_gather | solution.py:238
  7.3 111.1 %all-gather.8.cloned.1.call-start = ((), (), s32[]{:S(2)}) async-start(), calls=%async_computation.8 | async-start | bytes 4718592 | tf_op jit(solution)/shard_map/all_gather | solution.py:269
  8.7 4.7 %collective-permute-start = (bf16[16,128]{1,0:T(8,128)(2,1)S(1)}, bf16[16,128]{1,0:T(8,128)(2,1)S(1)}, u32[]{:S(2)}, u32[]{:S(2)}) collective-permute-start(bf16[16,128]{1,0:T(8,128)(2,1)S(1)} %slice.3), channel_id=1, source_target_pairs={{0,16},{16,32},{32,48},{48,64},{64,80},{80,96},{96,112},{112,128},... | collective-permute-start | bytes 12296 | tf_op jit(solution)/shard_map/ppermute | solution.py:27
  13.4 0.6 copy-start.6
  17.1 22.9 %all-to-all-start = ((f32[32,2,128]{2,1,0:T(2,128)}), f32[32,2,128]{2,1,0:T(2,128)S(1)}, u32[]{:S(2)}, u32[]{:S(2)}) async-start(f32[32,2,128]{2,1,0:T(2,128)} %get-tuple-element.18), calls=%async_computation | async-start | bytes 65536 | tf_op jit(solution)/shard_map/all_to_all | solution.py:268
  40.1 0.6 copy-start.4
  42.6 21.2 %copy-start.5 = (f32[32,2]{0,1:T(2,128)S(1)}, f32[32,2]{0,1:T(2,128)}, u32[]{:S(2)}) copy-start(f32[32,2]{0,1:T(2,128)} %param.26) | copy-start | bytes 772
  56.1 21.6 %all-to-all-start.2 = ((bf16[4,32,2048]{2,1,0:T(8,128)(2,1)}), bf16[4,32,2048]{2,1,0:T(8,128)(2,1)S(1)}, u32[]{:S(2)}, u32[]{:S(2)}) async-start(bf16[4,32,2048]{2,1,0:T(8,128)(2,1)} %bitcast.20), calls=%async_computation.2 | async-start | bytes 1048576 | tf_op jit(solution)/shard_map/all_to_all | solution.py:303
  62.9 58.9 %copy-start.2 = (bf16[1,2048,128]{2,1,0:T(8,128)(2,1)S(1)}, bf16[1,2048,128]{2,1,0:T(8,128)(2,1)}, u32[]{:S(2)}) copy-start(bf16[1,2048,128]{2,1,0:T(8,128)(2,1)} %param.27) | copy-start | bytes 1572868
  62.9 60.9 %copy-start.3 = (bf16[1,2048,128]{2,1,0:T(8,128)(2,1)S(1)}, bf16[1,2048,128]{2,1,0:T(8,128)(2,1)}, u32[]{:S(2)}) copy-start(bf16[1,2048,128]{2,1,0:T(8,128)(2,1)} %param.28) | copy-start | bytes 1572868
  62.9 99.2 %all-gather.6.cloned.1.call-start = ((), (), s32[]{:S(2)}) async-start(), calls=%async_computation.7 | async-start | bytes 3538944 | tf_op jit(solution)/shard_map/all_gather | solution.py:322
  77.7 0.8 copy-start.1
  97.2 117.6 %reduce-scatter.2.cloned.1.call-start = ((), (), s32[]{:S(2)}) async-start(), calls=%async_computation.9 | async-start | bytes 3538944 | tf_op jit(solution)/shard_map/reduce_scatter | solution.py:349
  119.5 7.9 %collective-permute-start.3 = (bf16[8,256,128]{2,1,0:T(8,128)(2,1)S(1)}, bf16[8,256,128]{2,1,0:T(8,128)(2,1)S(1)}, u32[]{:S(2)}, u32[]{:S(2)}) collective-permute-start(bf16[8,256,128]{2,1,0:T(8,128)(2,1)S(1)} %constant_dynamic-slice_fusion), channel_id=1, source_target_pairs={{0,1},{1,0},{2,3},{3,2},{4,5},{5,4},{6,7},{7,6},{8,9},{9,8},{10,11... | collective-permute-start | bytes 1572872 | tf_op jit(solution)/shard_map/ppermute | solution.py:36
  121.9 7.0 %collective-permute-start.1 = (bf16[2048,128]{1,0:T(8,128)(2,1)S(1)}, bf16[2048,128]{1,0:T(8,128)(2,1)S(1)}, u32[]{:S(2)}, u32[]{:S(2)}) collective-permute-start(bf16[2048,128]{1,0:T(8,128)(2,1)S(1)} %bitcast.22), channel_id=1, source_target_pairs={{0,1},{1,0},{2,3},{3,2},{4,5},{5,4},{6,7},{7,6},{8,9},{9,8},{10,11... | collective-permute-start | bytes 1572872 | tf_op jit(solution)/shard_map/ppermute | solution.py:36
  123.8 6.3 %collective-permute-start.2 = (bf16[2048,128]{1,0:T(8,128)(2,1)S(1)}, bf16[2048,128]{1,0:T(8,128)(2,1)S(1)}, u32[]{:S(2)}, u32[]{:S(2)}) collective-permute-start(bf16[2048,128]{1,0:T(8,128)(2,1)S(1)} %bitcast.24), channel_id=1, source_target_pairs={{0,1},{1,0},{2,3},{3,2},{4,5},{5,4},{6,7},{7,6},{8,9},{9,8},{10,11... | collective-permute-start | bytes 1572872 | tf_op jit(solution)/shard_map/ppermute | solution.py:36
Sparse Core Ops, SparseCore 0:
  9.4 40.3 all-gather.3
  51.9 66.4 all-gather.7
  120.5 41.6 all-gather.5
  168.7 46.0 reduce-scatter.1

commit v10 on v8

--- a/solution.py
+++ b/solution.py
@@ -267,6 +267,8 @@
     )(*operands)
 
     pieces = lax.all_to_all(total, "sp", 0, 0, tiled=True)
+    held = lax.optimization_barrier((gate_weight[0], up_weight[0], total))
+    gate_other, up_other = swap_cores(held[0]), swap_cores(held[1])
     own_routes = lax.dynamic_slice_in_dim(routes, here * rows_dev, rows_dev, 0)
     own_routes, pair = lax.optimization_barrier((own_routes, expert_pair_weight, total))[:2]
     column, line, pair = pl.pallas_call(
@@ -320,16 +322,16 @@
     arrived = arrived.reshape(slot_count, width)
 
     rows = lax.all_gather(arrived, "tp", axis=0, axis_index_groups=groups, tiled=True)
-    arrived, down_part, gate_own, up_own = lax.optimization_barrier(
-        (arrived, down_weight[0], gate_weight[0], up_weight[0])
+    arrived, down_part, gate_own, up_own, gate_other, up_other = lax.optimization_barrier(
+        (arrived, down_weight[0], gate_weight[0], up_weight[0], gate_other, up_other)
     )
     hidden = gate_own.shape[1]
     down_own = lax.all_to_all(
         down_part.reshape(chips, CORES * hidden, -1), "tp", 0, 0,
         axis_index_groups=groups, tiled=True,
     )
-    gate = natural(gate_own, swap_cores(gate_own), core, 1)
-    upward = natural(up_own, swap_cores(up_own), core, 1)
+    gate = natural(gate_own, gate_other, core, 1)
+    upward = natural(up_own, up_other, core, 1)
     down = natural(down_own[:, None], swap_cores(down_own)[:, None], core, 1)
     down = jnp.moveaxis(down.reshape(tp, CORES * hidden, -1), 0, 1).reshape(CORES * hidden, width)
     depth = CORES * hidden

time: 234 us -> 241 us (1.030)
  blocking collectives: 50.5 us -> 80.7 us
  starting transfers between devices: 49.1 us -> 35.4 us
  waiting for transfers between devices: 84.8 us -> 76.1 us
    all_to_all x0 -> x1, blocking collectives: none -> 30.2 us  [layer(): lax.all_to_all(down_part.reshape(chips, CORES * hidden, -1), 'tp', 0, 0,...]
    all_to_all x1 -> x0, waiting for transfers between devices: 9.38 us -> none  [layer(): lax.all_to_all(down_part.reshape(chips, CORES * hidden, -1), 'tp', 0, 0,...]
    all_to_all x1 -> x0, starting transfers between devices: 7.9 us -> none  [layer(): lax.all_to_all(down_part.reshape(chips, CORES * hidden, -1), 'tp', 0, 0,...]
    ppermute x3, starting transfers between devices: 16.2 us -> 10.2 us  [swap_cores(): return lax.ppermute(x, 'tp', [(i, i ^ 1) for i in range(size)])]
    all_gather x1, waiting for transfers between devices: 13.7 us -> 9.37 us  [layer(): lax.all_gather(arrived, 'tp', axis=0, axis_index_groups=groups, tiled=True)]
    reduce_scatter x1, waiting for transfers between devices: 41.1 us -> 44.1 us  [layer(): lax.psum_scatter(summed, 'tp', scatter_dimension=0, axis_index_groups=gro...]
  transfers between devices with their start and end apart: 10 -> 9, of which waited for: 6 -> 6; matrix products, arithmetic and copies ran while one was open for 3% -> 3% of each run, Pallas kernels for 3% -> 3%
where the time goes in v10:
time: 241 us; the launch traced here: 237 us
  blocking collectives  80.7 us (33%)
  waiting for transfers between devices  76.1 us (32%)
  starting transfers between devices  35.4 us (15%)
  Pallas kernels  20.4 us (8%)
  between operations  13.2 us (5%)
  local copies, waits for them, and re-layouts  8.7 us (4%)
    reduce_scatter x1, waiting for transfers between devices, layer(): lax.psum_scatter(summed, 'tp', scatter_dimension=0, axis_index_groups=gro...  44.1 us
    all_to_all x1, blocking collectives, layer(): lax.all_to_all(down_part.reshape(chips, CORES * hidden, -1), 'tp', 0, 0,...  30.2 us
    all_to_all x1, blocking collectives, layer(): returned = lax.all_to_all(result.reshape(packed), 'sp', 0, 0, tiled=True)  21.2 us
    all_to_all x1, blocking collectives, layer(): arrived = lax.all_to_all(outgoing.reshape(packed), 'sp', 0, 0, tiled=True)  18.3 us
    all_to_all x1, starting transfers between devices, layer(): pieces = lax.all_to_all(total, 'sp', 0, 0, tiled=True)  14.2 us
    all_to_all x1, blocking collectives, layer(): lax.all_to_all(branch, 'tp', 0, 0, axis_index_groups=quads, tiled=True)  11 us
    all_to_all x1, waiting for transfers between devices, layer(): lax.all_to_all(partial.reshape(tp // QUAD, rows_dev, width), 'tp', 0, 0,...  10.5 us
    ppermute x3, starting transfers between devices, swap_cores(): return lax.ppermute(x, 'tp', [(i, i ^ 1) for i in range(size)])  10.2 us
  transfers between devices with their start and end apart: 9, of which 6 were waited for; matrix products, arithmetic and copies ran while one was open for 3% of the time, Pallas kernels for 3%

profile of v10, /device:TPU:1, one launch (start us, length us, event | category | flops | bytes accessed | tf_op | source)
XLA Modules:
  0.0 236.8 jit_solution(17576077781649908441)
XLA Ops:
  6.5 0.0 copy-start
  6.5 0.0 all-gather.3.cloned.1.call-start
  6.5 0.7 all-gather.3.cloned.1.call-update
  7.3 0.7 slice.3
  8.0 3.9 %collective-permute-start = (bf16[16,128]{1,0:T(8,128)(2,1)S(1)}, bf16[16,128]{1,0:T(8,128)(2,1)S(1)}, u32[]{:S(2)}, u32[]{:S(2)}) collective-permute-start(bf16[16,128]{1,0:T(8,128)(2,1)S(1)} %slice.3), channel_id=1, source_target_pairs={{0,16},{16,32},{32,48},{48,64},{64,80},{80,96},{96,112},{112,128},... | collective-permute-start | bytes 12296 | tf_op jit(solution)/shard_map/ppermute | solution.py:27
  11.9 0.7 collective-permute-done.rim_ref
  12.6 0.0 copy-start.7
  12.6 0.6 copy-done.7
  13.2 3.2 %recurrence.1 = (f32[512,128]{1,0:T(8,128)}, f32[512,128]{1,0:T(8,128)}, f32[32,2,128]{2,1,0:T(2,128)}) custom-call(bf16[512,128]{1,0:T(8,128)(2,1)} %x_ref.1, bf16[16,128]{1,0:T(8,128)(2,1)} %copy-done.7, f32[4,128]{1,0:T(4,128)} %filter_ref.1, bf16[2,64,64]{2,1,0:T(8,128)(2,1)} %recur_ref.1, bf16[2,64,64]{2,1,0:T(8,128)(2,1)} %input_ref.1, ...), custom_call_target="tpu_custom_call" | custom-call | flops 1000000000 | bytes 1048576 | tf_op jit(solution)/shard_map/recurrence/pallas_call | solution.py:254
  16.4 14.2 %all-to-all-start = ((f32[32,2,128]{2,1,0:T(2,128)}), f32[32,2,128]{2,1,0:T(2,128)S(1)}, u32[]{:S(2)}, u32[]{:S(2)}) async-start(f32[32,2,128]{2,1,0:T(2,128)} %get-tuple-element.22), calls=%async_computation | async-start | bytes 65536 | tf_op jit(solution)/shard_map/all_to_all | solution.py:269
  30.6 8.7 %all-to-all-done.pieces_ref = f32[32,2,128]{2,1,0:T(2,128)S(1)} async-done(((f32[32,2,128]{2,1,0:T(2,128)}), f32[32,2,128]{2,1,0:T(2,128)S(1)}, u32[]{:S(2)}, u32[]{:S(2)}) %all-to-all-start) | async-done | bytes 32800 | tf_op jit(solution)/shard_map/all_to_all | solution.py:269
  39.3 0.0 copy-start.5
  39.3 0.6 copy-done.5
  39.9 1.9 branch.1
  41.8 0.0 copy-start.6
  41.8 11.0 %all_to_all.30.branch_ref = bf16[4,128,128]{2,1,0:T(8,128)(2,1)} all-to-all(bf16[4,128,128]{2,1,0:T(8,128)(2,1)} %branch.1), channel_id=1, replica_groups={{0,1,2,3},{4,5,6,7},{8,9,10,11},{12,13,14,15},{16,17,18,19},{20,21,22,2..., dimensions={0} | all-to-all | bytes 262144 | tf_op jit(solution)/shard_map/all_to_all | solution.py:292
  52.8 0.0 all-gather.3.cloned.1.call-done.weight_ref
  52.8 2.6 %project.1 = bf16[128,2048]{1,0:T(8,128)(2,1)} custom-call(bf16[4,128,128]{2,1,0:T(8,128)(2,1)} %all_to_all.30.branch_ref, bf16[512,2048]{1,0:T(8,128)(2,1)} %all-gather.3.cloned.1.call-done.weight_ref), custom_call_target="tpu_custom_call" | custom-call | tf_op jit(solution)/shard_map/project/pallas_call | solution.py:294
  55.4 0.0 copy-start.2
  55.4 0.0 copy-start.3
  55.4 0.0 copy-start.4
  55.4 7.0 %all-to-all-start.2 = ((bf16[4,32,2048]{2,1,0:T(8,128)(2,1)}), bf16[4,32,2048]{2,1,0:T(8,128)(2,1)S(1)}, u32[]{:S(2)}, u32[]{:S(2)}) async-start(bf16[4,32,2048]{2,1,0:T(8,128)(2,1)} %bitcast.22), calls=%async_computation.2 | async-start | bytes 1048576 | tf_op jit(solution)/shard_map/all_to_all | solution.py:305
  62.4 0.0 all-gather.5.cloned.1.call-start
  62.4 0.0 copy-done
  62.4 0.1 constant_dynamic-slice_fusion
  62.5 0.7 copy.19.routes_ref
  63.2 0.0 copy-done.6
  63.2 0.7 copy.17.weight_ref
  63.8 1.7 slots.1
  65.6 10.5 %all-to-all-done.2.parts_ref = bf16[4,32,2048]{2,1,0:T(8,128)(2,1)S(1)} async-done(((bf16[4,32,2048]{2,1,0:T(8,128)(2,1)}), bf16[4,32,2048]{2,1,0:T(8,128)(2,1)S(1)}, u32[]{:S(2)}, u32[]{:S(2)}) %all-to-all-start.2) | async-done | bytes 524320 | tf_op jit(solution)/shard_map/all_to_all | solution.py:305
  76.1 0.0 copy-start.1
  76.1 0.8 copy-done.1
  76.9 2.4 %dispatch.1 = (bf16[32,2048]{1,0:T(8,128)(2,1)}, bf16[768,256]{1,0:T(8,128)(2,1)}) custom-call(bf16[4,32,2048]{2,1,0:T(8,128)(2,1)} %copy-done.1, bf16[32,2048]{1,0:T(8,128)(2,1)} %resid_ref.1, f32[1,2048]{1,0:T(1,128)} %bitcast.31, s32[2,256]{1,0:T(2,128)} %get-tuple-element.27.line_ref), custom_call_target="tpu_custom_call" | custom-call | tf_op jit(solution)/shard_map/dispatch/pallas_call | solution.py:310
  79.3 18.3 %all_to_all.31 = bf16[32,24,256]{2,1,0:T(8,128)(2,1)S(1)} all-to-all(bf16[32,24,256]{2,1,0:T(8,128)(2,1)} %bitcast.30), channel_id=1, replica_groups=mesh['sp'=32,'tp'=16] {'sp'}, dimensions={0} | all-to-all | bytes 786432 | tf_op jit(solution)/shard_map/all_to_all | solution.py:321
  97.6 0.9 reshape.28
  98.5 0.0 all-gather.5.cloned.1.call-update
  98.6 0.0 reduce-scatter.2.cloned.1.call-start
  98.6 0.0 copy-done.2
  98.6 5.5 %collective-permute-start.1 = (bf16[2048,128]{1,0:T(8,128)(2,1)S(1)}, bf16[2048,128]{1,0:T(8,128)(2,1)S(1)}, u32[]{:S(2)}, u32[]{:S(2)}) collective-permute-start(bf16[2048,128]{1,0:T(8,128)(2,1)S(1)} %bitcast.24), channel_id=1, source_target_pairs={{0,1},{1,0},{2,3},{3,2},{4,5},{5,4},{6,7},{7,6},{8,9},{9,8},{10,11... | collective-permute-start | bytes 1572872 | tf_op jit(solution)/shard_map/ppermute | solution.py:36
  104.1 0.0 copy-done.3
  104.1 1.9 collective-permute-start.2
  106.0 0.0 collective-permute-done.1
  106.0 1.9 collective-permute-done.2
  107.9 0.0 copy-done.4
  107.9 30.2 %all_to_all.32 = bf16[8,256,128]{2,1,0:T(8,128)(2,1)S(1)} all-to-all(bf16[8,256,128]{2,1,0:T(8,128)(2,1)S(1)} %bitcast.29), channel_id=1, replica_groups={{0,2,4,6,8,10,12,14},{1,3,5,7,9,11,13,15},{16,18,20,22,24,26,28,30},{17..., dimensions={0} | all-to-all | bytes 1048576 | tf_op jit(solution)/shard_map/all_to_all | solution.py:329
  138.1 2.9 %collective-permute-start.3 = (bf16[8,256,128]{2,1,0:T(8,128)(2,1)S(1)}, bf16[8,256,128]{2,1,0:T(8,128)(2,1)S(1)}, u32[]{:S(2)}, u32[]{:S(2)}) collective-permute-start(bf16[8,256,128]{2,1,0:T(8,128)(2,1)S(1)} %all_to_all.32), channel_id=1, source_target_pairs={{0,1},{1,0},{2,3},{3,2},{4,5},{5,4},{6,7},{7,6},{8,9},{9,8},{10,11... | collective-permute-start | bytes 1572872 | tf_op jit(solution)/shard_map/ppermute | solution.py:36
  141.0 2.2 maximum_select_fusion
  143.2 0.0 collective-permute-done.3
  143.2 0.2 maximum_select_fusion.2
  143.3 1.1 copy.18
  144.4 1.3 copy.22
  145.8 9.4 %all-gather.5.cloned.1.call-done.rows_ref = bf16[768,2048]{1,0:T(8,128)(2,1)} async-done(((bf16[96,2048]{1,0:T(8,128)(2,1)}), bf16[768,2048]{1,0:T(8,128)(2,1)}) %all-gather.5.cloned.1.call-update) | async-done | bytes 3145744 | tf_op jit(solution)/shard_map/all_gather | solution.py:324
  155.2 6.5 %experts.1 = bf16[768,2048]{1,0:T(8,128)(2,1)} custom-call(bf16[768,2048]{1,0:T(8,128)(2,1)} %all-gather.5.cloned.1.call-done.rows_ref, bf16[2048,256]{1,0:T(8,128)(2,1)} %get-tuple-element.39.gate_ref, bf16[2048,256]{1,0:T(8,128)(2,1)} %get-tuple-element.40.up_ref, bf16[256,2048]{1,0:T(8,128)(2,1)} %bitcast.19), custom_call_target="tpu_custom_call" | custom-call | tf_op jit(solution)/shard_map/experts/pallas_call | solution.py:339
  161.6 0.0 reduce-scatter.2.cloned.1.call-update
  161.6 44.1 %reduce-scatter.2.cloned.1.call-done = bf16[96,2048]{1,0:T(8,128)(2,1)} async-done(((bf16[768,2048]{1,0:T(8,128)(2,1)}), bf16[96,2048]{1,0:T(8,128)(2,1)}) %reduce-scatter.2.cloned.1.call-update) | async-done | bytes 393232 | tf_op jit(solution)/shard_map/reduce_scatter | solution.py:352
  205.8 1.2 reshape.31
  206.9 21.2 %all_to_all.33 = bf16[32,24,256]{2,1,0:T(8,128)(2,1)} all-to-all(bf16[32,24,256]{2,1,0:T(8,128)(2,1)S(1)} %reshape.31), channel_id=1, replica_groups=mesh['sp'=32,'tp'=16] {'sp'}, dimensions={0} | all-to-all | bytes 786432 | tf_op jit(solution)/shard_map/all_to_all | solution.py:356
  228.1 2.1 combine.1
Async XLA Ops:
  6.5 55.9 %copy-start = (s32[512,2]{0,1:T(2,128)S(1)}, s32[512,2]{0,1:T(2,128)}, u32[]{:S(2)}) copy-start(s32[512,2]{0,1:T(2,128)} %param.25) | copy-start | bytes 12292
  6.5 46.2 %all-gather.3.cloned.1.call-start = ((), (), s32[]{:S(2)}) async-start(), calls=%async_computation.7 | async-start | bytes 2621440 | tf_op jit(solution)/shard_map/all_gather | solution.py:239
  8.0 4.7 %collective-permute-start = (bf16[16,128]{1,0:T(8,128)(2,1)S(1)}, bf16[16,128]{1,0:T(8,128)(2,1)S(1)}, u32[]{:S(2)}, u32[]{:S(2)}) collective-permute-start(bf16[16,128]{1,0:T(8,128)(2,1)S(1)} %slice.3), channel_id=1, source_target_pairs={{0,16},{16,32},{32,48},{48,64},{64,80},{80,96},{96,112},{112,128},... | collective-permute-start | bytes 12296 | tf_op jit(solution)/shard_map/ppermute | solution.py:27
  12.6 0.6 copy-start.7
  16.4 22.9 %all-to-all-start = ((f32[32,2,128]{2,1,0:T(2,128)}), f32[32,2,128]{2,1,0:T(2,128)S(1)}, u32[]{:S(2)}, u32[]{:S(2)}) async-start(f32[32,2,128]{2,1,0:T(2,128)} %get-tuple-element.22), calls=%async_computation | async-start | bytes 65536 | tf_op jit(solution)/shard_map/all_to_all | solution.py:269
  39.3 0.6 copy-start.5
  41.8 21.3 %copy-start.6 = (f32[32,2]{0,1:T(2,128)S(1)}, f32[32,2]{0,1:T(2,128)}, u32[]{:S(2)}) copy-start(f32[32,2]{0,1:T(2,128)} %param.26) | copy-start | bytes 772
  55.4 43.2 %copy-start.2 = (bf16[1,2048,128]{2,1,0:T(8,128)(2,1)S(1)}, bf16[1,2048,128]{2,1,0:T(8,128)(2,1)}, u32[]{:S(2)}) copy-start(bf16[1,2048,128]{2,1,0:T(8,128)(2,1)} %param.27) | copy-start | bytes 1572868
  55.4 48.7 %copy-start.3 = (bf16[1,2048,128]{2,1,0:T(8,128)(2,1)S(1)}, bf16[1,2048,128]{2,1,0:T(8,128)(2,1)}, u32[]{:S(2)}) copy-start(bf16[1,2048,128]{2,1,0:T(8,128)(2,1)} %param.28) | copy-start | bytes 1572868
  55.4 52.5 %copy-start.4 = (bf16[1,2048,128]{2,1,0:T(8,128)(2,1)S(1)}, bf16[1,2048,128]{2,1,0:T(8,128)(2,1)}, u32[]{:S(2)}) copy-start(bf16[1,2048,128]{2,1,0:T(8,128)(2,1)} %param.29) | copy-start | bytes 1572868
  55.4 20.7 %all-to-all-start.2 = ((bf16[4,32,2048]{2,1,0:T(8,128)(2,1)}), bf16[4,32,2048]{2,1,0:T(8,128)(2,1)S(1)}, u32[]{:S(2)}, u32[]{:S(2)}) async-start(bf16[4,32,2048]{2,1,0:T(8,128)(2,1)} %bitcast.22), calls=%async_computation.2 | async-start | bytes 1048576 | tf_op jit(solution)/shard_map/all_to_all | solution.py:305
  62.4 92.8 %all-gather.5.cloned.1.call-start = ((), (), s32[]{:S(2)}) async-start(), calls=%async_computation.8 | async-start | bytes 3538944 | tf_op jit(solution)/shard_map/all_gather | solution.py:324
  76.1 0.8 copy-start.1
  98.6 107.2 %reduce-scatter.2.cloned.1.call-start = ((), (), s32[]{:S(2)}) async-start(), calls=%async_computation.9 | async-start | bytes 3538944 | tf_op jit(solution)/shard_map/reduce_scatter | solution.py:352
  98.6 7.4 %collective-permute-start.1 = (bf16[2048,128]{1,0:T(8,128)(2,1)S(1)}, bf16[2048,128]{1,0:T(8,128)(2,1)S(1)}, u32[]{:S(2)}, u32[]{:S(2)}) collective-permute-start(bf16[2048,128]{1,0:T(8,128)(2,1)S(1)} %bitcast.24), channel_id=1, source_target_pairs={{0,1},{1,0},{2,3},{3,2},{4,5},{5,4},{6,7},{7,6},{8,9},{9,8},{10,11... | collective-permute-start | bytes 1572872 | tf_op jit(solution)/shard_map/ppermute | solution.py:36
  104.1 3.8 %collective-permute-start.2 = (bf16[2048,128]{1,0:T(8,128)(2,1)S(1)}, bf16[2048,128]{1,0:T(8,128)(2,1)S(1)}, u32[]{:S(2)}, u32[]{:S(2)}) collective-permute-start(bf16[2048,128]{1,0:T(8,128)(2,1)S(1)} %bitcast.26), channel_id=1, source_target_pairs={{0,1},{1,0},{2,3},{3,2},{4,5},{5,4},{6,7},{7,6},{8,9},{9,8},{10,11... | collective-permute-start | bytes 1572872 | tf_op jit(solution)/shard_map/ppermute | solution.py:36
  138.1 5.0 %collective-permute-start.3 = (bf16[8,256,128]{2,1,0:T(8,128)(2,1)S(1)}, bf16[8,256,128]{2,1,0:T(8,128)(2,1)S(1)}, u32[]{:S(2)}, u32[]{:S(2)}) collective-permute-start(bf16[8,256,128]{2,1,0:T(8,128)(2,1)S(1)} %all_to_all.32), channel_id=1, source_target_pairs={{0,1},{1,0},{2,3},{3,2},{4,5},{5,4},{6,7},{7,6},{8,9},{9,8},{10,11... | collective-permute-start | bytes 1572872 | tf_op jit(solution)/shard_map/ppermute | solution.py:36
Sparse Core Ops, SparseCore 0:
  9.4 40.3 all-gather.2
  98.7 56.4 all-gather.4
  161.8 43.9 reduce-scatter.1
